TPU v7x, 256 devices: a whole 4x4x8 slice. The times are simulated.
256 devices in a mesh: sp: 64 (over z, y, core), tp: 4 (over x).
Axes of the slice: x: 4, y: 4, z: 8, core: 2. Of those that a mesh axis runs over, the one named last changes fastest.
Arguments:
- residual: bfloat16 [16384, 2048], P(('sp', 'tp')), may hold values from -6 to 6
- queries: bfloat16 [16384, 2048], P('sp', 'tp'), may hold values from -40 to 40
- key_rows: bfloat16 [16384, 1024], P('sp', 'tp'), may hold values from -40 to 40
- value_rows: bfloat16 [16384, 1024], P('sp', 'tp'), may hold values from -6 to 6
- forget_sums: float32 [16384, 16], P('sp', 'tp'), as said below
- out_weight: bfloat16 [2048, 2048], P('tp'), may hold values from -0.25 to 0.25
- norm_gain: float32 [2048], replicated, may hold values from 0.1 to 1.9
- expert_ids: int32 [16384, 4], P(('sp', 'tp')), may hold values from 0 to 63, all different within a row; in each aligned block of 64 rows (0 to 63, 64 to 127, ...) at most 8 rows name the same one
- route_weights: float32 [16384, 4], P(('sp', 'tp')), may hold values from 0.1 to 1
- expert_gate: bfloat16 [64, 2048, 384], P('sp'), may hold values from -0.125 to 0.125
- expert_up: bfloat16 [64, 2048, 384], P('sp'), may hold values from -0.125 to 0.125
- expert_down: bfloat16 [64, 384, 2048], P('sp'), may hold values from -0.3125 to 0.3125
- shared_gate: bfloat16 [2048, 384], replicated, may hold values from -0.125 to 0.125
- shared_up: bfloat16 [2048, 384], replicated, may hold values from -0.125 to 0.125
- shared_down: bfloat16 [384, 2048], replicated, may hold values from -0.3125 to 0.3125
Outputs:
- layer_out: bfloat16 [16384, 2048], P(('sp', 'tp'))
Inputs may be any that keep to these rules, and one draw needn't show every extreme that they name: `forget_sums`: each head's column never rises from one position to the next. `expert_ids`: each row names 4 different experts; among the rows of one device no expert is named more than 8 times.
All inputs are finite; a program needn't handle non-finite values.
Results may differ from a plain program's by a relative error of at most 0.014.
Values may be sent and summed in bfloat16 or wider, within the bound.
No kernel may reach another device: no remote copies, remote signals or barrier semaphores. Data moves between devices by JAX's collectives and lax.ppermute only.
A program may use at most 128 MiB of HBM per device.

v0:
```python
import math

import jax
import jax.numpy as jnp
from jax import lax
from jax.sharding import PartitionSpec as P

HEADS = 16
KV_HEADS = 8
HEAD_DIM = 128
TOPK = 4


routed_scale = 2.5
norm_eps = 1e-06


def from_everyone(x, axis):
    copies = jnp.broadcast_to(x, (lax.axis_size(axis), *x.shape))
    return lax.all_to_all(copies, axis, split_axis=0, concat_axis=0, tiled=True)


def laid_out(blocks, dim):
    blocks = jnp.moveaxis(blocks, 0, dim)
    dims = blocks.shape
    return blocks.reshape(*dims[:dim], dims[dim] * dims[dim + 1], *dims[dim + 2 :])


def gather_directly(x, axis, dim):
    blocks = from_everyone(x, axis)
    return laid_out(blocks, dim)


def in_one_piece(arrays, axis, dim, along):
    ends, at = ([], 0)
    for a in arrays[:-1]:
        at += a.shape[along]
        ends.append(at)
    both = jnp.concatenate(arrays, axis=along)
    return tuple(jnp.split(lax.all_gather(both, axis, axis=dim, tiled=True), ends, axis=along))


def absorb_group(carried, query_group, shard_piece, sum_piece, score_scale):
    query_heads, query_sums, query_pos, last_pos = query_group
    key_piece, value_piece = shard_piece
    piece_rows = key_piece.shape[0]
    query_count, local_kv, group_size, head_size = query_heads.shape
    key_block = math.gcd(piece_rows, 1024)
    key_heads = key_piece.reshape(piece_rows, local_kv, head_size)
    value_heads = value_piece.reshape(piece_rows, local_kv, head_size)
    key_sums = sum_piece.reshape(piece_rows, local_kv, group_size).transpose(1, 2, 0)

    def update(block_start, held):
        row_max, row_sum, weighted = held
        key_part = lax.dynamic_slice_in_dim(key_heads, block_start, key_block, 0)
        value_part = lax.dynamic_slice_in_dim(value_heads, block_start, key_block, 0)
        sums_part = lax.dynamic_slice_in_dim(key_sums, block_start, key_block, 2)
        scores = (
            jnp.einsum("qhgd,khd->hgqk", query_heads, key_part, preferred_element_type=jnp.float32)
            * score_scale
        )
        scores = scores + (query_sums[:, :, :, None] - sums_part[:, :, None, :])
        key_pos = block_start + jnp.arange(key_block, dtype=jnp.int32)
        allowed = query_pos[:, None] >= key_pos[None, :]
        scores = jnp.where(allowed, scores, -jnp.inf)
        new_max = jnp.maximum(row_max, jnp.max(scores, axis=3))
        weights = jnp.exp(scores - new_max[:, :, :, None])
        factor = jnp.exp(row_max - new_max)
        row_sum = row_sum * factor + jnp.sum(weights, axis=3)
        products = jnp.einsum(
            "hgqk,khd->qhgd",
            weights.astype(jnp.bfloat16),
            value_part,
            preferred_element_type=jnp.float32,
        )
        weighted = weighted * factor.transpose(2, 0, 1)[:, :, :, None] + products
        return (new_max, row_sum, weighted)

    def one_block(block_index, held):
        block_start = block_index * key_block
        needed = block_start <= last_pos
        return lax.cond(needed, lambda inner: update(block_start, inner), lambda inner: inner, held)

    return lax.fori_loop(0, piece_rows // key_block, one_block, carried)


def finish(carried):
    row_max, row_sum, weighted = carried
    mixed = weighted / row_sum.transpose(2, 0, 1)[:, :, :, None]
    return mixed.reshape(mixed.shape[0], -1).astype(jnp.bfloat16)


def local(
    residual,
    queries,
    key_rows,
    value_rows,
    forget_sums,
    out_weight,
    norm_gain,
    expert_ids,
    route_weights,
    expert_gate,
    expert_up,
    expert_down,
    shared_gate,
    shared_up,
    shared_down,
):
    sp_count = lax.axis_size("sp")
    sp_index = lax.axis_index("sp")
    local_rows = queries.shape[0]
    local_kv = key_rows.shape[1] // HEAD_DIM
    group_size = HEADS // KV_HEADS
    score_scale = HEAD_DIM ** (-0.5)
    own_first = sp_index * local_rows
    all_sums = gather_directly(forget_sums, "sp", 0)
    positions = own_first + jnp.arange(local_rows, dtype=jnp.int32)
    groups = [
        (
            queries.reshape(queries.shape[0], local_kv, group_size, HEAD_DIM),
            forget_sums.reshape(forget_sums.shape[0], local_kv, group_size).transpose(1, 2, 0),
            positions,
            positions[-1],
        )
    ]

    def initial(query_count):
        return (
            jnp.full((local_kv, group_size, query_count), -1e30, jnp.float32),
            jnp.zeros((local_kv, group_size, query_count), jnp.float32),
            jnp.zeros((query_count, local_kv, group_size, HEAD_DIM), jnp.float32),
        )

    def absorb(states, shard_piece):
        return tuple(
            (
                absorb_group(held, query_group, shard_piece, all_sums, score_scale)
                for held, query_group in zip(states, groups)
            )
        )

    start_states = tuple((initial(query_group[0].shape[0]) for query_group in groups))
    states = absorb(start_states, in_one_piece((key_rows, value_rows), "sp", 0, 1))
    outputs = [finish(held) for held in states]
    attended = outputs[0]
    rows_out = local_rows // lax.axis_size("tp")
    token_heads = lax.all_to_all(attended, "tp", split_axis=0, concat_axis=1, tiled=True)
    branch = jnp.dot(
        token_heads,
        lax.all_gather(out_weight, "tp", axis=0, tiled=True),
        preferred_element_type=jnp.float32,
    )
    stream = (residual.astype(jnp.float32) + branch).astype(jnp.bfloat16)
    wide = lax.optimization_barrier(stream).astype(jnp.float32)
    normed = (
        wide * lax.rsqrt(jnp.mean(wide * wide, axis=1, keepdims=True) + norm_eps) * norm_gain
    ).astype(jnp.bfloat16)
    width = normed.shape[1]
    experts_here = expert_gate.shape[0]
    total_experts = experts_here * sp_count
    capacity = 2 * rows_out * TOPK // total_experts
    flat_ids = expert_ids.reshape(-1)
    assigned = flat_ids.shape[0]
    onehot = (flat_ids[:, None] == jnp.arange(total_experts, dtype=jnp.int32)[None, :]).astype(
        jnp.int32
    )
    slot_rank = jnp.sum((jnp.cumsum(onehot, axis=0) - 1) * onehot, axis=1)
    target = flat_ids * capacity + slot_rank
    slot_count = total_experts * capacity
    source = (
        jnp.full((slot_count,), assigned, jnp.int32)
        .at[target]
        .set(jnp.arange(assigned, dtype=jnp.int32))
    )
    padded = jnp.concatenate([normed, jnp.zeros((1, width), jnp.bfloat16)], axis=0)
    outgoing = padded[source // TOPK].reshape(sp_count, experts_here, capacity, width)
    arrived = lax.all_to_all(outgoing, "sp", split_axis=0, concat_axis=0, tiled=True)
    gate_part = jnp.einsum(
        "necd,edf->necf", arrived, expert_gate, preferred_element_type=jnp.float32
    )
    up_part = jnp.einsum("necd,edf->necf", arrived, expert_up, preferred_element_type=jnp.float32)
    hidden = (jax.nn.silu(gate_part) * up_part).astype(jnp.bfloat16)
    processed = jnp.einsum(
        "necf,efd->necd", hidden, expert_down, preferred_element_type=jnp.float32
    ).astype(jnp.bfloat16)
    returned = lax.all_to_all(processed, "sp", split_axis=0, concat_axis=0, tiled=True)
    results = returned.reshape(slot_count, width)
    picked = results[target].reshape(rows_out, TOPK, width).astype(jnp.float32)
    gates = route_weights / jnp.sum(route_weights, axis=1, keepdims=True) * routed_scale
    routed = jnp.sum(gates[:, :, None] * picked, axis=1)
    shared_hidden = (
        jax.nn.silu(jnp.dot(normed, shared_gate, preferred_element_type=jnp.float32))
        * jnp.dot(normed, shared_up, preferred_element_type=jnp.float32)
    ).astype(jnp.bfloat16)
    shared_out = jnp.dot(shared_hidden, shared_down, preferred_element_type=jnp.float32)
    return (wide + shared_out + routed).astype(jnp.bfloat16)


def solution(mesh):
    in_specs = (
        P(("sp", "tp"), None),
        P("sp", "tp"),
        P("sp", "tp"),
        P("sp", "tp"),
        P("sp", "tp"),
        P("tp", None),
        P(),
        P(("sp", "tp"), None),
        P(("sp", "tp"), None),
        P("sp", None, None),
        P("sp", None, None),
        P("sp", None, None),
        P(),
        P(),
        P(),
    )
    out_specs = P(("sp", "tp"), None)
    return jax.shard_map(local, mesh=mesh, in_specs=in_specs, out_specs=out_specs, check_vma=False)
```

profile of v0, /device:TPU:8, one launch (start us, length us, event | category | flops | bytes accessed | tf_op | source)
XLA Modules:
  0.0 427.4 jit_solution(19748104873882279)
XLA Ops:
  6.5 0.0 copy-start
  6.5 0.0 all-gather.3.cloned.1.call-start
  6.6 1.1 copy.48
  7.7 1.0 copy.49
  8.7 0.7 pad_maximum_fusion
  9.5 0.0 all-gather.3.cloned.1.call-update
  9.5 0.0 all-gather.5.cloned.1.call-start
  9.5 0.7 all-gather.5.cloned.1.call-update
  10.2 1.4 broadcast_in_dim.29
  11.7 12.1 %all-to-all-start = ((f32[64,256,4]{1,2,0:T(4,128)}), f32[64,256,4]{1,2,0:T(4,128)S(1)}, u32[]{:S(2)}, u32[]{:S(2)}) async-start(f32[64,256,4]{1,2,0:T(4,128)} %broadcast_in_dim.29), calls=%async_computation | async-start | bytes 524288 | tf_op jit(solution)/shard_map/all_to_all | solution.py:20
  23.8 0.0 copy-done.5
  23.8 0.0 copy-done.6
  23.8 0.1 copy.58
  23.9 0.1 eq.29
  24.0 0.1 eq.25
  24.1 0.6 slice.9
  24.8 0.0 copy-done.3
  24.8 0.1 copy.50
  24.9 0.2 copy.53
  25.1 0.6 reduce-window.6
  25.7 0.2 slice_reduce_fusion
  26.0 0.1 copy.57
  26.1 0.1 mul.106
  26.2 0.1 fusion.76
  26.3 1.4 scatter_custom_fusion
  27.7 9.7 %all-to-all-done = f32[64,256,4]{1,2,0:T(4,128)S(1)} async-done(((f32[64,256,4]{1,2,0:T(4,128)}), f32[64,256,4]{1,2,0:T(4,128)S(1)}, u32[]{:S(2)}, u32[]{:S(2)}) %all-to-all-start) | async-done | bytes 262176 | tf_op jit(solution)/shard_map/all_to_all | solution.py:20
  37.4 0.1 copy.51
  37.5 0.2 reshape_reshape.3
  37.7 82.5 %all-gather.3.cloned.1.call-done = bf16[16384,512]{0,1:T(8,128)(2,1)} async-done(((bf16[256,512]{0,1:T(8,128)(2,1)}), bf16[16384,512]{0,1:T(8,128)(2,1)}) %all-gather.3.cloned.1.call-update) | async-done | bytes 16777232 | tf_op jit(solution)/shard_map/all_gather | solution.py:40
  120.2 11.4 %fusion.89 = (bf16[16384,256]{0,1:T(8,128)(2,1)}, bf16[16384,256]{0,1:T(8,128)(2,1)}) fusion(bf16[16384,512]{0,1:T(8,128)(2,1)} %all-gather.3.cloned.1.call-done), kind=kLoop, calls=%fused_computation.94 | loop fusion | bytes 33554432 | tf_op jit(solution)/shard_map/split | solution.py:40
  131.7 12.1 %copy.52 = bf16[16384,2,128]{2,0,1:T(8,128)(2,1)} copy(bf16[16384,2,128]{0,2,1:T(8,128)(2,1)} %bitcast.147) | data formatting | bytes 16777216
  143.8 0.0 copy-start.2
  143.8 18.1 %while.18 = (s32[]{:T(128)}, f32[2,2,256]{2,1,0:T(2,128)S(1)}, f32[2,2,256]{2,1,0:T(2,128)S(1)}, f32[256,2,2,128]{0,3,2,1:T(8,128)S(1)}, s32[]{:T(128)}, /*index...) while((s32[]{:T(128)}, f32[2,2,256]{2,1,0:T(2,128)S(1)}, ...), condition=%wide.region_5.6_spmd.clone, body=%wide.region_0.5_spmd.clone.sunk | while | flops 555225344 | bytes 16163165 | solution.py:84
  144.5 6.6 %conditional.3 = ((f32[2,2,256]{2,1,0:T(2,128)S(1)}, f32[2,2,256]{2,1,0:T(2,128)S(1)}, f32[256,2,2,128]{0,3,2,1:T(8,128)S(1)})) conditional(s32[]{:T(128)} %convert_element_type.118, (f32[2,2,256]{2,1,0:T(2,128)S(1)}, f32[2,2,256]{2,1,0:T(2,128)S(1)}, f32[256,2,2,128]{0,3,2,1:T(8,128)S(1)}) %tuple.48, (s32[]{:T(128)}, s32[]{:T(128)}, ...), branch_computations={%region_1.0_spmd, %region_2.4_spmd} | conditional | flops 555225344 | bytes 16161878 | solution.py:82
  144.6 0.2 broadcast_compare_fusion
  144.8 2.3 fusion.5
  147.1 2.7 fusion.12
  149.8 1.4 fusion.4
  162.0 0.2 copy.54
  162.2 0.8 convert_element_type.63
  163.0 4.2 all-to-all-start.1
  167.2 10.6 %all-to-all-done.1 = bf16[4,64,512]{2,1,0:T(8,128)(2,1)S(1)} async-done(((bf16[4,64,512]{2,1,0:T(8,128)(2,1)}), bf16[4,64,512]{2,1,0:T(8,128)(2,1)S(1)}, u32[]{:S(2)}, u32[]{:S(2)}) %all-to-all-start.1) | async-done | bytes 262176 | tf_op jit(solution)/shard_map/all_to_all | solution.py:148
  177.8 32.3 %all-gather.5.cloned.1.call-done = bf16[2048,2048]{1,0:T(8,128)(2,1)} async-done(((bf16[512,2048]{1,0:T(8,128)(2,1)}), bf16[2048,2048]{1,0:T(8,128)(2,1)}) %all-gather.5.cloned.1.call-update) | async-done | bytes 8388624 | tf_op jit(solution)/shard_map/all_gather | solution.py:151
  210.2 0.0 copy-done.2
  210.2 5.0 %fusion.28 = bf16[64,2048]{1,0:T(8,128)(2,1)S(1)} fusion(bf16[64,2048]{1,0:T(8,128)(2,1)S(1)} %bitcast.150, bf16[2048,2048]{1,0:T(8,128)(2,1)} %all-gather.5.cloned.1.call-done, bf16[64,2048]{1,0:T(8,128)(2,1)S(1)} %copy-done.2), kind=kOutput, calls=%fused_computation.36 | convolution fusion | flops 537264128 | bytes 9175040 | tf_op jit(solution)/shard_map/dot_general | solution.py:149
  215.2 0.2 fusion.66
  215.3 0.0 copy-done.4
  215.3 0.1 fusion.68
  215.5 3.3 gather_fusion
  218.9 122.8 %all_to_all.31 = bf16[64,1,8,2048]{3,2,1,0:T(8,128)(2,1)S(1)} all-to-all(bf16[64,1,8,2048]{3,2,1,0:T(8,128)(2,1)} %bitcast.148), channel_id=1, replica_groups=mesh['sp'=64,'tp'=4] {'sp'}, dimensions={0} | all-to-all | bytes 4194304 | tf_op jit(solution)/shard_map/all_to_all | solution.py:178
  341.7 1.3 copy-done.1
  343.0 0.0 copy-done.8
  343.0 2.1 fusion.36
  345.1 0.0 copy-done
  345.1 5.9 %fusion.25 = bf16[64,1,8,2048]{3,2,1,0:T(8,128)(2,1)} fusion(bf16[1,384,2048]{2,1,0:T(8,128)(2,1)S(1)} %copy-done, bf16[1,2048,384]{2,1,0:T(8,128)(2,1)} %param.29, bf16[64,1,8,2048]{3,2,1,0:T(8,128)(2,1)} %copy-done.1, f32[64,1,8,384]{3,2,0,1:T(8,128)} %fusion.36), kind=kOutput, calls=%fused_computation.31 | convolution fusion | flops 1612840960 | bytes 8126464 | tf_op jit(solution)/shard_map/necf,efd->necd/dot_general | solution.py:184
  351.0 5.8 %all-to-all-start.3 = ((bf16[64,1,8,2048]{3,2,1,0:T(8,128)(2,1)}), bf16[64,1,8,2048]{3,2,1,0:T(8,128)(2,1)}, u32[]{:S(2)}, u32[]{:S(2)}) async-start(bf16[64,1,8,2048]{3,2,1,0:T(8,128)(2,1)} %fusion.25), calls=%async_computation.3 | async-start | bytes 4194304 | tf_op jit(solution)/shard_map/all_to_all | solution.py:187
  356.8 0.0 copy-done.7
  356.8 0.1 copy.56
  356.9 1.8 fusion.87
  358.8 49.2 %all-to-all-done.3 = bf16[64,1,8,2048]{3,2,1,0:T(8,128)(2,1)} async-done(((bf16[64,1,8,2048]{3,2,1,0:T(8,128)(2,1)}), bf16[64,1,8,2048]{3,2,1,0:T(8,128)(2,1)}, u32[]{:S(2)}, u32[]{:S(2)}) %all-to-all-start.3) | async-done | bytes 2097184 | tf_op jit(solution)/shard_map/all_to_all | solution.py:187
  407.9 4.2 gather_fusion.1
  412.2 1.7 reshape.128
  413.9 3.2 multiply_reduce_fusion
  417.1 3.4 fusion.27
  (64 shorter events, 0.5 us)
Async XLA Ops:
  6.5 338.6 %copy-start = (bf16[1,384,2048]{2,1,0:T(8,128)(2,1)S(1)}, bf16[1,384,2048]{2,1,0:T(8,128)(2,1)}, u32[]{:S(2)}) copy-start(bf16[1,384,2048]{2,1,0:T(8,128)(2,1)} %param.30) | copy-start | bytes 4718596
  6.5 17.2 %copy-start.5 = (f32[256,4]{0,1:T(4,128)S(1)}, f32[256,4]{0,1:T(4,128)}, u32[]{:S(2)}) copy-start(f32[256,4]{0,1:T(4,128)} %param.23) | copy-start | bytes 12292
  6.5 17.3 %copy-start.6 = (s32[64,4]{0,1:T(4,128)S(1)}, s32[64,4]{0,1:T(4,128)}, u32[]{:S(2)}) copy-start(s32[64,4]{0,1:T(4,128)} %param.26) | copy-start | bytes 3076
  6.5 18.2 %copy-start.3 = (bf16[256,512]{1,0:T(8,128)(2,1)S(1)}, bf16[256,512]{1,0:T(8,128)(2,1)}, u32[]{:S(2)}) copy-start(bf16[256,512]{1,0:T(8,128)(2,1)} %param.20) | copy-start | bytes 786436
  6.5 113.7 %all-gather.3.cloned.1.call-start = ((), (), s32[]{:S(2)}) async-start(), calls=%async_computation.4 | async-start | bytes 17039360 | tf_op jit(solution)/shard_map/all_gather | solution.py:40
  9.5 200.7 %all-gather.5.cloned.1.call-start = ((), (), s32[]{:S(2)}) async-start(), calls=%async_computation.5 | async-start | bytes 10485760 | tf_op jit(solution)/shard_map/all_gather | solution.py:151
  11.7 25.8 %all-to-all-start = ((f32[64,256,4]{1,2,0:T(4,128)}), f32[64,256,4]{1,2,0:T(4,128)S(1)}, u32[]{:S(2)}, u32[]{:S(2)}) async-start(f32[64,256,4]{1,2,0:T(4,128)} %broadcast_in_dim.29), calls=%async_computation | async-start | bytes 524288 | tf_op jit(solution)/shard_map/all_to_all | solution.py:20
  143.8 66.4 %copy-start.2 = (bf16[64,2048]{1,0:T(8,128)(2,1)S(1)}, bf16[64,2048]{1,0:T(8,128)(2,1)}, u32[]{:S(2)}) copy-start(bf16[64,2048]{1,0:T(8,128)(2,1)} %param.19) | copy-start | bytes 786436
  163.0 14.8 %all-to-all-start.1 = ((bf16[4,64,512]{2,1,0:T(8,128)(2,1)}), bf16[4,64,512]{2,1,0:T(8,128)(2,1)S(1)}, u32[]{:S(2)}, u32[]{:S(2)}) async-start(bf16[4,64,512]{2,1,0:T(8,128)(2,1)} %convert_element_type.63), calls=%async_computation.1 | async-start | bytes 524288 | tf_op jit(solution)/shard_map/all_to_all | solution.py:148
  210.2 5.1 %copy-start.4 = (f32[2048]{0:T(1024)S(1)}, f32[2048]{0:T(1024)}, u32[]{:S(2)}) copy-start(f32[2048]{0:T(1024)} %param.25) | copy-start | bytes 24580
  218.9 124.1 %copy-start.8 = (bf16[1,2048,384]{2,1,0:T(8,128)(2,1)S(1)}, bf16[1,2048,384]{2,1,0:T(8,128)(2,1)}, u32[]{:S(2)}) copy-start(bf16[1,2048,384]{2,1,0:T(8,128)(2,1)} %param.28) | copy-start | bytes 4718596
  341.7 1.3 copy-start.1
  351.0 5.8 %copy-start.7 = (f32[64,4]{0,1:T(4,128)S(1)}, f32[64,4]{0,1:T(4,128)}, u32[]{:S(2)}) copy-start(f32[64,4]{0,1:T(4,128)} %param.27) | copy-start | bytes 3076
  351.0 56.9 %all-to-all-start.3 = ((bf16[64,1,8,2048]{3,2,1,0:T(8,128)(2,1)}), bf16[64,1,8,2048]{3,2,1,0:T(8,128)(2,1)}, u32[]{:S(2)}, u32[]{:S(2)}) async-start(bf16[64,1,8,2048]{3,2,1,0:T(8,128)(2,1)} %fusion.25), calls=%async_computation.3 | async-start | bytes 4194304 | tf_op jit(solution)/shard_map/all_to_all | solution.py:187
Sparse Core Ops, SparseCore 0:
  10.0 110.1 all-gather.2
  122.0 88.1 all-gather.4
where the time goes:
time: 430 us; the launch traced here: 427 us
  waiting for transfers between devices  185 us (43%)
  blocking collectives  123 us (29%)
  local copies, waits for them, and re-layouts  42.2 us (10%)
  matrix products  23.2 us (5%)
  starting transfers between devices  22.2 us (5%)
  between operations  13.7 us (3%)
  loops' own time  11.5 us (3%)
  other arithmetic  6.65 us (2%)
    all_to_all x1, blocking collectives, local(): lax.all_to_all(outgoing, 'sp', split_axis=0, concat_axis=0, tiled=True)  123 us
    all_gather x1, waiting for transfers between devices, in_one_piece(): lax.all_gather(both, axis, axis=dim, tiled=True)  82.5 us
    all_to_all x1, waiting for transfers between devices, local(): lax.all_to_all(processed, 'sp', split_axis=0, concat_axis=0, tiled=True)  49.2 us
    all_gather x1, waiting for transfers between devices, local(): lax.all_gather(out_weight, 'tp', axis=0, tiled=True)  32.3 us
    unnamed x24, local copies, waits for them, and re-layouts  15.9 us
    all_to_all x1, starting transfers between devices, from_everyone(): return lax.all_to_all(copies, axis, split_axis=0, concat_axis=0, tiled=True)  12.1 us
    split x1, local copies, waits for them, and re-layouts, in_one_piece(): jnp.split(lax.all_gather(both, axis, axis=dim, tiled=True), ends, axis=al...  11.4 us
    another operation x1, loops' own time, absorb_group(): return lax.fori_loop(0, piece_rows // key_block, one_block, carried)  11.3 us
  transfers between devices with their start and end apart: 5, of which 5 were waited for; matrix products, arithmetic and copies ran while one was open for 9% of the time, Pallas kernels for 0%

commit v1 on v0

v1 whole, which is shorter than its diff:
```python
import functools
import math

import jax
import jax.numpy as jnp
from jax import lax
from jax.experimental import pallas as pl
from jax.experimental.pallas import tpu as pltpu
from jax.sharding import Mesh, PartitionSpec as P

HEADS = 16
KV_HEADS = 8
HEAD_DIM = 128
TOPK = 4
ROUTED_SCALE = 2.5
NORM_EPS = 1e-06
LOG2E = math.log2(math.e)
SCORE2 = HEAD_DIM**-0.5 * LOG2E
LOW = -1e30
TAIL = 16

BF = jnp.bfloat16
F32 = jnp.float32


def pieces(row):
    high = row.astype(BF)
    rest = row - high.astype(F32)
    mid = rest.astype(BF)
    low = (rest - mid.astype(F32)).astype(BF)
    return [high.astype(F32), mid.astype(F32), low.astype(F32)]


def tail_block(rows, width):
    parts = [piece for row in rows for piece in pieces(row)]
    parts.append(jnp.zeros((TAIL - len(parts), width), F32))
    return jnp.concatenate(parts, axis=0).astype(BF)


def row_of(tail, j):
    return tail[3 * j : 3 * j + 1] + tail[3 * j + 1 : 3 * j + 2] + tail[3 * j + 2 : 3 * j + 3]


def pack_kernel(q_ref, k_ref, v_ref, f_ref, kv_out, q_out):
    rows = q_ref.shape[0]
    ys = q_out.shape[0] // 2
    for c in range(2):
        tail = tail_block([f_ref[2 * c : 2 * c + 1, :], f_ref[2 * c + 1 : 2 * c + 2, :]], rows)
        kv_out[c, :rows, :HEAD_DIM] = k_ref[:, c * HEAD_DIM : (c + 1) * HEAD_DIM]
        kv_out[c, :rows, HEAD_DIM:] = v_ref[:, c * HEAD_DIM : (c + 1) * HEAD_DIM]
        kv_out[c, rows:, :] = tail
        q_part = q_ref[:, c * 2 * HEAD_DIM : (c + 1) * 2 * HEAD_DIM]
        for y in range(ys):
            q_out[2 * y + c, :rows, :] = q_part
            q_out[2 * y + c, rows:, :] = tail


def pack(q, k, v, f_t, ys):
    rows = q.shape[0]
    width = 2 * HEAD_DIM
    return pl.pallas_call(
        pack_kernel,
        out_shape=(
            jax.ShapeDtypeStruct((2, rows + TAIL, width), BF),
            jax.ShapeDtypeStruct((2 * ys, rows + TAIL, width), BF),
        ),
        name="pack",
    )(q, k, v, f_t)


def attend_kernel(info, *refs, blocks, own, first, last, tiles, rows):
    q_ref, ref_tail = refs[0], refs[1]
    kv_refs = refs[2 : 2 + blocks]
    at = 2 + blocks
    if not first:
        acc_in, stat_in = refs[at], refs[at + 1]
        at += 2
    if last:
        (o_out,) = refs[at : at + 1]
    else:
        acc_out, stat_out = refs[at : at + 2]
    step = pl.program_id(0)
    first_tail = ref_tail[0].astype(F32)
    keys, values, biases = [], [], []
    ones = jnp.ones((rows, HEAD_DIM), BF)
    for b in range(blocks):
        for c in range(2):
            keys.append(kv_refs[b].at[c, pl.ds(0, rows), pl.ds(0, HEAD_DIM)])
            values.append(kv_refs[b].at[c, pl.ds(0, rows), pl.ds(HEAD_DIM, HEAD_DIM)])
            tail = kv_refs[b][c, rows:, :].astype(F32)
            pair = []
            for j in range(2):
                bias = (row_of(first_tail, j)[:, :1] - row_of(tail, j)) * LOG2E
                pair.append(jnp.where(info[1 + b] > 0, bias, -jnp.inf))
            biases.append(pair)
    lane = lax.broadcasted_iota(jnp.int32, (rows, HEAD_DIM), 1)
    for i in range(tiles):
        tile_first = (step * tiles + i) * rows
        if not first:
            stat_old = stat_in[i]
        stat_new = jnp.zeros((rows, HEAD_DIM), F32)
        lse_rows = []
        for j in range(2):
            cols = pl.ds(j * HEAD_DIM, HEAD_DIM)
            query = q_ref[i, pl.ds(0, rows), cols]
            scores = []
            for u in range(2 * blocks):
                raw = lax.dot_general(
                    query, keys[u][...], (((1,), (1,)), ((), ())), preferred_element_type=F32
                )
                score = raw * SCORE2 + biases[u][j]
                if own and u < 2:
                    q_pos = tile_first + lax.broadcasted_iota(jnp.int32, (rows, rows), 0)
                    k_pos = info[0] + u * rows + lax.broadcasted_iota(jnp.int32, (rows, rows), 1)
                    score = jnp.where(q_pos >= k_pos, score, -jnp.inf)
                scores.append(score)
            top = scores[0]
            for score in scores[1:]:
                top = jnp.maximum(top, score)
            row_max = jnp.max(top, axis=1, keepdims=True)
            if first:
                row_max = jnp.maximum(row_max, LOW)
            else:
                old_max = stat_old[:, j : j + 1]
                row_max = jnp.maximum(row_max, old_max)
            total = None
            for u in range(2 * blocks):
                weights = jnp.exp2(scores[u] - row_max).astype(BF)
                value = jnp.concatenate([values[u][...], ones], axis=1)
                part = jnp.dot(weights, value, preferred_element_type=F32)
                total = part if total is None else total + part
            weighted = total[:, :HEAD_DIM]
            row_sum = total[:, HEAD_DIM : HEAD_DIM + 1]
            if not first:
                factor = jnp.exp2(old_max - row_max)
                weighted = weighted + acc_in[i, :, cols] * factor
                row_sum = row_sum + stat_old[:, 2 + j : 3 + j] * factor
            if last:
                some = row_sum > 0.0
                mixed = weighted * (1.0 / jnp.where(some, row_sum, 1.0))
                per = rows // 4
                for p in range(4):
                    o_out[4 * i + p, pl.ds(0, per), cols] = mixed[p * per : (p + 1) * per].astype(BF)
                lse = jnp.where(some, row_max + jnp.log2(jnp.where(some, row_sum, 1.0)), LOW)
                wide = jnp.broadcast_to(lse, (rows, rows))
                eye = lax.broadcasted_iota(jnp.int32, (rows, rows), 0) == lax.broadcasted_iota(
                    jnp.int32, (rows, rows), 1
                )
                lse_rows.append(jnp.sum(jnp.where(eye, wide, 0.0), axis=0, keepdims=True))
            else:
                acc_out[i, :, cols] = weighted
                stat_new = jnp.where(lane == j, row_max, stat_new)
                stat_new = jnp.where(lane == 2 + j, row_sum, stat_new)
        if last:
            tail = tail_block(lse_rows, rows)
            for p in range(4):
                o_out[4 * i + p, pl.ds(rows // 4, TAIL), :] = tail
        else:
            stat_out[i] = stat_new


def attend(info, q_all, kvs, state, own, last, name, tiles=2):
    count, padded, width = q_all.shape
    rows = padded - TAIL
    first = state is None
    grid = count // tiles
    blocks = len(kvs)
    tile_map = lambda g, info: (g, 0, 0)
    whole = lambda g, info: (0, 0, 0)
    in_specs = [
        pl.BlockSpec((tiles, padded, width), tile_map),
        pl.BlockSpec((1, TAIL, width), lambda g, info: (0, rows // TAIL, 0)),
    ]
    in_specs += [pl.BlockSpec((2, padded, width), whole)] * blocks
    operands = [q_all, q_all, *kvs]
    state_specs = [
        pl.BlockSpec((tiles, rows, width), tile_map),
        pl.BlockSpec((tiles, rows, HEAD_DIM), tile_map),
    ]
    aliases = {}
    if not first:
        in_specs += state_specs
        operands += list(state)
        if not last:
            aliases = {1 + len(operands) - 2: 0, 1 + len(operands) - 1: 1}
    if last:
        out_specs = pl.BlockSpec((4 * tiles, rows // 4 + TAIL, width), tile_map)
        out_shape = jax.ShapeDtypeStruct((4 * count, rows // 4 + TAIL, width), BF)
    else:
        out_specs = state_specs
        out_shape = [
            jax.ShapeDtypeStruct((count, rows, width), F32),
            jax.ShapeDtypeStruct((count, rows, HEAD_DIM), F32),
        ]
    scores = count * rows * 2 * blocks * 2 * rows
    return pl.pallas_call(
        functools.partial(
            attend_kernel, blocks=blocks, own=own, first=first, last=last, tiles=tiles, rows=rows
        ),
        grid_spec=pltpu.PrefetchScalarGridSpec(
            num_scalar_prefetch=1, grid=(grid,), in_specs=in_specs, out_specs=out_specs
        ),
        out_shape=out_shape,
        input_output_aliases=aliases,
        cost_estimate=pl.CostEstimate(
            flops=scores * 768, transcendentals=scores, bytes_accessed=6_000_000
        ),
        compiler_params=pltpu.CompilerParams(
            dimension_semantics=("arbitrary",), vmem_limit_bytes=40 * 1024 * 1024
        ),
        name=name,
    )(info, *operands)


def post_kernel(
    tp_ref, part_ref, w_ref, res_ref, gain_ref, ids_ref, stream_out, normed_out, send_out, att, strm
):
    step = pl.program_id(0)
    sources = part_ref.shape[0]
    own_rows = res_ref.shape[0]
    width = part_ref.shape[2]
    groups = att.shape[1] // width
    ys = sources // groups

    @pl.when(step == 0)
    def _():
        pick = lax.broadcasted_iota(jnp.int32, (own_rows, width), 1) == (
            tp_ref[0] * own_rows + lax.broadcasted_iota(jnp.int32, (own_rows, width), 0)
        )
        for g in range(groups):
            core, tp = g // (groups // 2), g % (groups // 2)
            col = (tp * 2 + core) * width
            tails = [part_ref[y * groups + g, own_rows:, :].astype(F32) for y in range(ys)]
            for j in range(2):
                sums = []
                for y in range(ys):
                    row = row_of(tails[y], j)
                    sums.append(jnp.sum(jnp.where(pick, row, 0.0), axis=1, keepdims=True))
                top = sums[0]
                for s in sums[1:]:
                    top = jnp.maximum(top, s)
                weights = [jnp.exp2(s - top) for s in sums]
                total = weights[0]
                for w in weights[1:]:
                    total = total + w
                inverse = 1.0 / total
                mixed = None
                for y in range(ys):
                    part = part_ref[
                        y * groups + g, pl.ds(0, own_rows), pl.ds(j * HEAD_DIM, HEAD_DIM)
                    ].astype(F32) * (weights[y] * inverse)
                    mixed = part if mixed is None else mixed + part
                att[:, pl.ds(col + j * HEAD_DIM, HEAD_DIM)] = mixed.astype(BF)

    block = w_ref.shape[1]
    cols = pl.ds(pl.multiple_of(step * block, block), block)
    branch = jnp.dot(att[...], w_ref[...], preferred_element_type=F32)
    stream = (res_ref[...].astype(F32) + branch).astype(BF)
    stream_out[...] = stream
    strm[:, cols] = stream

    @pl.when(step == pl.num_programs(0) - 1)
    def _():
        wide = strm[...].astype(F32)
        mean = jnp.mean(wide * wide, axis=1, keepdims=True)
        normed = (wide * lax.rsqrt(mean + NORM_EPS) * gain_ref[...]).astype(BF)
        normed_out[...] = normed
        experts = send_out.shape[0]
        cap = send_out.shape[1]
        expert = lax.broadcasted_iota(jnp.int32, (experts, own_rows), 0)
        named = jnp.zeros((experts, own_rows), F32)
        for k in range(TOPK):
            named = jnp.where(ids_ref[k : k + 1, :] == expert, 1.0, named)
        earlier = (
            lax.broadcasted_iota(jnp.int32, (own_rows, own_rows), 0)
            < lax.broadcasted_iota(jnp.int32, (own_rows, own_rows), 1)
        ).astype(BF)
        rank = jnp.dot(named.astype(BF), earlier, preferred_element_type=F32)
        rank = jnp.where(named > 0.5, rank, -1.0)
        slot = lax.broadcasted_iota(jnp.int32, (experts, cap, own_rows), 1).astype(F32)
        chosen = (rank[:, None, :] == slot).astype(F32).reshape(experts * cap, own_rows).astype(BF)
        sent = jnp.dot(chosen, normed, preferred_element_type=F32).astype(BF)
        send_out[...] = sent.reshape(send_out.shape)


def post(tp, parts, weight, residual, gain, ids_t, experts, cap):
    rows, width = residual.shape
    block = 256
    fixed2 = lambda g, tp: (0, 0)
    fixed3 = lambda g, tp: (0, 0, 0)
    tiled = lambda g, tp: (0, g)
    return pl.pallas_call(
        post_kernel,
        grid_spec=pltpu.PrefetchScalarGridSpec(
            num_scalar_prefetch=1,
            grid=(width // block,),
            in_specs=[
                pl.BlockSpec(parts.shape, fixed3),
                pl.BlockSpec((width, block), tiled),
                pl.BlockSpec((rows, block), tiled),
                pl.BlockSpec((1, width), fixed2),
                pl.BlockSpec(ids_t.shape, fixed2),
            ],
            out_specs=[
                pl.BlockSpec((rows, block), tiled),
                pl.BlockSpec((rows, width), fixed2),
                pl.BlockSpec((experts, cap, width), fixed3),
            ],
            scratch_shapes=[pltpu.VMEM((rows, width), BF), pltpu.VMEM((rows, width), BF)],
        ),
        out_shape=[
            jax.ShapeDtypeStruct((rows, width), BF),
            jax.ShapeDtypeStruct((rows, width), BF),
            jax.ShapeDtypeStruct((experts, cap, width), BF),
        ],
        compiler_params=pltpu.CompilerParams(
            dimension_semantics=("arbitrary",), vmem_limit_bytes=40 * 1024 * 1024
        ),
        name="post",
    )(tp, parts, weight, residual, gain, ids_t)


def finish_kernel(res_ref, base_ref, ids_ref, route_ref, out_ref):
    rows = base_ref.shape[0]
    experts, cap, width = res_ref.shape
    slots = experts * cap
    route = route_ref[...]
    gates = route / jnp.sum(route, axis=1, keepdims=True) * ROUTED_SCALE
    expert = lax.broadcasted_iota(jnp.int32, (rows, experts), 1)
    named = jnp.zeros((rows, experts), F32)
    gate = jnp.zeros((rows, experts), F32)
    for k in range(TOPK):
        here = ids_ref[:, k : k + 1] == expert
        named = jnp.where(here, 1.0, named)
        gate = jnp.where(here, gates[:, k : k + 1], gate)
    earlier = (
        lax.broadcasted_iota(jnp.int32, (rows, rows), 1)
        < lax.broadcasted_iota(jnp.int32, (rows, rows), 0)
    ).astype(BF)
    rank = jnp.dot(earlier, named.astype(BF), preferred_element_type=F32)
    rank = jnp.where(named > 0.5, rank, 128.0)
    slot = lax.broadcasted_iota(jnp.int32, (experts, slots), 1)
    first = lax.broadcasted_iota(jnp.int32, (experts, slots), 0) * cap
    spread = ((slot >= first) & (slot < first + cap)).astype(BF)
    rank_x = jnp.dot(rank.astype(BF), spread, preferred_element_type=F32)
    place = (lax.broadcasted_iota(jnp.int32, (rows, slots), 1) % cap).astype(F32)
    chosen = rank_x == place
    high = gate.astype(BF)
    low = (gate - high.astype(F32)).astype(BF)
    high_x = jnp.where(chosen, jnp.dot(high, spread, preferred_element_type=F32), 0.0).astype(BF)
    low_x = jnp.where(chosen, jnp.dot(low, spread, preferred_element_type=F32), 0.0).astype(BF)
    results = res_ref[...].reshape(slots, width)
    routed = jnp.dot(high_x, results, preferred_element_type=F32) + jnp.dot(
        low_x, results, preferred_element_type=F32
    )
    out_ref[...] = (base_ref[...] + routed).astype(BF)


def finish(results, base, ids, route):
    return pl.pallas_call(
        finish_kernel,
        out_shape=jax.ShapeDtypeStruct(base.shape, BF),
        compiler_params=pltpu.CompilerParams(vmem_limit_bytes=40 * 1024 * 1024),
        name="finish",
    )(results, base, ids, route)


def local(
    residual,
    queries,
    key_rows,
    value_rows,
    forget_sums,
    out_weight,
    norm_gain,
    expert_ids,
    route_weights,
    expert_gate,
    expert_up,
    expert_down,
    shared_gate,
    shared_up,
    shared_down,
):
    z_count = lax.axis_size("z")
    y_count = lax.axis_size("y")
    z = lax.axis_index("z")
    y = lax.axis_index("y")
    rows = queries.shape[0]
    experts = z_count * y_count * 2
    cap = 2 * residual.shape[0] * TOPK // experts

    weight = lax.all_gather(out_weight, "tp", axis=0, tiled=True)
    kv_send, q_send = pack(queries, key_rows, value_rows, forget_sums.T, y_count)
    own = lax.all_to_all(kv_send, "c", split_axis=0, concat_axis=0)
    up_ring = [(i, (i + 1) % z_count) for i in range(z_count)]
    down_ring = [(i, (i - 1) % z_count) for i in range(z_count)]
    half = z_count // 2
    ups, downs = [own], [own]
    for s in range(1, half + 1):
        ups.append(lax.ppermute(ups[-1], "z", up_ring))
        if s < half:
            downs.append(lax.ppermute(downs[-1], "z", down_ring))
    q_all = lax.all_to_all(q_send, ("y", "c"), split_axis=0, concat_axis=0)

    def flags(*steps):
        good = []
        for direction, s in steps:
            if s == 0:
                good.append(jnp.int32(1))
            elif direction > 0:
                good.append((z >= s).astype(jnp.int32))
            else:
                good.append((z + s >= z_count).astype(jnp.int32))
        return jnp.stack([2 * y * rows, *good]).astype(jnp.int32)

    state = attend(
        flags((1, 0), (1, 1), (-1, 1)), q_all, [own, ups[1], downs[1]], None, True, False, "attend1"
    )
    for s in range(2, half):
        state = attend(
            flags((1, s), (-1, s)), q_all, [ups[s], downs[s]], state, False, False, f"attend{s}"
        )
    sent = attend(flags((1, half)), q_all, [ups[half]], state, False, True, "attend_last")
    parts = lax.all_to_all(sent, ("y", "c", "tp"), split_axis=0, concat_axis=0)
    tp = lax.axis_index("tp").astype(jnp.int32).reshape(1)
    stream, normed, outgoing = post(
        tp, parts, weight, residual, norm_gain[None, :], expert_ids.T, experts, cap
    )
    arrived = lax.all_to_all(outgoing, ("z", "y", "c"), split_axis=0, concat_axis=0)
    shared_hidden = (
        jax.nn.silu(jnp.dot(normed, shared_gate, preferred_element_type=F32))
        * jnp.dot(normed, shared_up, preferred_element_type=F32)
    ).astype(BF)
    base = stream.astype(F32) + jnp.dot(shared_hidden, shared_down, preferred_element_type=F32)
    tokens = arrived.reshape(experts * cap, -1)
    gate_part = jnp.dot(tokens, expert_gate[0], preferred_element_type=F32)
    up_part = jnp.dot(tokens, expert_up[0], preferred_element_type=F32)
    hidden = (jax.nn.silu(gate_part) * up_part).astype(BF)
    processed = jnp.dot(hidden, expert_down[0], preferred_element_type=F32).astype(BF)
    returned = lax.all_to_all(
        processed.reshape(arrived.shape), ("z", "y", "c"), split_axis=0, concat_axis=0
    )
    return finish(returned, base, expert_ids, route_weights)


def solution(mesh):
    sp = mesh.shape["sp"]
    tp = mesh.shape["tp"]
    grid = Mesh(mesh.devices.reshape(8, sp // 16, 2, tp), ("z", "y", "c", "tp"))
    seq = ("z", "y", "c")
    in_specs = (
        P((*seq, "tp"), None),
        P(seq, "tp"),
        P(seq, "tp"),
        P(seq, "tp"),
        P(seq, "tp"),
        P("tp", None),
        P(),
        P((*seq, "tp"), None),
        P((*seq, "tp"), None),
        P(seq, None, None),
        P(seq, None, None),
        P(seq, None, None),
        P(),
        P(),
        P(),
    )
    out_specs = P((*seq, "tp"), None)
    return jax.shard_map(local, mesh=grid, in_specs=in_specs, out_specs=out_specs, check_vma=False)
```

time: 430 us -> 270 us (0.63)
  waiting for transfers between devices: 185 us -> 84 us
  blocking collectives: 123 us -> 65 us
  Pallas kernels: 0 us -> 56.2 us
  local copies, waits for them, and re-layouts: 42.2 us -> 7.69 us
  loops' own time: 11.5 us -> 0 us
  matrix products: 23.2 us -> 12.1 us
  starting transfers between devices: 22.2 us -> 30.4 us
  other arithmetic: 6.65 us -> 0.3 us
    all_gather x2 -> x1, waiting for transfers between devices: 115 us -> 0.01 us  [local(): weight = lax.all_gather(out_weight, 'tp', axis=0, tiled=True)]
    all_to_all x1 -> x2, blocking collectives: 123 us -> 65 us  [the longest x1 60 us: local(): lax.all_to_all(outgoing, ('z', 'y', 'c'), split_axis=0, concat_axis=0)]
    pallas_call x0 -> x7, Pallas kernels: none -> 56.2 us  [the longest x4 44.8 us: attend(): pl.pallas_call(functools.partial(attend_kernel, blocks=blocks, own=own, f...]
    ppermute x0 -> x7, waiting for transfers between devices: none -> 17.8 us  [the longest x4 17.8 us: local(): ups.append(lax.ppermute(ups[-1], 'z', up_ring))]
    ppermute x0 -> x7, starting transfers between devices: none -> 11.7 us  [the longest x3 10.4 us: local(): downs.append(lax.ppermute(downs[-1], 'z', down_ring))]
    another operation x17 -> x0, loops' own time: 11.5 us -> none  [the longest x1 11.3 us: absorb_group(): return lax.fori_loop(0, piece_rows // key_block, one_block, carried)]
    split x1 -> x0, local copies, waits for them, and re-layouts: 11.4 us -> none  [in_one_piece(): jnp.split(lax.all_gather(both, axis, axis=dim, tiled=True), ends, axis=al...]
    dot_general x7 -> x4, matrix products: 23.2 us -> 12.1 us  [the longest x1 5.47 us: local(): jnp.dot(hidden, expert_down[0], preferred_element_type=F32).astype(BF)]
  transfers between devices with their start and end apart: 5 -> 11, of which waited for: 5 -> 5; matrix products, arithmetic and copies ran while one was open for 9% -> 2% of each run, Pallas kernels for 0% -> 17%
where the time goes in v1:
time: 270 us; the launch traced here: 269 us
  waiting for transfers between devices  84 us (31%)
  blocking collectives  65 us (24%)
  Pallas kernels  56.2 us (21%)
  starting transfers between devices  30.4 us (11%)
  between operations  13.6 us (5%)
  matrix products  12.1 us (4%)
  local copies, waits for them, and re-layouts  7.69 us (3%)
    all_to_all x1, blocking collectives, local(): lax.all_to_all(outgoing, ('z', 'y', 'c'), split_axis=0, concat_axis=0)  60 us
    all_to_all x1, waiting for transfers between devices, local(): lax.all_to_all(processed.reshape(arrived.shape), ('z', 'y', 'c'), split_a...  46.5 us
    pallas_call x4, Pallas kernels, attend(): pl.pallas_call(functools.partial(attend_kernel, blocks=blocks, own=own, f...  44.8 us
    all_to_all x1, waiting for transfers between devices, local(): parts = lax.all_to_all(sent, ('y', 'c', 'tp'), split_axis=0, concat_axis=0)  19 us
    ppermute x4, waiting for transfers between devices, local(): ups.append(lax.ppermute(ups[-1], 'z', up_ring))  17.8 us
    ppermute x3, starting transfers between devices, local(): downs.append(lax.ppermute(downs[-1], 'z', down_ring))  10.4 us
    unnamed x30, local copies, waits for them, and re-layouts  7.69 us
    all_to_all x1, starting transfers between devices, local(): parts = lax.all_to_all(sent, ('y', 'c', 'tp'), split_axis=0, concat_axis=0)  7.36 us
  transfers between devices with their start and end apart: 11, of which 5 were waited for; matrix products, arithmetic and copies ran while one was open for 2% of the time, Pallas kernels for 17%

profile of v1, /device:TPU:8, one launch (start us, length us, event | category | flops | bytes accessed | tf_op | source)
XLA Modules:
  0.0 269.2 jit_solution(4818534999061521391)
XLA Ops:
  6.5 0.0 copy-start
  6.5 0.0 all-gather.2.cloned.1.call-start
  6.5 0.7 all-gather.2.cloned.1.call-update
  7.3 2.3 pack.1
  9.6 5.0 %all_to_all.25.refs_2_ = bf16[2,272,256]{2,1,0:T(8,128)(2,1)S(1)} all-to-all(bf16[2,272,256]{2,1,0:T(8,128)(2,1)} %get-tuple-element.17), channel_id=1, replica_groups=mesh['z'=8,'y'=4,'c'=2,'tp'=4] {'c'}, dimensions={0} | all-to-all | bytes 557056 | tf_op jit(solution)/shard_map/all_to_all | solution.py:395
  14.6 5.6 %all-to-all-start = ((bf16[8,272,256]{2,1,0:T(8,128)(2,1)}), bf16[8,272,256]{2,1,0:T(8,128)(2,1)S(1)}, u32[]{:S(2)}, u32[]{:S(2)}) async-start(bf16[8,272,256]{2,1,0:T(8,128)(2,1)} %get-tuple-element.16), calls=%async_computation | async-start | bytes 2228224 | tf_op jit(solution)/shard_map/all_to_all | solution.py:404
  20.2 1.2 collective-permute-start
  21.4 3.9 %collective-permute-start.4 = (bf16[2,272,256]{2,1,0:T(8,128)(2,1)S(1)}, bf16[2,272,256]{2,1,0:T(8,128)(2,1)S(1)}, u32[]{:S(2)}, u32[]{:S(2)}) collective-permute-start(bf16[2,272,256]{2,1,0:T(8,128)(2,1)S(1)} %all_to_all.25.refs_2_), channel_id=1, source_target_pairs={{0,224},{32,0},{64,32},{96,64},{128,96},{160,128},{192,160},{224,1... | collective-permute-start | bytes 835592 | tf_op jit(solution)/shard_map/ppermute | solution.py:403
  25.3 6.9 %collective-permute-done.refs_3_ = bf16[2,272,256]{2,1,0:T(8,128)(2,1)S(1)} collective-permute-done((bf16[2,272,256]{2,1,0:T(8,128)(2,1)S(1)}, bf16[2,272,256]{2,1,0:T(8,128)(2,1)S(1)}, u32[]{:S(2)}, u32[]{:S(2)}) %collective-permute-start) | collective-permute-done | bytes 278560 | tf_op jit(solution)/shard_map/ppermute | solution.py:401
  32.3 0.0 collective-permute-start.1
  32.3 0.1 pad_add_fusion.info
  32.3 0.0 collective-permute-done.4.refs_4_
  32.4 3.2 %collective-permute-start.5 = (bf16[2,272,256]{2,1,0:T(8,128)(2,1)S(1)}, bf16[2,272,256]{2,1,0:T(8,128)(2,1)}, u32[]{:S(2)}, u32[]{:S(2)}) collective-permute-start(bf16[2,272,256]{2,1,0:T(8,128)(2,1)S(1)} %collective-permute-done.4.refs_4_), channel_id=1, source_target_pairs={{0,224},{32,0},{64,32},{96,64},{128,96},{160,128},{192,160},{224,1... | collective-permute-start | bytes 835592 | tf_op jit(solution)/shard_map/ppermute | solution.py:403
  35.6 0.0 copy-start.8
  35.6 0.7 copy-done.8
  36.3 5.5 %collective-permute-done.1.refs_2_ = bf16[2,272,256]{2,1,0:T(8,128)(2,1)} collective-permute-done((bf16[2,272,256]{2,1,0:T(8,128)(2,1)S(1)}, bf16[2,272,256]{2,1,0:T(8,128)(2,1)}, u32[]{:S(2)}, u32[]{:S(2)}) %collective-permute-start.1) | collective-permute-done | bytes 278560 | tf_op jit(solution)/shard_map/ppermute | solution.py:401
  41.8 0.0 collective-permute-start.2
  41.8 0.1 pad_add_fusion.2.info
  41.9 0.1 pad_add_fusion.1.info
  41.9 0.1 pad_add_fusion.3.info
  42.0 0.0 collective-permute-done.5.refs_3_
  42.0 3.3 %collective-permute-start.6 = (bf16[2,272,256]{2,1,0:T(8,128)(2,1)}, bf16[2,272,256]{2,1,0:T(8,128)(2,1)}, u32[]{:S(2)}, u32[]{:S(2)}) collective-permute-start(bf16[2,272,256]{2,1,0:T(8,128)(2,1)} %collective-permute-done.5.refs_3_), channel_id=1, source_target_pairs={{0,224},{32,0},{64,32},{96,64},{128,96},{160,128},{192,160},{224,1... | collective-permute-start | bytes 835592 | tf_op jit(solution)/shard_map/ppermute | solution.py:403
  45.3 5.4 %collective-permute-done.2.refs_2_ = bf16[2,272,256]{2,1,0:T(8,128)(2,1)} collective-permute-done((bf16[2,272,256]{2,1,0:T(8,128)(2,1)}, bf16[2,272,256]{2,1,0:T(8,128)(2,1)}, u32[]{:S(2)}, u32[]{:S(2)}) %collective-permute-start.2) | collective-permute-done | bytes 278560 | tf_op jit(solution)/shard_map/ppermute | solution.py:401
  50.7 0.0 collective-permute-start.3
  50.7 0.0 all-to-all-done.refs_0_.refs_1_
  50.7 0.0 copy-start.9
  50.7 1.0 copy-done.9
  51.6 10.9 %attend1.1 = (f32[8,256,256]{2,1,0:T(8,128)S(1)}, f32[8,256,128]{2,1,0:T(8,128)S(1)}) custom-call(s32[4]{0:T(128)S(1)} %pad_add_fusion.3.info, bf16[8,272,256]{2,1,0:T(8,128)(2,1)S(1)} %all-to-all-done.refs_0_.refs_1_, bf16[8,272,256]{2,1,0:T(8,128)(2,1)S(1)} %all-to-all-done.refs_0_.refs_1_, bf16[2,272,256]{2,1,0:T(8,128)(2,1)S(1)} %all_to_all.25.refs_2_, ...), custom_call_target="tpu_custom_call" | custom-call | flops 4831838208 | bytes 6000000 | tf_op jit(solution)/shard_map/attend1/pallas_call | solution.py:196
  62.5 11.0 %attend2.1 = (f32[8,256,256]{2,1,0:T(8,128)S(1)}, f32[8,256,128]{2,1,0:T(8,128)S(1)}) custom-call(s32[3]{0:T(128)S(1)} %pad_add_fusion.2.info, bf16[8,272,256]{2,1,0:T(8,128)(2,1)S(1)} %all-to-all-done.refs_0_.refs_1_, bf16[8,272,256]{2,1,0:T(8,128)(2,1)S(1)} %all-to-all-done.refs_0_.refs_1_, ...), custom_call_target="tpu_custom_call", output_to_operand_aliasing={{0}: (5, {}), {1}: (6, {})} | custom-call | flops 3221225472 | bytes 6000000 | tf_op jit(solution)/shard_map/attend2/pallas_call | solution.py:196
  73.5 0.0 collective-permute-done.6.refs_3_
  73.5 11.0 %attend3.1 = (f32[8,256,256]{2,1,0:T(8,128)S(1)}, f32[8,256,128]{2,1,0:T(8,128)S(1)}) custom-call(s32[3]{0:T(128)S(1)} %pad_add_fusion.1.info, bf16[8,272,256]{2,1,0:T(8,128)(2,1)S(1)} %all-to-all-done.refs_0_.refs_1_, bf16[8,272,256]{2,1,0:T(8,128)(2,1)S(1)} %all-to-all-done.refs_0_.refs_1_, ...), custom_call_target="tpu_custom_call", output_to_operand_aliasing={{0}: (5, {}), {1}: (6, {})} | custom-call | flops 3221225472 | bytes 6000000 | tf_op jit(solution)/shard_map/attend3/pallas_call | solution.py:196
  84.5 0.0 collective-permute-done.3.refs_2_
  84.5 11.9 %attend_last.1 = bf16[32,80,256]{2,1,0:T(8,128)(2,1)S(1)} custom-call(s32[2]{0:T(128)S(1)} %pad_add_fusion.info, bf16[8,272,256]{2,1,0:T(8,128)(2,1)S(1)} %all-to-all-done.refs_0_.refs_1_, bf16[8,272,256]{2,1,0:T(8,128)(2,1)S(1)} %all-to-all-done.refs_0_.refs_1_, bf16[2,272,256]{2,1,0:T(8,128)(2,1)S(1)} %collective-permute-done.3.refs_2_, ...), custom_call_target="tpu_custom_call" | custom-call | flops 1610612736 | bytes 6000000 | tf_op jit(solution)/shard_map/attend_last/pallas_call | solution.py:196
  96.5 0.0 copy-start.2
  96.5 1.1 copy-done.2
  97.6 0.0 copy-start.3
  97.6 7.4 %all-to-all-start.2 = ((bf16[32,80,256]{2,1,0:T(8,128)(2,1)}), bf16[32,80,256]{2,1,0:T(8,128)(2,1)S(1)}, u32[]{:S(2)}, u32[]{:S(2)}) async-start(bf16[32,80,256]{2,1,0:T(8,128)(2,1)} %copy-done.2), calls=%async_computation.2 | async-start | bytes 2621440 | tf_op jit(solution)/shard_map/all_to_all | solution.py:425
  105.0 19.0 %all-to-all-done.2.part_ref = bf16[32,80,256]{2,1,0:T(8,128)(2,1)S(1)} async-done(((bf16[32,80,256]{2,1,0:T(8,128)(2,1)}), bf16[32,80,256]{2,1,0:T(8,128)(2,1)S(1)}, u32[]{:S(2)}, u32[]{:S(2)}) %all-to-all-start.2) | async-done | bytes 1310752 | tf_op jit(solution)/shard_map/all_to_all | solution.py:425
  124.0 0.0 copy-done.3
  124.0 0.0 copy-done.6
  124.0 0.0 copy-done.7
  124.0 0.0 copy-start.1
  124.0 3.4 %copy-done.1 = bf16[2048,2048]{1,0:T(8,128)(2,1)S(1)} copy-done((bf16[2048,2048]{1,0:T(8,128)(2,1)S(1)}, bf16[2048,2048]{1,0:T(8,128)(2,1)}, u32[]{:S(2)}) %copy-start.1) | copy-done | bytes 8388632
  127.3 5.6 %post.1 = (bf16[64,2048]{1,0:T(8,128)(2,1)S(1)}, bf16[64,2048]{1,0:T(8,128)(2,1)S(1)}, bf16[64,8,2048]{2,1,0:T(8,128)(2,1)S(1)}) custom-call(s32[1]{0:T(128)} %bitcast.tp_ref, bf16[32,80,256]{2,1,0:T(8,128)(2,1)S(1)} %all-to-all-done.2.part_ref, bf16[2048,2048]{1,0:T(8,128)(2,1)S(1)} %copy-done.1, bf16[64,2048]{1,0:T(8,128)(2,1)S(1)} %copy-done.3, ...), custom_call_target="tpu_custom_call" | custom-call | tf_op jit(solution)/shard_map/post/pallas_call | solution.py:292
  132.9 0.0 copy-start.4
  132.9 0.0 copy-start.12
  132.9 60.0 %all_to_all.26 = bf16[64,8,2048]{2,1,0:T(8,128)(2,1)S(1)} all-to-all(bf16[64,8,2048]{2,1,0:T(8,128)(2,1)S(1)} %get-tuple-element.24), channel_id=1, replica_groups=mesh['z'=8,'y'=4,'c'=2,'tp'=4] {'z','y','c'}, dimensions={0} | all-to-all | bytes 4194304 | tf_op jit(solution)/shard_map/all_to_all | solution.py:430
  192.9 0.0 copy-done.4
  192.9 1.3 copy-done.10
  194.2 0.0 copy-done.12
  194.3 2.1 fusion.3
  196.4 0.0 copy-done
  196.4 0.0 copy-done.13
  196.4 5.5 %fusion = bf16[64,8,2048]{2,1,0:T(8,128)(2,1)} fusion(bf16[1,384,2048]{2,1,0:T(8,128)(2,1)S(1)} %copy-done, bf16[1,2048,384]{2,1,0:T(8,128)(2,1)S(1)} %copy-done.13, bf16[64,8,2048]{2,1,0:T(8,128)(2,1)} %copy-done.10, f32[512,384]{1,0:T(8,128)} %fusion.3), kind=kOutput, calls=%fused_computation.1 | convolution fusion | flops 1612840960 | bytes 8126464 | tf_op jit(solution)/shard_map/dot_general | solution.py:440
  201.9 5.8 %all-to-all-start.4 = ((bf16[64,8,2048]{2,1,0:T(8,128)(2,1)}), bf16[64,8,2048]{2,1,0:T(8,128)(2,1)}, u32[]{:S(2)}, u32[]{:S(2)}) async-start(bf16[64,8,2048]{2,1,0:T(8,128)(2,1)} %fusion), calls=%async_computation.4 | async-start | bytes 4194304 | tf_op jit(solution)/shard_map/all_to_all | solution.py:441
  207.6 0.0 copy-start.5
  207.7 0.1 copy.20.ids_ref
  207.8 0.0 copy-done.11
  207.8 0.1 copy.21.route_ref
  207.8 1.8 fusion.33
  209.6 0.0 copy-done.5
  209.6 2.7 %convert_add_fusion.base_ref = f32[64,2048]{1,0:T(8,128)S(1)} fusion(bf16[64,2048]{1,0:T(8,128)(2,1)S(1)} %copy-done.5, bf16[384,2048]{1,0:T(8,128)(2,1)} %param.29, bf16[64,2048]{1,0:T(8,128)(2,1)S(1)} %get-tuple-element.26, bf16[2048,384]{1,0:T(8,128)(2,1)} %param.28, f32[64,384]{1,0:T(8,128)S(1)} %fusion.33), kind=kOutput, calls=%fused_computation.14 | convolution fusion | flops 201736192 | bytes 4292608 | tf_op jit(solution)/shard_map/dot_general | solution.py:435
  212.3 46.5 %all-to-all-done.4.res_ref = bf16[64,8,2048]{2,1,0:T(8,128)(2,1)} async-done(((bf16[64,8,2048]{2,1,0:T(8,128)(2,1)}), bf16[64,8,2048]{2,1,0:T(8,128)(2,1)}, u32[]{:S(2)}, u32[]{:S(2)}) %all-to-all-start.4) | async-done | bytes 2097184 | tf_op jit(solution)/shard_map/all_to_all | solution.py:441
  258.8 3.5 %finish.1 = bf16[64,2048]{1,0:T(8,128)(2,1)} custom-call(bf16[64,8,2048]{2,1,0:T(8,128)(2,1)} %all-to-all-done.4.res_ref, f32[64,2048]{1,0:T(8,128)S(1)} %convert_add_fusion.base_ref, s32[64,4]{1,0:T(8,128)S(1)} %copy.20.ids_ref, f32[64,4]{1,0:T(8,128)S(1)} %copy.21.route_ref), custom_call_target="tpu_custom_call" | custom-call | tf_op jit(solution)/shard_map/finish/pallas_call | solution.py:360
  (6 shorter events, 0.0 us)
Async XLA Ops:
  6.5 189.9 %copy-start = (bf16[1,384,2048]{2,1,0:T(8,128)(2,1)S(1)}, bf16[1,384,2048]{2,1,0:T(8,128)(2,1)}, u32[]{:S(2)}) copy-start(bf16[1,384,2048]{2,1,0:T(8,128)(2,1)} %param.26) | copy-start | bytes 4718596
  6.5 117.4 %all-gather.2.cloned.1.call-start = ((), (), s32[]{:S(2)}) async-start(), calls=%async_computation.5 | async-start | bytes 10485760 | tf_op jit(solution)/shard_map/all_gather | solution.py:393
  14.6 36.1 %all-to-all-start = ((bf16[8,272,256]{2,1,0:T(8,128)(2,1)}), bf16[8,272,256]{2,1,0:T(8,128)(2,1)S(1)}, u32[]{:S(2)}, u32[]{:S(2)}) async-start(bf16[8,272,256]{2,1,0:T(8,128)(2,1)} %get-tuple-element.16), calls=%async_computation | async-start | bytes 2228224 | tf_op jit(solution)/shard_map/all_to_all | solution.py:404
  20.2 12.1 %collective-permute-start = (bf16[2,272,256]{2,1,0:T(8,128)(2,1)S(1)}, bf16[2,272,256]{2,1,0:T(8,128)(2,1)S(1)}, u32[]{:S(2)}, u32[]{:S(2)}) collective-permute-start(bf16[2,272,256]{2,1,0:T(8,128)(2,1)S(1)} %all_to_all.25.refs_2_), channel_id=1, source_target_pairs={{0,32},{32,64},{64,96},{96,128},{128,160},{160,192},{192,224},{224... | collective-permute-start | bytes 835592 | tf_op jit(solution)/shard_map/ppermute | solution.py:401
  21.4 11.0 %collective-permute-start.4 = (bf16[2,272,256]{2,1,0:T(8,128)(2,1)S(1)}, bf16[2,272,256]{2,1,0:T(8,128)(2,1)S(1)}, u32[]{:S(2)}, u32[]{:S(2)}) collective-permute-start(bf16[2,272,256]{2,1,0:T(8,128)(2,1)S(1)} %all_to_all.25.refs_2_), channel_id=1, source_target_pairs={{0,224},{32,0},{64,32},{96,64},{128,96},{160,128},{192,160},{224,1... | collective-permute-start | bytes 835592 | tf_op jit(solution)/shard_map/ppermute | solution.py:403
  32.3 9.5 %collective-permute-start.1 = (bf16[2,272,256]{2,1,0:T(8,128)(2,1)S(1)}, bf16[2,272,256]{2,1,0:T(8,128)(2,1)}, u32[]{:S(2)}, u32[]{:S(2)}) collective-permute-start(bf16[2,272,256]{2,1,0:T(8,128)(2,1)S(1)} %collective-permute-done.refs_3_), channel_id=1, source_target_pairs={{0,32},{32,64},{64,96},{96,128},{128,160},{160,192},{192,224},{224... | collective-permute-start | bytes 835592 | tf_op jit(solution)/shard_map/ppermute | solution.py:401
  32.4 9.7 %collective-permute-start.5 = (bf16[2,272,256]{2,1,0:T(8,128)(2,1)S(1)}, bf16[2,272,256]{2,1,0:T(8,128)(2,1)}, u32[]{:S(2)}, u32[]{:S(2)}) collective-permute-start(bf16[2,272,256]{2,1,0:T(8,128)(2,1)S(1)} %collective-permute-done.4.refs_4_), channel_id=1, source_target_pairs={{0,224},{32,0},{64,32},{96,64},{128,96},{160,128},{192,160},{224,1... | collective-permute-start | bytes 835592 | tf_op jit(solution)/shard_map/ppermute | solution.py:403
  35.6 0.7 copy-start.8
  41.8 8.9 %collective-permute-start.2 = (bf16[2,272,256]{2,1,0:T(8,128)(2,1)}, bf16[2,272,256]{2,1,0:T(8,128)(2,1)}, u32[]{:S(2)}, u32[]{:S(2)}) collective-permute-start(bf16[2,272,256]{2,1,0:T(8,128)(2,1)} %collective-permute-done.1.refs_2_), channel_id=1, source_target_pairs={{0,32},{32,64},{64,96},{96,128},{128,160},{160,192},{192,224},{224... | collective-permute-start | bytes 835592 | tf_op jit(solution)/shard_map/ppermute | solution.py:401
  42.0 31.5 %collective-permute-start.6 = (bf16[2,272,256]{2,1,0:T(8,128)(2,1)}, bf16[2,272,256]{2,1,0:T(8,128)(2,1)}, u32[]{:S(2)}, u32[]{:S(2)}) collective-permute-start(bf16[2,272,256]{2,1,0:T(8,128)(2,1)} %collective-permute-done.5.refs_3_), channel_id=1, source_target_pairs={{0,224},{32,0},{64,32},{96,64},{128,96},{160,128},{192,160},{224,1... | collective-permute-start | bytes 835592 | tf_op jit(solution)/shard_map/ppermute | solution.py:403
  50.7 33.9 %collective-permute-start.3 = (bf16[2,272,256]{2,1,0:T(8,128)(2,1)}, bf16[2,272,256]{2,1,0:T(8,128)(2,1)S(1)}, u32[]{:S(2)}, u32[]{:S(2)}) collective-permute-start(bf16[2,272,256]{2,1,0:T(8,128)(2,1)} %collective-permute-done.2.refs_2_), channel_id=1, source_target_pairs={{0,32},{32,64},{64,96},{96,128},{128,160},{160,192},{192,224},{224... | collective-permute-start | bytes 835592 | tf_op jit(solution)/shard_map/ppermute | solution.py:401
  50.7 1.0 copy-start.9
  96.5 1.1 copy-start.2
  97.6 26.4 %copy-start.3 = (bf16[64,2048]{1,0:T(8,128)(2,1)S(1)}, bf16[64,2048]{1,0:T(8,128)(2,1)}, u32[]{:S(2)}) copy-start(bf16[64,2048]{1,0:T(8,128)(2,1)} %res_ref.1) | copy-start | bytes 786436
  97.6 26.4 %copy-start.6 = (f32[2048]{0:T(1024)S(1)}, f32[2048]{0:T(1024)}, u32[]{:S(2)}) copy-start(f32[2048]{0:T(1024)} %param.21) | copy-start | bytes 24580
  97.6 26.4 %copy-start.7 = (s32[64,4]{0,1:T(4,128)S(1)}, s32[64,4]{0,1:T(4,128)}, u32[]{:S(2)}) copy-start(s32[64,4]{0,1:T(4,128)} %param.22) | copy-start | bytes 3076
  97.6 26.4 %all-to-all-start.2 = ((bf16[32,80,256]{2,1,0:T(8,128)(2,1)}), bf16[32,80,256]{2,1,0:T(8,128)(2,1)S(1)}, u32[]{:S(2)}, u32[]{:S(2)}) async-start(bf16[32,80,256]{2,1,0:T(8,128)(2,1)} %copy-done.2), calls=%async_computation.2 | async-start | bytes 2621440 | tf_op jit(solution)/shard_map/all_to_all | solution.py:425
  124.0 3.4 %copy-start.1 = (bf16[2048,2048]{1,0:T(8,128)(2,1)S(1)}, bf16[2048,2048]{1,0:T(8,128)(2,1)}, u32[]{:S(2)}) copy-start(bf16[2048,2048]{1,0:T(8,128)(2,1)} %all-gather.2.cloned.1.call-done.w_ref) | copy-start | bytes 25165828
  132.9 60.0 %copy-start.4 = (bf16[64,2048]{1,0:T(8,128)(2,1)}, bf16[64,2048]{1,0:T(8,128)(2,1)S(1)}, u32[]{:S(2)}) copy-start(bf16[64,2048]{1,0:T(8,128)(2,1)S(1)} %get-tuple-element.25) | copy-start | bytes 786436
  132.9 61.3 %copy-start.12 = (bf16[1,2048,384]{2,1,0:T(8,128)(2,1)S(1)}, bf16[1,2048,384]{2,1,0:T(8,128)(2,1)}, u32[]{:S(2)}) copy-start(bf16[1,2048,384]{2,1,0:T(8,128)(2,1)} %param.24) | copy-start | bytes 4718596
  192.9 1.3 copy-start.10
  194.3 2.1 copy-start.13
  201.9 5.9 %copy-start.11 = (f32[64,4]{0,1:T(4,128)S(1)}, f32[64,4]{0,1:T(4,128)}, u32[]{:S(2)}) copy-start(f32[64,4]{0,1:T(4,128)} %param.23) | copy-start | bytes 3076
  201.9 56.9 %all-to-all-start.4 = ((bf16[64,8,2048]{2,1,0:T(8,128)(2,1)}), bf16[64,8,2048]{2,1,0:T(8,128)(2,1)}, u32[]{:S(2)}, u32[]{:S(2)}) async-start(bf16[64,8,2048]{2,1,0:T(8,128)(2,1)} %fusion), calls=%async_computation.4 | async-start | bytes 4194304 | tf_op jit(solution)/shard_map/all_to_all | solution.py:441
  207.6 2.0 copy-start.5
Sparse Core Ops, SparseCore 0:
  9.1 88.4 all-gather.1

commit v2 on v1

--- a/solution.py
+++ b/solution.py
@@ -17,7 +17,7 @@
 LOG2E = math.log2(math.e)
 SCORE2 = HEAD_DIM**-0.5 * LOG2E
 LOW = -1e30
-TAIL = 16
+TAIL = 8
 
 BF = jnp.bfloat16
 F32 = jnp.float32
@@ -94,62 +94,75 @@
                 pair.append(jnp.where(info[1 + b] > 0, bias, -jnp.inf))
             biases.append(pair)
     lane = lax.broadcasted_iota(jnp.int32, (rows, HEAD_DIM), 1)
-    for i in range(tiles):
-        tile_first = (step * tiles + i) * rows
-        if not first:
-            stat_old = stat_in[i]
+
+    def score_tiles(i):
+        both = jnp.concatenate(
+            [q_ref[i, pl.ds(0, rows), pl.ds(j * HEAD_DIM, HEAD_DIM)] for j in range(2)], axis=0
+        )
+        found = [[], []]
+        for u in range(2 * blocks):
+            raw = lax.dot_general(
+                both, keys[u][...], (((1,), (1,)), ((), ())), preferred_element_type=F32
+            )
+            for j in range(2):
+                score = raw[j * rows : (j + 1) * rows] * SCORE2 + biases[u][j]
+                if own and u < 2:
+                    q_pos = (step * tiles + i) * rows + lax.broadcasted_iota(
+                        jnp.int32, (rows, rows), 0
+                    )
+                    k_pos = info[0] + u * rows + lax.broadcasted_iota(jnp.int32, (rows, rows), 1)
+                    score = jnp.where(q_pos >= k_pos, score, -jnp.inf)
+                found[j].append(score)
+        return found
+
+    def absorb(i, scores):
+        maxes, olds = [], []
+        for j in range(2):
+            top = scores[j][0]
+            for score in scores[j][1:]:
+                top = jnp.maximum(top, score)
+            row_max = jnp.max(top, axis=1, keepdims=True)
+            old_max = LOW if first else stat_in[i, :, j : j + 1]
+            olds.append(old_max)
+            maxes.append(jnp.maximum(row_max, old_max))
+        total = None
+        for u in range(2 * blocks):
+            weights = jnp.concatenate(
+                [jnp.exp2(scores[j][u] - maxes[j]).astype(BF) for j in range(2)], axis=0
+            )
+            value = jnp.concatenate([values[u][...], ones], axis=1)
+            part = jnp.dot(weights, value, preferred_element_type=F32)
+            total = part if total is None else total + part
         stat_new = jnp.zeros((rows, HEAD_DIM), F32)
         lse_rows = []
         for j in range(2):
             cols = pl.ds(j * HEAD_DIM, HEAD_DIM)
-            query = q_ref[i, pl.ds(0, rows), cols]
-            scores = []
-            for u in range(2 * blocks):
-                raw = lax.dot_general(
-                    query, keys[u][...], (((1,), (1,)), ((), ())), preferred_element_type=F32
-                )
-                score = raw * SCORE2 + biases[u][j]
-                if own and u < 2:
-                    q_pos = tile_first + lax.broadcasted_iota(jnp.int32, (rows, rows), 0)
-                    k_pos = info[0] + u * rows + lax.broadcasted_iota(jnp.int32, (rows, rows), 1)
-                    score = jnp.where(q_pos >= k_pos, score, -jnp.inf)
-                scores.append(score)
-            top = scores[0]
-            for score in scores[1:]:
-                top = jnp.maximum(top, score)
-            row_max = jnp.max(top, axis=1, keepdims=True)
-            if first:
-                row_max = jnp.maximum(row_max, LOW)
-            else:
-                old_max = stat_old[:, j : j + 1]
-                row_max = jnp.maximum(row_max, old_max)
-            total = None
-            for u in range(2 * blocks):
-                weights = jnp.exp2(scores[u] - row_max).astype(BF)
-                value = jnp.concatenate([values[u][...], ones], axis=1)
-                part = jnp.dot(weights, value, preferred_element_type=F32)
-                total = part if total is None else total + part
-            weighted = total[:, :HEAD_DIM]
-            row_sum = total[:, HEAD_DIM : HEAD_DIM + 1]
+            weighted = total[j * rows : (j + 1) * rows, :HEAD_DIM]
+            row_sum = total[j * rows : (j + 1) * rows, HEAD_DIM:]
             if not first:
-                factor = jnp.exp2(old_max - row_max)
+                factor = jnp.exp2(olds[j] - maxes[j])
                 weighted = weighted + acc_in[i, :, cols] * factor
-                row_sum = row_sum + stat_old[:, 2 + j : 3 + j] * factor
+                row_sum = row_sum + stat_in[i, :, 2 + j : 3 + j] * factor
             if last:
                 some = row_sum > 0.0
-                mixed = weighted * (1.0 / jnp.where(some, row_sum, 1.0))
+                row_sum = jnp.where(some, row_sum, 1.0)
+                mixed = weighted * (1.0 / row_sum)
                 per = rows // 4
                 for p in range(4):
                     o_out[4 * i + p, pl.ds(0, per), cols] = mixed[p * per : (p + 1) * per].astype(BF)
-                lse = jnp.where(some, row_max + jnp.log2(jnp.where(some, row_sum, 1.0)), LOW)
-                wide = jnp.broadcast_to(lse, (rows, rows))
-                eye = lax.broadcasted_iota(jnp.int32, (rows, rows), 0) == lax.broadcasted_iota(
-                    jnp.int32, (rows, rows), 1
+                lse = jnp.where(some, maxes[j] + jnp.log2(row_sum), LOW)
+                flat = []
+                eye = lax.broadcasted_iota(jnp.int32, (HEAD_DIM, HEAD_DIM), 0) == (
+                    lax.broadcasted_iota(jnp.int32, (HEAD_DIM, HEAD_DIM), 1)
                 )
-                lse_rows.append(jnp.sum(jnp.where(eye, wide, 0.0), axis=0, keepdims=True))
+                for at in range(0, rows, HEAD_DIM):
+                    flat.append(
+                        jnp.sum(jnp.where(eye, lse[at : at + HEAD_DIM], 0.0), axis=0, keepdims=True)
+                    )
+                lse_rows.append(jnp.concatenate(flat, axis=1))
             else:
                 acc_out[i, :, cols] = weighted
-                stat_new = jnp.where(lane == j, row_max, stat_new)
+                stat_new = jnp.where(lane == j, maxes[j], stat_new)
                 stat_new = jnp.where(lane == 2 + j, row_sum, stat_new)
         if last:
             tail = tail_block(lse_rows, rows)
@@ -158,8 +171,14 @@
         else:
             stat_out[i] = stat_new
 
-
-def attend(info, q_all, kvs, state, own, last, name, tiles=2):
+    pending = score_tiles(0)
+    for i in range(tiles):
+        following = score_tiles(i + 1) if i + 1 < tiles else None
+        absorb(i, pending)
+        pending = following
+
+
+def attend(info, q_all, kvs, state, own, last, name, tiles=4):
     count, padded, width = q_all.shape
     rows = padded - TAIL
     first = state is None
@@ -213,7 +232,18 @@
 
 
 def post_kernel(
-    tp_ref, part_ref, w_ref, res_ref, gain_ref, ids_ref, stream_out, normed_out, send_out, att, strm
+    place,
+    part_ref,
+    w_own_ref,
+    w_other_ref,
+    res_ref,
+    gain_ref,
+    ids_ref,
+    stream_out,
+    normed_out,
+    send_out,
+    att,
+    strm,
 ):
     step = pl.program_id(0)
     sources = part_ref.shape[0]
@@ -225,12 +255,12 @@
     @pl.when(step == 0)
     def _():
         pick = lax.broadcasted_iota(jnp.int32, (own_rows, width), 1) == (
-            tp_ref[0] * own_rows + lax.broadcasted_iota(jnp.int32, (own_rows, width), 0)
+            place[0] * own_rows + lax.broadcasted_iota(jnp.int32, (own_rows, width), 0)
         )
         for g in range(groups):
-            core, tp = g // (groups // 2), g % (groups // 2)
-            col = (tp * 2 + core) * width
-            tails = [part_ref[y * groups + g, own_rows:, :].astype(F32) for y in range(ys)]
+            source = ((g // (groups // 2)) ^ place[1]) * (groups // 2) + g % (groups // 2)
+            col = g * width
+            tails = [part_ref[y * groups + source, own_rows:, :].astype(F32) for y in range(ys)]
             for j in range(2):
                 sums = []
                 for y in range(ys):
@@ -247,14 +277,17 @@
                 mixed = None
                 for y in range(ys):
                     part = part_ref[
-                        y * groups + g, pl.ds(0, own_rows), pl.ds(j * HEAD_DIM, HEAD_DIM)
+                        y * groups + source, pl.ds(0, own_rows), pl.ds(j * HEAD_DIM, HEAD_DIM)
                     ].astype(F32) * (weights[y] * inverse)
                     mixed = part if mixed is None else mixed + part
                 att[:, pl.ds(col + j * HEAD_DIM, HEAD_DIM)] = mixed.astype(BF)
 
-    block = w_ref.shape[1]
+    block = w_own_ref.shape[1]
+    half = w_own_ref.shape[0]
     cols = pl.ds(pl.multiple_of(step * block, block), block)
-    branch = jnp.dot(att[...], w_ref[...], preferred_element_type=F32)
+    branch = jnp.dot(att[:, :half], w_own_ref[...], preferred_element_type=F32) + jnp.dot(
+        att[:, half:], w_other_ref[...], preferred_element_type=F32
+    )
     stream = (res_ref[...].astype(F32) + branch).astype(BF)
     stream_out[...] = stream
     strm[:, cols] = stream
@@ -283,12 +316,12 @@
         send_out[...] = sent.reshape(send_out.shape)
 
 
-def post(tp, parts, weight, residual, gain, ids_t, experts, cap):
+def post(place, parts, w_own, w_other, residual, gain, ids_t, experts, cap):
     rows, width = residual.shape
     block = 256
-    fixed2 = lambda g, tp: (0, 0)
-    fixed3 = lambda g, tp: (0, 0, 0)
-    tiled = lambda g, tp: (0, g)
+    fixed2 = lambda g, place: (0, 0)
+    fixed3 = lambda g, place: (0, 0, 0)
+    tiled = lambda g, place: (0, g)
     return pl.pallas_call(
         post_kernel,
         grid_spec=pltpu.PrefetchScalarGridSpec(
@@ -296,7 +329,8 @@
             grid=(width // block,),
             in_specs=[
                 pl.BlockSpec(parts.shape, fixed3),
-                pl.BlockSpec((width, block), tiled),
+                pl.BlockSpec((width // 2, block), tiled),
+                pl.BlockSpec((width // 2, block), tiled),
                 pl.BlockSpec((rows, block), tiled),
                 pl.BlockSpec((1, width), fixed2),
                 pl.BlockSpec(ids_t.shape, fixed2),
@@ -317,7 +351,39 @@
             dimension_semantics=("arbitrary",), vmem_limit_bytes=40 * 1024 * 1024
         ),
         name="post",
-    )(tp, parts, weight, residual, gain, ids_t)
+    )(place, parts, w_own, w_other, residual, gain, ids_t)
+
+
+def expert_kernel(x_ref, gate_ref, up_ref, down_ref, out_ref):
+    peers, cap, width = x_ref.shape
+    x = x_ref[...].reshape(peers * cap, width)
+    gate = jnp.dot(x, gate_ref[0], preferred_element_type=F32)
+    up = jnp.dot(x, up_ref[0], preferred_element_type=F32)
+    hidden = (gate / (1.0 + jnp.exp(-gate)) * up).astype(BF)
+    out = jnp.dot(hidden, down_ref[0], preferred_element_type=F32).astype(BF)
+    out_ref[...] = out.reshape(peers, cap, width)
+
+
+def expert(arrived, gate, up, down, steps=4):
+    peers, cap, width = arrived.shape
+    rows = pl.BlockSpec((peers // steps, cap, width), lambda g: (g, 0, 0))
+    whole = lambda g: (0, 0, 0)
+    return pl.pallas_call(
+        expert_kernel,
+        grid=(steps,),
+        in_specs=[
+            rows,
+            pl.BlockSpec(gate.shape, whole),
+            pl.BlockSpec(up.shape, whole),
+            pl.BlockSpec(down.shape, whole),
+        ],
+        out_specs=rows,
+        out_shape=jax.ShapeDtypeStruct(arrived.shape, BF),
+        compiler_params=pltpu.CompilerParams(
+            dimension_semantics=("arbitrary",), vmem_limit_bytes=40 * 1024 * 1024
+        ),
+        name="expert",
+    )(arrived, gate, up, down)
 
 
 def finish_kernel(res_ref, base_ref, ids_ref, route_ref, out_ref):
@@ -390,42 +456,40 @@
     experts = z_count * y_count * 2
     cap = 2 * residual.shape[0] * TOPK // experts
 
-    weight = lax.all_gather(out_weight, "tp", axis=0, tiled=True)
+    core = lax.axis_index("c")
+    half_rows = out_weight.shape[0] // 2
+    own_part = lax.dynamic_slice_in_dim(out_weight, core * half_rows, half_rows, 0)
+    w_own = lax.all_gather(own_part, "tp", axis=0, tiled=True)
     kv_send, q_send = pack(queries, key_rows, value_rows, forget_sums.T, y_count)
     own = lax.all_to_all(kv_send, "c", split_axis=0, concat_axis=0)
     up_ring = [(i, (i + 1) % z_count) for i in range(z_count)]
     down_ring = [(i, (i - 1) % z_count) for i in range(z_count)]
-    half = z_count // 2
-    ups, downs = [own], [own]
-    for s in range(1, half + 1):
-        ups.append(lax.ppermute(ups[-1], "z", up_ring))
-        if s < half:
-            downs.append(lax.ppermute(downs[-1], "z", down_ring))
     q_all = lax.all_to_all(q_send, ("y", "c"), split_axis=0, concat_axis=0)
 
+    def up(block):
+        return lax.ppermute(block, "z", up_ring)
+
+    def down(block):
+        return lax.ppermute(block, "z", down_ring)
+
     def flags(*steps):
-        good = []
-        for direction, s in steps:
-            if s == 0:
-                good.append(jnp.int32(1))
-            elif direction > 0:
-                good.append((z >= s).astype(jnp.int32))
-            else:
-                good.append((z + s >= z_count).astype(jnp.int32))
+        good = [(z >= s) if s >= 0 else (z - s >= z_count) for s in steps]
         return jnp.stack([2 * y * rows, *good]).astype(jnp.int32)
 
-    state = attend(
-        flags((1, 0), (1, 1), (-1, 1)), q_all, [own, ups[1], downs[1]], None, True, False, "attend1"
-    )
-    for s in range(2, half):
-        state = attend(
-            flags((1, s), (-1, s)), q_all, [ups[s], downs[s]], state, False, False, f"attend{s}"
-        )
-    sent = attend(flags((1, half)), q_all, [ups[half]], state, False, True, "attend_last")
+    up1, down1 = up(own), down(own)
+    up2, down2 = up(up1), down(down1)
+    up3, down3 = up(up2), down(down2)
+    state = attend(flags(0, 1, -1), q_all, [own, up1, down1], None, True, False, "attend1")
+    state, up3, down3 = lax.optimization_barrier((state, up3, down3))
+    up4 = up(up3)
+    state = attend(flags(2, -2), q_all, [up2, down2], state, False, False, "attend2")
+    sent = attend(flags(3, -3, 4), q_all, [up3, down3, up4], state, False, True, "attend3")
+    sent, w_own = lax.optimization_barrier((sent, w_own))
+    w_other = lax.ppermute(w_own, "c", [(0, 1), (1, 0)])
     parts = lax.all_to_all(sent, ("y", "c", "tp"), split_axis=0, concat_axis=0)
-    tp = lax.axis_index("tp").astype(jnp.int32).reshape(1)
+    place = jnp.stack([lax.axis_index("tp"), core]).astype(jnp.int32)
     stream, normed, outgoing = post(
-        tp, parts, weight, residual, norm_gain[None, :], expert_ids.T, experts, cap
+        place, parts, w_own, w_other, residual, norm_gain[None, :], expert_ids.T, experts, cap
     )
     arrived = lax.all_to_all(outgoing, ("z", "y", "c"), split_axis=0, concat_axis=0)
     shared_hidden = (
@@ -433,13 +497,9 @@
         * jnp.dot(normed, shared_up, preferred_element_type=F32)
     ).astype(BF)
     base = stream.astype(F32) + jnp.dot(shared_hidden, shared_down, preferred_element_type=F32)
-    tokens = arrived.reshape(experts * cap, -1)
-    gate_part = jnp.dot(tokens, expert_gate[0], preferred_element_type=F32)
-    up_part = jnp.dot(tokens, expert_up[0], preferred_element_type=F32)
-    hidden = (jax.nn.silu(gate_part) * up_part).astype(BF)
-    processed = jnp.dot(hidden, expert_down[0], preferred_element_type=F32).astype(BF)
+    processed = expert(arrived, expert_gate, expert_up, expert_down)
     returned = lax.all_to_all(
-        processed.reshape(arrived.shape), ("z", "y", "c"), split_axis=0, concat_axis=0
+        processed, ("z", "y", "c"), split_axis=0, concat_axis=0
     )
     return finish(returned, base, expert_ids, route_weights)
 

time: 270 us -> 250 us (0.926)
  matrix products: 12.1 us -> 4.47 us
  waiting for transfers between devices: 84 us -> 76.9 us
  Pallas kernels: 56.2 us -> 49.5 us
    pallas_call x4 -> x3, Pallas kernels: 44.8 us -> 30.7 us  [attend(): pl.pallas_call(functools.partial(attend_kernel, blocks=blocks, own=own, f...]
    dot_general x2 -> x0, matrix products: 7.61 us -> none  [the longest x1 5.47 us: local(): jnp.dot(hidden, expert_down[0], preferred_element_type=F32).astype(BF)]
    ppermute x7 -> x8, waiting for transfers between devices: 17.8 us -> 12.9 us  [the longest x4 12.8 us: up(): return lax.ppermute(block, 'z', up_ring)]
    pallas_call x0 -> x1, Pallas kernels: none -> 4.4 us  [expert(): pl.pallas_call(expert_kernel, grid=(steps,), in_specs=[rows, pl.BlockSpec...]
    pallas_call x1, Pallas kernels: 5.56 us -> 8.59 us  [post(): pl.pallas_call(post_kernel, grid_spec=pltpu.PrefetchScalarGridSpec(num_sc...]
    unnamed x30 -> x28, local copies, waits for them, and re-layouts: 7.69 us -> 7.3 us
    ppermute x7 -> x8, starting transfers between devices: 11.7 us -> 11.9 us  [the longest x3 10.4 us: down(): return lax.ppermute(block, 'z', down_ring)]
  transfers between devices with their start and end apart: 11 -> 12, of which waited for: 5 -> 4; matrix products, arithmetic and copies ran while one was open for 2% -> 2% of each run, Pallas kernels for 17% -> 13%
where the time goes in v2:
time: 250 us; the launch traced here: 249 us
  waiting for transfers between devices  76.9 us (31%)
  blocking collectives  65.2 us (26%)
  Pallas kernels  49.5 us (20%)
  starting transfers between devices  30.8 us (12%)
  between operations  13.6 us (5%)
  local copies, waits for them, and re-layouts  8.4 us (3%)
  matrix products  4.47 us (2%)
    all_to_all x1, blocking collectives, local(): lax.all_to_all(outgoing, ('z', 'y', 'c'), split_axis=0, concat_axis=0)  60.2 us
    all_to_all x1, waiting for transfers between devices, local(): lax.all_to_all(processed, ('z', 'y', 'c'), split_axis=0, concat_axis=0)  46.4 us
    pallas_call x3, Pallas kernels, attend(): pl.pallas_call(functools.partial(attend_kernel, blocks=blocks, own=own, f...  30.7 us
    all_to_all x1, waiting for transfers between devices, local(): parts = lax.all_to_all(sent, ('y', 'c', 'tp'), split_axis=0, concat_axis=0)  17.5 us
    ppermute x4, waiting for transfers between devices, up(): return lax.ppermute(block, 'z', up_ring)  12.8 us
    ppermute x3, starting transfers between devices, down(): return lax.ppermute(block, 'z', down_ring)  10.4 us
    pallas_call x1, Pallas kernels, post(): pl.pallas_call(post_kernel, grid_spec=pltpu.PrefetchScalarGridSpec(num_sc...  8.59 us
    all_to_all x1, starting transfers between devices, local(): parts = lax.all_to_all(sent, ('y', 'c', 'tp'), split_axis=0, concat_axis=0)  7.57 us
  transfers between devices with their start and end apart: 12, of which 4 were waited for; matrix products, arithmetic and copies ran while one was open for 2% of the time, Pallas kernels for 13%

profile of v2, /device:TPU:8, one launch (start us, length us, event | category | flops | bytes accessed | tf_op | source)
XLA Modules:
  0.0 249.2 jit_solution(12355680399873007604)
XLA Ops:
  6.5 0.0 copy-start
  6.5 0.0 all-gather.2.cloned.1.call-start
  6.5 1.6 copy-done
  8.1 1.1 constant_dynamic-slice_fusion
  9.2 0.0 all-gather.2.cloned.1.call-update
  9.3 2.3 pack.1
  11.5 5.0 %all_to_all.25.refs_2_ = bf16[2,264,256]{2,1,0:T(8,128)(2,1)S(1)} all-to-all(bf16[2,264,256]{2,1,0:T(8,128)(2,1)} %get-tuple-element.21), channel_id=1, replica_groups=mesh['z'=8,'y'=4,'c'=2,'tp'=4] {'c'}, dimensions={0} | all-to-all | bytes 540672 | tf_op jit(solution)/shard_map/all_to_all | solution.py:464
  16.5 5.6 %all-to-all-start = ((bf16[8,264,256]{2,1,0:T(8,128)(2,1)}), bf16[8,264,256]{2,1,0:T(8,128)(2,1)S(1)}, u32[]{:S(2)}, u32[]{:S(2)}) async-start(bf16[8,264,256]{2,1,0:T(8,128)(2,1)} %get-tuple-element.20), calls=%async_computation | async-start | bytes 2162688 | tf_op jit(solution)/shard_map/all_to_all | solution.py:467
  22.2 1.2 collective-permute-start
  23.4 3.9 %collective-permute-start.1 = (bf16[2,264,256]{2,1,0:T(8,128)(2,1)S(1)}, bf16[2,264,256]{2,1,0:T(8,128)(2,1)}, u32[]{:S(2)}, u32[]{:S(2)}) collective-permute-start(bf16[2,264,256]{2,1,0:T(8,128)(2,1)S(1)} %all_to_all.25.refs_2_), channel_id=1, source_target_pairs={{0,224},{32,0},{64,32},{96,64},{128,96},{160,128},{192,160},{224,1... | collective-permute-start | bytes 811016 | tf_op jit(solution)/shard_map/ppermute | solution.py:473
  27.3 6.9 %collective-permute-done.refs_3_ = bf16[2,264,256]{2,1,0:T(8,128)(2,1)} collective-permute-done((bf16[2,264,256]{2,1,0:T(8,128)(2,1)S(1)}, bf16[2,264,256]{2,1,0:T(8,128)(2,1)}, u32[]{:S(2)}, u32[]{:S(2)}) %collective-permute-start) | collective-permute-done | bytes 270368 | tf_op jit(solution)/shard_map/ppermute | solution.py:470
  34.2 0.0 collective-permute-start.2
  34.2 0.0 collective-permute-done.1.refs_4_
  34.2 3.2 %collective-permute-start.4 = (bf16[2,264,256]{2,1,0:T(8,128)(2,1)}, bf16[2,264,256]{2,1,0:T(8,128)(2,1)}, u32[]{:S(2)}, u32[]{:S(2)}) collective-permute-start(bf16[2,264,256]{2,1,0:T(8,128)(2,1)} %collective-permute-done.1.refs_4_), channel_id=1, source_target_pairs={{0,224},{32,0},{64,32},{96,64},{128,96},{160,128},{192,160},{224,1... | collective-permute-start | bytes 811016 | tf_op jit(solution)/shard_map/ppermute | solution.py:473
  37.4 0.1 pad_add_fusion.3.info
  37.5 0.1 pad_add_fusion.2.info
  37.6 0.1 pad_add_fusion.1.info
  37.6 6.0 %collective-permute-done.2.refs_2_ = bf16[2,264,256]{2,1,0:T(8,128)(2,1)} collective-permute-done((bf16[2,264,256]{2,1,0:T(8,128)(2,1)}, bf16[2,264,256]{2,1,0:T(8,128)(2,1)}, u32[]{:S(2)}, u32[]{:S(2)}) %collective-permute-start.2) | collective-permute-done | bytes 270368 | tf_op jit(solution)/shard_map/ppermute | solution.py:470
  43.6 0.0 collective-permute-start.3
  43.6 0.0 collective-permute-done.4.refs_3_
  43.6 3.2 %collective-permute-start.5 = (bf16[2,264,256]{2,1,0:T(8,128)(2,1)}, bf16[2,264,256]{2,1,0:T(8,128)(2,1)}, u32[]{:S(2)}, u32[]{:S(2)}) collective-permute-start(bf16[2,264,256]{2,1,0:T(8,128)(2,1)} %collective-permute-done.4.refs_3_), channel_id=1, source_target_pairs={{0,224},{32,0},{64,32},{96,64},{128,96},{160,128},{192,160},{224,1... | collective-permute-start | bytes 811016 | tf_op jit(solution)/shard_map/ppermute | solution.py:473
  46.9 0.0 all-to-all-done.refs_0_.refs_1_
  46.9 9.8 %attend1.1 = (f32[8,256,256]{2,1,0:T(8,128)S(1)}, f32[8,256,128]{2,1,0:T(8,128)S(1)}) custom-call(s32[4]{0:T(128)S(1)} %pad_add_fusion.2.info, bf16[8,264,256]{2,1,0:T(8,128)(2,1)S(1)} %all-to-all-done.refs_0_.refs_1_, bf16[8,264,256]{2,1,0:T(8,128)(2,1)S(1)} %all-to-all-done.refs_0_.refs_1_, bf16[2,264,256]{2,1,0:T(8,128)(2,1)S(1)} %all_to_all.25.refs_2_, ...), custom_call_target="tpu_custom_call" | custom-call | flops 4831838208 | bytes 6000000 | tf_op jit(solution)/shard_map/attend1/pallas_call | solution.py:215
  56.7 0.0 collective-permute-done.3.refs_2_
  56.7 0.0 collective-permute-done.5.refs_3_
  56.7 0.3 collective-permute-start.6
  57.0 10.0 %attend2.1 = (f32[8,256,256]{2,1,0:T(8,128)S(1)}, f32[8,256,128]{2,1,0:T(8,128)S(1)}) custom-call(s32[3]{0:T(128)S(1)} %pad_add_fusion.3.info, bf16[8,264,256]{2,1,0:T(8,128)(2,1)S(1)} %all-to-all-done.refs_0_.refs_1_, bf16[8,264,256]{2,1,0:T(8,128)(2,1)S(1)} %all-to-all-done.refs_0_.refs_1_, ...), custom_call_target="tpu_custom_call", output_to_operand_aliasing={{0}: (5, {}), {1}: (6, {})} | custom-call | flops 3221225472 | bytes 6000000 | tf_op jit(solution)/shard_map/attend2/pallas_call | solution.py:215
  67.0 0.0 collective-permute-done.6.refs_4_
  67.0 10.9 %attend3.1 = bf16[32,72,256]{2,1,0:T(8,128)(2,1)S(1)} custom-call(s32[4]{0:T(128)S(1)} %pad_add_fusion.1.info, bf16[8,264,256]{2,1,0:T(8,128)(2,1)S(1)} %all-to-all-done.refs_0_.refs_1_, bf16[8,264,256]{2,1,0:T(8,128)(2,1)S(1)} %all-to-all-done.refs_0_.refs_1_, bf16[2,264,256]{2,1,0:T(8,128)(2,1)} %collective-permute-done.3.refs_2_, ...), custom_call_target="tpu_custom_call" | custom-call | flops 4831838208 | bytes 6000000 | tf_op jit(solution)/shard_map/attend3/pallas_call | solution.py:215
  77.9 0.0 copy-start.6
  77.9 1.0 copy-done.6
  78.9 0.0 copy-start.10
  79.0 0.0 collective-permute-start.7
  79.0 7.6 %all-to-all-start.2 = ((bf16[32,72,256]{2,1,0:T(8,128)(2,1)}), bf16[32,72,256]{2,1,0:T(8,128)(2,1)S(1)}, u32[]{:S(2)}, u32[]{:S(2)}) async-start(bf16[32,72,256]{2,1,0:T(8,128)(2,1)} %copy-done.6), calls=%async_computation.2 | async-start | bytes 2359296 | tf_op jit(solution)/shard_map/all_to_all | solution.py:489
  86.5 0.1 pad_add_fusion.place
  86.6 17.5 %all-to-all-done.2.part_ref = bf16[32,72,256]{2,1,0:T(8,128)(2,1)S(1)} async-done(((bf16[32,72,256]{2,1,0:T(8,128)(2,1)}), bf16[32,72,256]{2,1,0:T(8,128)(2,1)S(1)}, u32[]{:S(2)}, u32[]{:S(2)}) %all-to-all-start.2) | async-done | bytes 1179680 | tf_op jit(solution)/shard_map/all_to_all | solution.py:489
  104.2 0.0 collective-permute-done.7.w_other_ref
  104.2 0.0 copy-done.10
  104.2 0.0 copy-done.11
  104.2 0.0 copy-start.2
  104.2 2.2 copy-done.2
  106.4 0.9 copy-done.7
  107.3 8.6 %post.1 = (bf16[64,2048]{1,0:T(8,128)(2,1)S(1)}, bf16[64,2048]{1,0:T(8,128)(2,1)S(1)}, bf16[64,8,2048]{2,1,0:T(8,128)(2,1)S(1)}) custom-call(s32[2]{0:T(128)S(1)} %pad_add_fusion.place, bf16[32,72,256]{2,1,0:T(8,128)(2,1)S(1)} %all-to-all-done.2.part_ref, bf16[1024,2048]{1,0:T(8,128)(2,1)S(1)} %copy-done.2, ...), custom_call_target="tpu_custom_call" | custom-call | tf_op jit(solution)/shard_map/post/pallas_call | solution.py:325
  115.9 0.0 copy-start.8
  115.9 0.0 copy-start.3
  115.9 0.0 copy-start.4
  115.9 60.2 %all_to_all.26.x_ref = bf16[64,8,2048]{2,1,0:T(8,128)(2,1)S(1)} all-to-all(bf16[64,8,2048]{2,1,0:T(8,128)(2,1)S(1)} %get-tuple-element.32), channel_id=1, replica_groups=mesh['z'=8,'y'=4,'c'=2,'tp'=4] {'z','y','c'}, dimensions={0} | all-to-all | bytes 4194304 | tf_op jit(solution)/shard_map/all_to_all | solution.py:494
  176.1 0.0 copy-done.8
  176.1 0.0 copy-done.5
  176.1 0.0 copy-done.3
  176.1 0.0 copy-done.4
  176.2 4.4 %expert.1 = bf16[64,8,2048]{2,1,0:T(8,128)(2,1)S(1)} custom-call(bf16[64,8,2048]{2,1,0:T(8,128)(2,1)S(1)} %all_to_all.26.x_ref, bf16[1,2048,384]{2,1,0:T(8,128)(2,1)S(1)} %copy-done.3, bf16[1,2048,384]{2,1,0:T(8,128)(2,1)S(1)} %copy-done.4, bf16[1,384,2048]{2,1,0:T(8,128)(2,1)S(1)} %copy-done.5), custom_call_target="tpu_custom_call" | custom-call | tf_op jit(solution)/shard_map/expert/pallas_call | solution.py:371
  180.6 0.0 copy-start.1
  180.6 1.3 copy-done.1
  181.9 5.7 %all-to-all-start.4 = ((bf16[64,8,2048]{2,1,0:T(8,128)(2,1)}), bf16[64,8,2048]{2,1,0:T(8,128)(2,1)}, u32[]{:S(2)}, u32[]{:S(2)}) async-start(bf16[64,8,2048]{2,1,0:T(8,128)(2,1)} %copy-done.1), calls=%async_computation.4 | async-start | bytes 4194304 | tf_op jit(solution)/shard_map/all_to_all | solution.py:501
  187.6 0.0 copy-start.9
  187.7 0.1 copy.18.ids_ref
  187.8 0.0 copy-done.12
  187.8 0.1 copy.19.route_ref
  187.9 1.8 fusion.5
  189.6 0.0 copy-done.9
  189.6 2.7 %convert_add_fusion.base_ref = f32[64,2048]{1,0:T(8,128)S(1)} fusion(bf16[64,2048]{1,0:T(8,128)(2,1)S(1)} %copy-done.9, bf16[384,2048]{1,0:T(8,128)(2,1)} %param.29, f32[64,384]{1,0:T(8,128)S(1)} %fusion.5, bf16[64,2048]{1,0:T(8,128)(2,1)S(1)} %get-tuple-element.34, bf16[2048,384]{1,0:T(8,128)(2,1)} %param.28), kind=kOutput, calls=%fused_computation | convolution fusion | flops 201736192 | bytes 4292608 | tf_op jit(solution)/shard_map/dot_general | solution.py:499
  192.4 46.4 %all-to-all-done.4.res_ref = bf16[64,8,2048]{2,1,0:T(8,128)(2,1)} async-done(((bf16[64,8,2048]{2,1,0:T(8,128)(2,1)}), bf16[64,8,2048]{2,1,0:T(8,128)(2,1)}, u32[]{:S(2)}, u32[]{:S(2)}) %all-to-all-start.4) | async-done | bytes 2097184 | tf_op jit(solution)/shard_map/all_to_all | solution.py:501
  238.8 3.5 %finish.1 = bf16[64,2048]{1,0:T(8,128)(2,1)} custom-call(bf16[64,8,2048]{2,1,0:T(8,128)(2,1)} %all-to-all-done.4.res_ref, f32[64,2048]{1,0:T(8,128)S(1)} %convert_add_fusion.base_ref, s32[64,4]{1,0:T(8,128)S(1)} %copy.18.ids_ref, f32[64,4]{1,0:T(8,128)S(1)} %copy.19.route_ref), custom_call_target="tpu_custom_call" | custom-call | tf_op jit(solution)/shard_map/finish/pallas_call | solution.py:426
  (5 shorter events, 0.0 us)
Async XLA Ops:
  6.5 1.6 copy-start
  6.5 72.4 %all-gather.2.cloned.1.call-start = ((), (), s32[]{:S(2)}) async-start(), calls=%async_computation.5 | async-start | bytes 5242880 | tf_op jit(solution)/shard_map/all_gather | solution.py:462
  16.5 30.3 %all-to-all-start = ((bf16[8,264,256]{2,1,0:T(8,128)(2,1)}), bf16[8,264,256]{2,1,0:T(8,128)(2,1)S(1)}, u32[]{:S(2)}, u32[]{:S(2)}) async-start(bf16[8,264,256]{2,1,0:T(8,128)(2,1)} %get-tuple-element.20), calls=%async_computation | async-start | bytes 2162688 | tf_op jit(solution)/shard_map/all_to_all | solution.py:467
  22.2 12.0 %collective-permute-start = (bf16[2,264,256]{2,1,0:T(8,128)(2,1)S(1)}, bf16[2,264,256]{2,1,0:T(8,128)(2,1)}, u32[]{:S(2)}, u32[]{:S(2)}) collective-permute-start(bf16[2,264,256]{2,1,0:T(8,128)(2,1)S(1)} %all_to_all.25.refs_2_), channel_id=1, source_target_pairs={{0,32},{32,64},{64,96},{96,128},{128,160},{160,192},{192,224},{224... | collective-permute-start | bytes 811016 | tf_op jit(solution)/shard_map/ppermute | solution.py:470
  23.4 10.8 %collective-permute-start.1 = (bf16[2,264,256]{2,1,0:T(8,128)(2,1)S(1)}, bf16[2,264,256]{2,1,0:T(8,128)(2,1)}, u32[]{:S(2)}, u32[]{:S(2)}) collective-permute-start(bf16[2,264,256]{2,1,0:T(8,128)(2,1)S(1)} %all_to_all.25.refs_2_), channel_id=1, source_target_pairs={{0,224},{32,0},{64,32},{96,64},{128,96},{160,128},{192,160},{224,1... | collective-permute-start | bytes 811016 | tf_op jit(solution)/shard_map/ppermute | solution.py:473
  34.2 9.5 %collective-permute-start.2 = (bf16[2,264,256]{2,1,0:T(8,128)(2,1)}, bf16[2,264,256]{2,1,0:T(8,128)(2,1)}, u32[]{:S(2)}, u32[]{:S(2)}) collective-permute-start(bf16[2,264,256]{2,1,0:T(8,128)(2,1)} %collective-permute-done.refs_3_), channel_id=1, source_target_pairs={{0,32},{32,64},{64,96},{96,128},{128,160},{160,192},{192,224},{224... | collective-permute-start | bytes 811016 | tf_op jit(solution)/shard_map/ppermute | solution.py:470
  34.2 9.5 %collective-permute-start.4 = (bf16[2,264,256]{2,1,0:T(8,128)(2,1)}, bf16[2,264,256]{2,1,0:T(8,128)(2,1)}, u32[]{:S(2)}, u32[]{:S(2)}) collective-permute-start(bf16[2,264,256]{2,1,0:T(8,128)(2,1)} %collective-permute-done.1.refs_4_), channel_id=1, source_target_pairs={{0,224},{32,0},{64,32},{96,64},{128,96},{160,128},{192,160},{224,1... | collective-permute-start | bytes 811016 | tf_op jit(solution)/shard_map/ppermute | solution.py:473
  43.6 13.0 %collective-permute-start.3 = (bf16[2,264,256]{2,1,0:T(8,128)(2,1)}, bf16[2,264,256]{2,1,0:T(8,128)(2,1)}, u32[]{:S(2)}, u32[]{:S(2)}) collective-permute-start(bf16[2,264,256]{2,1,0:T(8,128)(2,1)} %collective-permute-done.2.refs_2_), channel_id=1, source_target_pairs={{0,32},{32,64},{64,96},{96,128},{128,160},{160,192},{192,224},{224... | collective-permute-start | bytes 811016 | tf_op jit(solution)/shard_map/ppermute | solution.py:470
  43.6 13.0 %collective-permute-start.5 = (bf16[2,264,256]{2,1,0:T(8,128)(2,1)}, bf16[2,264,256]{2,1,0:T(8,128)(2,1)}, u32[]{:S(2)}, u32[]{:S(2)}) collective-permute-start(bf16[2,264,256]{2,1,0:T(8,128)(2,1)} %collective-permute-done.4.refs_3_), channel_id=1, source_target_pairs={{0,224},{32,0},{64,32},{96,64},{128,96},{160,128},{192,160},{224,1... | collective-permute-start | bytes 811016 | tf_op jit(solution)/shard_map/ppermute | solution.py:473
  56.7 10.3 %collective-permute-start.6 = (bf16[2,264,256]{2,1,0:T(8,128)(2,1)}, bf16[2,264,256]{2,1,0:T(8,128)(2,1)S(1)}, u32[]{:S(2)}, u32[]{:S(2)}) collective-permute-start(bf16[2,264,256]{2,1,0:T(8,128)(2,1)} %collective-permute-done.3.refs_2_), channel_id=1, source_target_pairs={{0,32},{32,64},{64,96},{96,128},{128,160},{160,192},{192,224},{224... | collective-permute-start | bytes 811016 | tf_op jit(solution)/shard_map/ppermute | solution.py:470
  77.9 1.0 copy-start.6
  78.9 25.2 %copy-start.10 = (f32[2048]{0:T(1024)S(1)}, f32[2048]{0:T(1024)}, u32[]{:S(2)}) copy-start(f32[2048]{0:T(1024)} %param.21) | copy-start | bytes 24580
  79.0 25.2 %copy-start.11 = (s32[64,4]{0,1:T(4,128)S(1)}, s32[64,4]{0,1:T(4,128)}, u32[]{:S(2)}) copy-start(s32[64,4]{0,1:T(4,128)} %param.22) | copy-start | bytes 3076
  79.0 25.2 %collective-permute-start.7 = (bf16[1024,2048]{1,0:T(8,128)(2,1)}, bf16[1024,2048]{1,0:T(8,128)(2,1)}, u32[]{:S(2)}, u32[]{:S(2)}) collective-permute-start(bf16[1024,2048]{1,0:T(8,128)(2,1)} %all-gather.2.cloned.1.call-done.w_own_ref), channel_id=1, source_target_pairs={{0,4},{4,0},{1,5},{5,1},{2,6},{6,2},{3,7},{7,3},{8,12},{12,8},{9,1... | collective-permute-start | bytes 12582920 | tf_op jit(solution)/shard_map/ppermute | solution.py:488
  79.0 25.2 %all-to-all-start.2 = ((bf16[32,72,256]{2,1,0:T(8,128)(2,1)}), bf16[32,72,256]{2,1,0:T(8,128)(2,1)S(1)}, u32[]{:S(2)}, u32[]{:S(2)}) async-start(bf16[32,72,256]{2,1,0:T(8,128)(2,1)} %copy-done.6), calls=%async_computation.2 | async-start | bytes 2359296 | tf_op jit(solution)/shard_map/all_to_all | solution.py:489
  104.2 2.2 copy-start.2
  106.4 0.9 copy-start.7
  107.3 68.8 %copy-start.5 = (bf16[1,384,2048]{2,1,0:T(8,128)(2,1)S(1)}, bf16[1,384,2048]{2,1,0:T(8,128)(2,1)}, u32[]{:S(2)}) copy-start(bf16[1,384,2048]{2,1,0:T(8,128)(2,1)} %down_ref.1) | copy-start | bytes 4718596
  115.9 60.2 %copy-start.8 = (bf16[64,2048]{1,0:T(8,128)(2,1)}, bf16[64,2048]{1,0:T(8,128)(2,1)S(1)}, u32[]{:S(2)}) copy-start(bf16[64,2048]{1,0:T(8,128)(2,1)S(1)} %get-tuple-element.33) | copy-start | bytes 786436
  115.9 60.2 %copy-start.3 = (bf16[1,2048,384]{2,1,0:T(8,128)(2,1)S(1)}, bf16[1,2048,384]{2,1,0:T(8,128)(2,1)}, u32[]{:S(2)}) copy-start(bf16[1,2048,384]{2,1,0:T(8,128)(2,1)} %gate_ref.1) | copy-start | bytes 4718596
  115.9 60.2 %copy-start.4 = (bf16[1,2048,384]{2,1,0:T(8,128)(2,1)S(1)}, bf16[1,2048,384]{2,1,0:T(8,128)(2,1)}, u32[]{:S(2)}) copy-start(bf16[1,2048,384]{2,1,0:T(8,128)(2,1)} %up_ref.1) | copy-start | bytes 4718596
  180.6 1.3 copy-start.1
  181.9 5.9 %copy-start.12 = (f32[64,4]{0,1:T(4,128)S(1)}, f32[64,4]{0,1:T(4,128)}, u32[]{:S(2)}) copy-start(f32[64,4]{0,1:T(4,128)} %param.23) | copy-start | bytes 3076
  181.9 56.9 %all-to-all-start.4 = ((bf16[64,8,2048]{2,1,0:T(8,128)(2,1)}), bf16[64,8,2048]{2,1,0:T(8,128)(2,1)}, u32[]{:S(2)}, u32[]{:S(2)}) async-start(bf16[64,8,2048]{2,1,0:T(8,128)(2,1)} %copy-done.1), calls=%async_computation.4 | async-start | bytes 4194304 | tf_op jit(solution)/shard_map/all_to_all | solution.py:501
  187.6 2.0 copy-start.9
Sparse Core Ops, SparseCore 0:
  9.4 53.5 all-gather.1

commit v3 on v2

v3 whole, which is shorter than its diff:
```python
import functools
import math

import jax
import jax.numpy as jnp
from jax import lax
from jax.experimental import pallas as pl
from jax.experimental.pallas import tpu as pltpu
from jax.sharding import Mesh, PartitionSpec as P

HEAD_DIM = 128
TOPK = 4
ROUTED_SCALE = 2.5
NORM_EPS = 1e-06
LOG2E = math.log2(math.e)
SCORE2 = HEAD_DIM**-0.5 * LOG2E
LOW = -1e30
TAIL = 8

BF = jnp.bfloat16
F32 = jnp.float32


def pieces(row):
    high = row.astype(BF)
    rest = row - high.astype(F32)
    mid = rest.astype(BF)
    low = (rest - mid.astype(F32)).astype(BF)
    return [high.astype(F32), mid.astype(F32), low.astype(F32)]


def tail_block(rows, width):
    parts = [piece for row in rows for piece in pieces(row)]
    parts.append(jnp.zeros((TAIL - len(parts), width), F32))
    return jnp.concatenate(parts, axis=0).astype(BF)


def row_of(tail, j):
    return tail[3 * j : 3 * j + 1] + tail[3 * j + 1 : 3 * j + 2] + tail[3 * j + 2 : 3 * j + 3]


def pack_keys_kernel(k_ref, v_ref, f_ref, out):
    rows = k_ref.shape[0]
    for c in range(2):
        out[c, :rows, :HEAD_DIM] = k_ref[:, c * HEAD_DIM : (c + 1) * HEAD_DIM]
        out[c, :rows, HEAD_DIM:] = v_ref[:, c * HEAD_DIM : (c + 1) * HEAD_DIM]
        out[c, rows:, :] = tail_block([f_ref[2 * c : 2 * c + 1, :], f_ref[2 * c + 1 : 2 * c + 2, :]], rows)


def pack_queries_kernel(q_ref, f_ref, _, out):
    rows = q_ref.shape[0]
    for c in range(2):
        tail = tail_block([f_ref[2 * c : 2 * c + 1, :], f_ref[2 * c + 1 : 2 * c + 2, :]], rows)
        part = q_ref[:, c * 2 * HEAD_DIM : (c + 1) * 2 * HEAD_DIM]
        for y in range(out.shape[0] // 2):
            out[2 * y + c, :rows, :] = part
            out[2 * y + c, rows:, :] = tail


def pack_keys(k, v, f_t):
    return pl.pallas_call(
        pack_keys_kernel,
        out_shape=pltpu.HBM((2, k.shape[0] + TAIL, 2 * HEAD_DIM), BF),
        name="pack_keys",
    )(k, v, f_t)


def pack_queries(q, f_t, after, ys):
    return pl.pallas_call(
        pack_queries_kernel,
        in_specs=[pl.BlockSpec(), pl.BlockSpec(), pl.BlockSpec(memory_space=pl.ANY)],
        out_shape=pltpu.HBM((2 * ys, q.shape[0] + TAIL, 2 * HEAD_DIM), BF),
        name="pack_queries",
    )(q, f_t, after)


def attend_kernel(info, *refs, steps, z_count, first, last, tiles, rows):
    blocks, own = len(steps), 0 in steps
    q_ref = refs[0]
    kv_refs = refs[1 : 1 + blocks]
    at = 1 + blocks
    if not first:
        acc_in, stat_in = refs[at], refs[at + 1]
        at += 2
    if last:
        (o_out,) = refs[at : at + 1]
    else:
        acc_out, stat_out = refs[at : at + 2]
    first_tail = q_ref[0, rows:, :].astype(F32)
    keys, values, biases = [], [], []
    ones = jnp.ones((rows, HEAD_DIM), BF)
    for b, s in enumerate(steps):
        valid = info[1] >= s if s >= 0 else info[1] - s >= z_count
        for c in range(2):
            keys.append(kv_refs[b].at[c, pl.ds(0, rows), pl.ds(0, HEAD_DIM)])
            values.append(kv_refs[b].at[c, pl.ds(0, rows), pl.ds(HEAD_DIM, HEAD_DIM)])
            tail = kv_refs[b][c, rows:, :].astype(F32)
            pair = []
            for j in range(2):
                bias = (row_of(first_tail, j)[:, :1] - row_of(tail, j)) * LOG2E
                pair.append(jnp.where(valid, bias, -jnp.inf))
            biases.append(pair)

    def score_tiles(i):
        both = jnp.concatenate(
            [q_ref[i, pl.ds(0, rows), pl.ds(j * HEAD_DIM, HEAD_DIM)] for j in range(2)], axis=0
        )
        found = [[], []]
        for u in range(2 * blocks):
            raw = lax.dot_general(
                both, keys[u][...], (((1,), (1,)), ((), ())), preferred_element_type=F32
            )
            for j in range(2):
                score = raw[j * rows : (j + 1) * rows] * SCORE2 + biases[u][j]
                if own and u < 2:
                    q_pos = i * rows + lax.broadcasted_iota(
                        jnp.int32, (rows, rows), 0
                    )
                    k_pos = info[0] + u * rows + lax.broadcasted_iota(jnp.int32, (rows, rows), 1)
                    score = jnp.where(q_pos >= k_pos, score, -jnp.inf)
                found[j].append(score)
        return found

    def absorb(i, scores):
        maxes, olds = [], []
        for j in range(2):
            top = scores[j][0]
            for score in scores[j][1:]:
                top = jnp.maximum(top, score)
            row_max = jnp.max(top, axis=1, keepdims=True)
            cols = pl.ds(j * HEAD_DIM, HEAD_DIM)
            old_max = jnp.full((rows, HEAD_DIM), LOW, F32) if first else stat_in[i, :, cols]
            olds.append(old_max)
            maxes.append(jnp.maximum(row_max, old_max))
        total = None
        wide = rows // HEAD_DIM
        for u in range(2 * blocks):
            weights = jnp.concatenate(
                [
                    jnp.exp2(scores[j][u] - jnp.concatenate([maxes[j]] * wide, axis=1)).astype(BF)
                    for j in range(2)
                ],
                axis=0,
            )
            value = jnp.concatenate([values[u][...], ones], axis=1)
            part = jnp.dot(weights, value, preferred_element_type=F32)
            total = part if total is None else total + part
        lse_rows = []
        for j in range(2):
            cols = pl.ds(j * HEAD_DIM, HEAD_DIM)
            weighted = total[j * rows : (j + 1) * rows, :HEAD_DIM]
            row_sum = total[j * rows : (j + 1) * rows, HEAD_DIM:]
            if not first:
                factor = jnp.exp2(olds[j] - maxes[j])
                sums = pl.ds((2 + j) * HEAD_DIM, HEAD_DIM)
                weighted = weighted + acc_in[i, :, cols] * factor
                row_sum = row_sum + acc_in[i, :, sums] * factor
            if last:
                some = row_sum > 0.0
                row_sum = jnp.where(some, row_sum, 1.0)
                mixed = weighted * (1.0 / row_sum)
                per = rows // 4
                for p in range(4):
                    o_out[4 * i + p, pl.ds(0, per), cols] = mixed[p * per : (p + 1) * per].astype(BF)
                lse = jnp.where(some, maxes[j] + jnp.log2(row_sum), LOW)
                flat = []
                eye = lax.broadcasted_iota(jnp.int32, (HEAD_DIM, HEAD_DIM), 0) == (
                    lax.broadcasted_iota(jnp.int32, (HEAD_DIM, HEAD_DIM), 1)
                )
                for at in range(0, rows, HEAD_DIM):
                    flat.append(
                        jnp.sum(jnp.where(eye, lse[at : at + HEAD_DIM], 0.0), axis=0, keepdims=True)
                    )
                lse_rows.append(jnp.concatenate(flat, axis=1))
            else:
                acc_out[i, :, cols] = weighted
                acc_out[i, :, pl.ds((2 + j) * HEAD_DIM, HEAD_DIM)] = row_sum
                stat_out[i, :, cols] = maxes[j]
        if last:
            tail = tail_block(lse_rows, rows)
            for p in range(4):
                o_out[4 * i + p, pl.ds(rows // 4, TAIL), :] = tail

    def some_tiles(step, _):
        pending = score_tiles(step * tiles)
        for n in range(tiles):
            i = step * tiles + n
            following = score_tiles(i + 1) if n + 1 < tiles else None
            absorb(i, pending)
            pending = following
        return 0

    lax.fori_loop(0, q_ref.shape[0] // tiles, some_tiles, 0)


def attend(info, q_all, kvs, steps, z_count, state, last, tiles=4):
    count, padded, width = q_all.shape
    rows = padded - TAIL
    first = state is None
    blocks = len(kvs)
    vmem = pl.BlockSpec(memory_space=pltpu.VMEM)
    operands = [q_all, *kvs]
    aliases = {}
    if not first:
        operands += list(state)
        if not last:
            aliases = {len(operands) - 1: 0, len(operands): 1}
    if last:
        out_shape = jax.ShapeDtypeStruct((4 * count, rows // 4 + TAIL, width), BF)
    else:
        out_shape = [
            jax.ShapeDtypeStruct((count, rows, 2 * width), F32),
            jax.ShapeDtypeStruct((count, rows, width), F32),
        ]
    scores = count * rows * 2 * blocks * 2 * rows
    return pl.pallas_call(
        functools.partial(
            attend_kernel, steps=steps, z_count=z_count, first=first, last=last, tiles=tiles, rows=rows
        ),
        in_specs=[pl.BlockSpec(memory_space=pltpu.SMEM)] + [vmem] * len(operands),
        out_specs=vmem if last else [vmem, vmem],
        out_shape=out_shape,
        input_output_aliases=aliases,
        cost_estimate=pl.CostEstimate(
            flops=scores * 768, transcendentals=scores, bytes_accessed=6_000_000
        ),
        compiler_params=pltpu.CompilerParams(vmem_limit_bytes=24 * 1024 * 1024),
    )(info, *operands)


def post_kernel(info, part_ref, *refs, turns, count):
    w_refs = refs[:count]
    res_ref, gain_ref, ids_ref, stream_out, normed_out, send_out, att, weight, sems = refs[count:]
    sources = part_ref.shape[0]
    own_rows = res_ref.shape[0]
    width = part_ref.shape[2]
    tps = len(turns)
    groups = 2 * tps
    ys = sources // groups
    copies = []
    at = 0
    for n, w_ref in enumerate(w_refs):
        size = w_ref.shape[0]
        copies.append(pltpu.make_async_copy(w_ref, weight.at[pl.ds(at, size)], sems.at[n]))
        copies[-1].start()
        at += size

    pick = lax.broadcasted_iota(jnp.int32, (own_rows, width), 1) == (
        info[2] * own_rows + lax.broadcasted_iota(jnp.int32, (own_rows, width), 0)
    )
    for s, turn in enumerate(turns):
        tp = (info[2] + turn) % tps
        for k in range(2):
            core = k if turn == 0 else info[3] ^ k
            col = (2 * s + k) * width
            index = core * tps + tp
            tails = [part_ref[y * groups + index, own_rows:, :].astype(F32) for y in range(ys)]
            for j in range(2):
                sums = []
                for y in range(ys):
                    row = row_of(tails[y], j)
                    sums.append(jnp.sum(jnp.where(pick, row, 0.0), axis=1, keepdims=True))
                top = sums[0]
                for one in sums[1:]:
                    top = jnp.maximum(top, one)
                weights = [jnp.exp2(one - top) for one in sums]
                total = weights[0]
                for w in weights[1:]:
                    total = total + w
                inverse = 1.0 / total
                mixed = None
                for y in range(ys):
                    part = part_ref[
                        y * groups + index, pl.ds(0, own_rows), pl.ds(j * HEAD_DIM, HEAD_DIM)
                    ].astype(F32) * (weights[y] * inverse)
                    mixed = part if mixed is None else mixed + part
                att[:, pl.ds(col + j * HEAD_DIM, HEAD_DIM)] = mixed.astype(BF)

    experts = send_out.shape[0]
    cap = send_out.shape[1]
    expert = lax.broadcasted_iota(jnp.int32, (experts, own_rows), 0)
    named = jnp.zeros((experts, own_rows), F32)
    for k in range(TOPK):
        named = jnp.where(ids_ref[k : k + 1, :] == expert, 1.0, named)
    earlier = (
        lax.broadcasted_iota(jnp.int32, (own_rows, own_rows), 0)
        < lax.broadcasted_iota(jnp.int32, (own_rows, own_rows), 1)
    ).astype(BF)
    rank = jnp.dot(named.astype(BF), earlier, preferred_element_type=F32)
    rank = jnp.where(named > 0.5, rank, -1.0)
    slot = lax.broadcasted_iota(jnp.int32, (experts, cap, own_rows), 1).astype(F32)
    chosen = (rank[:, None, :] == slot).astype(F32).reshape(experts * cap, own_rows).astype(BF)

    for copy in copies:
        copy.wait()
    block = 256
    squares = jnp.zeros((own_rows, 1), F32)
    for n in range(0, weight.shape[1], block):
        branch = jnp.dot(att[...], weight[:, n : n + block], preferred_element_type=F32)
        stream = (res_ref[:, n : n + block].astype(F32) + branch).astype(BF)
        stream_out[:, n : n + block] = stream
        wide = stream.astype(F32)
        squares = squares + jnp.sum(wide * wide, axis=1, keepdims=True)
    scale = lax.rsqrt(squares / weight.shape[1] + NORM_EPS)
    for n in range(0, weight.shape[1], 2 * block):
        cols = slice(n, n + 2 * block)
        normed = (stream_out[:, cols].astype(F32) * scale * gain_ref[:, cols]).astype(BF)
        normed_out[:, cols] = normed
        sent = jnp.dot(chosen, normed, preferred_element_type=F32).astype(BF)
        send_out[:, :, cols] = sent.reshape(experts, cap, 2 * block)


def post(info, parts, weights, turns, residual, gain, ids_t, experts, cap):
    rows, width = residual.shape
    vmem = pl.BlockSpec(memory_space=pltpu.VMEM)
    return pl.pallas_call(
        functools.partial(post_kernel, turns=turns, count=len(weights)),
        in_specs=[pl.BlockSpec(memory_space=pltpu.SMEM), vmem]
        + [pl.BlockSpec(memory_space=pltpu.HBM)] * len(weights)
        + [vmem] * 3,
        out_specs=[vmem] * 3,
        scratch_shapes=[
            pltpu.VMEM((rows, width), BF),
            pltpu.VMEM((width, width), BF),
            pltpu.SemaphoreType.DMA((len(weights),)),
        ],
        out_shape=[
            jax.ShapeDtypeStruct((rows, width), BF),
            jax.ShapeDtypeStruct((rows, width), BF),
            jax.ShapeDtypeStruct((experts, cap, width), BF),
        ],
        compiler_params=pltpu.CompilerParams(vmem_limit_bytes=40 * 1024 * 1024),
        name="post",
    )(info, parts, *weights, residual, gain, ids_t)


def expert_kernel(x_ref, gate_ref, up_ref, down_ref, out_ref):
    peers, cap, width = x_ref.shape
    x = x_ref[...].reshape(peers * cap, width)
    gate = jnp.dot(x, gate_ref[0], preferred_element_type=F32)
    up = jnp.dot(x, up_ref[0], preferred_element_type=F32)
    hidden = (gate / (1.0 + jnp.exp(-gate)) * up).astype(BF)
    out = jnp.dot(hidden, down_ref[0], preferred_element_type=F32).astype(BF)
    out_ref[...] = out.reshape(peers, cap, width)


def expert(arrived, gate, up, down, steps=4):
    peers, cap, width = arrived.shape
    rows = pl.BlockSpec((peers // steps, cap, width), lambda g: (g, 0, 0))
    whole = lambda g: (0, 0, 0)
    return pl.pallas_call(
        expert_kernel,
        grid=(steps,),
        in_specs=[
            rows,
            pl.BlockSpec(gate.shape, whole),
            pl.BlockSpec(up.shape, whole),
            pl.BlockSpec(down.shape, whole),
        ],
        out_specs=rows,
        out_shape=pltpu.HBM(arrived.shape, BF),
        compiler_params=pltpu.CompilerParams(
            dimension_semantics=("arbitrary",), vmem_limit_bytes=40 * 1024 * 1024
        ),
        name="expert",
    )(arrived, gate, up, down)


def finish_kernel(res_ref, base_ref, ids_ref, route_ref, out_ref, mix):
    rows = base_ref.shape[0]
    experts, cap, block = res_ref.shape
    slots = experts * cap

    @pl.when(pl.program_id(0) == 0)
    def _():
        route = route_ref[...]
        gates = route / jnp.sum(route, axis=1, keepdims=True) * ROUTED_SCALE
        expert = lax.broadcasted_iota(jnp.int32, (rows, experts), 1)
        named = jnp.zeros((rows, experts), F32)
        gate = jnp.zeros((rows, experts), F32)
        for k in range(TOPK):
            here = ids_ref[:, k : k + 1] == expert
            named = jnp.where(here, 1.0, named)
            gate = jnp.where(here, gates[:, k : k + 1], gate)
        earlier = (
            lax.broadcasted_iota(jnp.int32, (rows, rows), 1)
            < lax.broadcasted_iota(jnp.int32, (rows, rows), 0)
        ).astype(BF)
        rank = jnp.dot(earlier, named.astype(BF), preferred_element_type=F32)
        rank = jnp.where(named > 0.5, rank, 128.0)
        high = gate.astype(BF)
        low = (gate - high.astype(F32)).astype(BF)
        slot = lax.broadcasted_iota(jnp.int32, (experts, slots), 1)
        first = lax.broadcasted_iota(jnp.int32, (experts, slots), 0) * cap
        spread = ((slot >= first) & (slot < first + cap)).astype(BF)
        stacked = jnp.concatenate([rank.astype(BF), high, low], axis=0)
        wide = jnp.dot(stacked, spread, preferred_element_type=F32)
        place = (lax.broadcasted_iota(jnp.int32, (rows, slots), 1) % cap).astype(F32)
        chosen = wide[:rows] == place
        mix[:rows] = jnp.where(chosen, wide[rows : 2 * rows], 0.0).astype(BF)
        mix[rows:] = jnp.where(chosen, wide[2 * rows :], 0.0).astype(BF)

    results = res_ref[...].reshape(slots, block)
    routed = jnp.dot(mix[...], results, preferred_element_type=F32)
    out_ref[...] = (base_ref[...] + routed[:rows] + routed[rows:]).astype(BF)


def finish(results, base, ids, route):
    experts, cap, width = results.shape
    rows = base.shape[0]
    block = 512
    tiled = pl.BlockSpec((rows, block), lambda g: (0, g))
    fixed = pl.BlockSpec(ids.shape, lambda g: (0, 0))
    return pl.pallas_call(
        finish_kernel,
        grid=(width // block,),
        in_specs=[
            pl.BlockSpec((experts, cap, block), lambda g: (0, 0, g)),
            tiled,
            fixed,
            fixed,
        ],
        out_specs=tiled,
        scratch_shapes=[pltpu.VMEM((2 * rows, experts * cap), BF)],
        out_shape=jax.ShapeDtypeStruct(base.shape, BF),
        compiler_params=pltpu.CompilerParams(dimension_semantics=("arbitrary",)),
        name="finish",
    )(results, base, ids, route)


def local(
    residual,
    queries,
    key_rows,
    value_rows,
    forget_sums,
    out_weight,
    norm_gain,
    expert_ids,
    route_weights,
    expert_gate,
    expert_up,
    expert_down,
    shared_gate,
    shared_up,
    shared_down,
):
    z_count = lax.axis_size("z")
    y_count = lax.axis_size("y")
    z = lax.axis_index("z")
    y = lax.axis_index("y")
    rows = queries.shape[0]
    experts = z_count * y_count * 2
    cap = 2 * residual.shape[0] * TOPK // experts

    tps = lax.axis_size("tp")
    f_t = forget_sums.T
    kv_send = pack_keys(key_rows, value_rows, f_t)
    own = lax.all_to_all(kv_send, "c", split_axis=0, concat_axis=0)
    up_ring = [(i, (i + 1) % z_count) for i in range(z_count)]
    down_ring = [(i, (i - 1) % z_count) for i in range(z_count)]
    q_send = pack_queries(queries, f_t, own, y_count)
    q_all = lax.all_to_all(q_send, ("y", "c"), split_axis=0, concat_axis=0)
    core = lax.axis_index("c")
    half_rows = out_weight.shape[0] // 2
    mine = lax.dynamic_slice_in_dim(out_weight, core * half_rows, half_rows, 0)
    next_tp = [(i, (i + 1) % tps) for i in range(tps)]
    last_tp = [(i, (i - 1) % tps) for i in range(tps)]
    w_up = lax.ppermute(mine, "tp", next_tp)
    w_down = lax.ppermute(mine, "tp", last_tp)

    def swap(x):
        return lax.ppermute(x, "c", [(0, 1), (1, 0)])

    def up(block):
        return lax.ppermute(block, "z", up_ring)

    def down(block):
        return lax.ppermute(block, "z", down_ring)

    info = jnp.stack([2 * y * rows, z, lax.axis_index("tp"), core]).astype(jnp.int32)
    up1, down1 = up(own), down(own)
    up2, down2 = up(up1), down(down1)
    up3, down3 = up(up2), down(down2)
    state = attend(info, q_all, [own, up1, down1], (0, 1, -1), z_count, None, False)
    state, up3, down3, w_up = lax.optimization_barrier((state, up3, down3, w_up))
    up4 = up(up3)
    w_far = lax.ppermute(w_up, "tp", next_tp)
    state = attend(info, q_all, [up2, down2], (2, -2), z_count, state, False)
    state, w_down = lax.optimization_barrier((state, w_down))
    w_up2, w_down2 = swap(w_up), swap(w_down)
    sent = attend(info, q_all, [up3, down3, up4], (3, -3, 4), z_count, state, True)
    sent, w_far = lax.optimization_barrier((sent, w_far))
    w_far2 = swap(w_far)
    parts = lax.all_to_all(sent, ("y", "c", "tp"), split_axis=0, concat_axis=0)
    weights = [out_weight, w_up, w_up2, w_down, w_down2, w_far, w_far2]
    stream, normed, outgoing = post(
        info,
        parts,
        weights,
        (0, tps - 1, 1, 2),
        residual,
        norm_gain[None, :],
        expert_ids.T,
        experts,
        cap,
    )
    arrived = lax.all_to_all(outgoing, ("z", "y", "c"), split_axis=0, concat_axis=0)
    shared_hidden = (
        jax.nn.silu(jnp.dot(normed, shared_gate, preferred_element_type=F32))
        * jnp.dot(normed, shared_up, preferred_element_type=F32)
    ).astype(BF)
    base = stream.astype(F32) + jnp.dot(shared_hidden, shared_down, preferred_element_type=F32)
    processed = expert(arrived, expert_gate, expert_up, expert_down)
    returned = lax.all_to_all(
        processed, ("z", "y", "c"), split_axis=0, concat_axis=0
    )
    return finish(returned, base, expert_ids, route_weights)


def solution(mesh):
    sp = mesh.shape["sp"]
    tp = mesh.shape["tp"]
    grid = Mesh(mesh.devices.reshape(8, sp // 16, 2, tp), ("z", "y", "c", "tp"))
    seq = ("z", "y", "c")
    in_specs = (
        P((*seq, "tp"), None),
        P(seq, "tp"),
        P(seq, "tp"),
        P(seq, "tp"),
        P(seq, "tp"),
        P("tp", None),
        P(),
        P((*seq, "tp"), None),
        P((*seq, "tp"), None),
        P(seq, None, None),
        P(seq, None, None),
        P(seq, None, None),
        P(),
        P(),
        P(),
    )
    out_specs = P((*seq, "tp"), None)

    return jax.shard_map(local, mesh=grid, in_specs=in_specs, out_specs=out_specs, check_vma=False)
```

time: 250 us -> 238 us (0.952)
  between operations: 13.6 us -> 0.16 us
  local copies, waits for them, and re-layouts: 8.4 us -> 13.1 us
  Pallas kernels: 49.5 us -> 45.2 us
  starting transfers between devices: 30.8 us -> 34.3 us
  waiting for transfers between devices: 76.9 us -> 74.2 us
    ppermute x1 -> x6, waiting for transfers between devices: 0.01 us -> 7.62 us  [the longest x1 3.87 us: local(): w_far = lax.ppermute(w_up, 'tp', next_tp)]
    all_to_all x1, waiting for transfers between devices: 17.5 us -> 10.2 us  [local(): parts = lax.all_to_all(sent, ('y', 'c', 'tp'), split_axis=0, concat_axis=0)]
    pallas_call x6 -> x7, Pallas kernels: 45.1 us -> 39.9 us  [the longest x3 26.7 us: attend(): pl.pallas_call(functools.partial(attend_kernel, steps=steps, z_count=z_co...]
    ppermute x1 -> x6, starting transfers between devices: 0.01 us -> 4.81 us  [the longest x1 1.75 us: local(): w_down = lax.ppermute(mine, 'tp', last_tp)]
    unnamed x28 -> x36, local copies, waits for them, and re-layouts: 7.3 us -> 10.7 us
  transfers between devices with their start and end apart: 12 -> 16, of which waited for: 4 -> 7; matrix products, arithmetic and copies ran while one was open for 2% -> 4% of each run, Pallas kernels for 13% -> 11%
where the time goes in v3:
time: 238 us; the launch traced here: 237 us
  waiting for transfers between devices  74.2 us (31%)
  blocking collectives  65.1 us (27%)
  Pallas kernels  45.2 us (19%)
  starting transfers between devices  34.3 us (14%)
  local copies, waits for them, and re-layouts  13.1 us (6%)
  matrix products  4.78 us (2%)
    all_to_all x1, blocking collectives, local(): lax.all_to_all(outgoing, ('z', 'y', 'c'), split_axis=0, concat_axis=0)  59.3 us
    all_to_all x1, waiting for transfers between devices, local(): lax.all_to_all(processed, ('z', 'y', 'c'), split_axis=0, concat_axis=0)  44.9 us
    pallas_call x3, Pallas kernels, attend(): pl.pallas_call(functools.partial(attend_kernel, steps=steps, z_count=z_co...  26.7 us
    ppermute x4, waiting for transfers between devices, up(): return lax.ppermute(block, 'z', up_ring)  11.4 us
    unnamed x36, local copies, waits for them, and re-layouts  10.7 us
    ppermute x3, starting transfers between devices, down(): return lax.ppermute(block, 'z', down_ring)  10.4 us
    all_to_all x1, waiting for transfers between devices, local(): parts = lax.all_to_all(sent, ('y', 'c', 'tp'), split_axis=0, concat_axis=0)  10.2 us
    all_to_all x1, starting transfers between devices, local(): parts = lax.all_to_all(sent, ('y', 'c', 'tp'), split_axis=0, concat_axis=0)  5.82 us
  transfers between devices with their start and end apart: 16, of which 7 were waited for; matrix products, arithmetic and copies ran while one was open for 4% of the time, Pallas kernels for 11%

profile of v3, /device:TPU:8, one launch (start us, length us, event | category | flops | bytes accessed | tf_op | source)
XLA Modules:
  0.0 236.8 jit_solution(13707674387118695179)
XLA Ops:
  0.0 0.0 copy-start
  0.0 1.9 pack_keys.1
  1.9 5.8 %all_to_all.25._.refs_1_ = bf16[2,264,256]{2,1,0:T(8,128)(2,1)} all-to-all(bf16[2,264,256]{2,1,0:T(8,128)(2,1)} %pack_keys.1), channel_id=1, replica_groups=mesh['z'=8,'y'=4,'c'=2,'tp'=4] {'c'}, dimensions={0} | all-to-all | bytes 540672 | tf_op jit(solution)/shard_map/all_to_all | solution.py:459
  7.6 2.0 pack_queries.1
  9.7 5.6 %all-to-all-start.1 = ((bf16[8,264,256]{2,1,0:T(8,128)(2,1)}), bf16[8,264,256]{2,1,0:T(8,128)(2,1)S(1)}, u32[]{:S(2)}, u32[]{:S(2)}) async-start(bf16[8,264,256]{2,1,0:T(8,128)(2,1)} %pack_queries.1), calls=%async_computation.1 | async-start | bytes 2162688 | tf_op jit(solution)/shard_map/all_to_all | solution.py:463
  15.3 2.4 constant_dynamic-slice_fusion
  17.6 0.8 collective-permute-start.6
  18.4 0.0 copy-done.6
  18.4 1.9 collective-permute-start
  20.3 3.9 %collective-permute-start.1 = (bf16[2,264,256]{2,1,0:T(8,128)(2,1)S(1)}, bf16[2,264,256]{2,1,0:T(8,128)(2,1)}, u32[]{:S(2)}, u32[]{:S(2)}) collective-permute-start(bf16[2,264,256]{2,1,0:T(8,128)(2,1)S(1)} %copy-done.6), channel_id=1, source_target_pairs={{0,224},{32,0},{64,32},{96,64},{128,96},{160,128},{192,160},{224,1... | collective-permute-start | bytes 811016 | tf_op jit(solution)/shard_map/ppermute | solution.py:479
  24.3 6.6 %collective-permute-done.refs_2_ = bf16[2,264,256]{2,1,0:T(8,128)(2,1)} collective-permute-done((bf16[2,264,256]{2,1,0:T(8,128)(2,1)S(1)}, bf16[2,264,256]{2,1,0:T(8,128)(2,1)}, u32[]{:S(2)}, u32[]{:S(2)}) %collective-permute-start) | collective-permute-done | bytes 270368 | tf_op jit(solution)/shard_map/ppermute | solution.py:476
  30.9 0.0 collective-permute-start.2
  30.9 0.0 collective-permute-done.1.refs_3_
  30.9 3.2 %collective-permute-start.4 = (bf16[2,264,256]{2,1,0:T(8,128)(2,1)}, bf16[2,264,256]{2,1,0:T(8,128)(2,1)S(1)}, u32[]{:S(2)}, u32[]{:S(2)}) collective-permute-start(bf16[2,264,256]{2,1,0:T(8,128)(2,1)} %collective-permute-done.1.refs_3_), channel_id=1, source_target_pairs={{0,224},{32,0},{64,32},{96,64},{128,96},{160,128},{192,160},{224,1... | collective-permute-start | bytes 811016 | tf_op jit(solution)/shard_map/ppermute | solution.py:479
  34.1 1.7 collective-permute-start.8
  35.9 0.1 pad_add_fusion.info
  35.9 4.0 %collective-permute-done.2.refs_1_ = bf16[2,264,256]{2,1,0:T(8,128)(2,1)S(1)} collective-permute-done((bf16[2,264,256]{2,1,0:T(8,128)(2,1)}, bf16[2,264,256]{2,1,0:T(8,128)(2,1)S(1)}, u32[]{:S(2)}, u32[]{:S(2)}) %collective-permute-start.2) | collective-permute-done | bytes 270368 | tf_op jit(solution)/shard_map/ppermute | solution.py:476
  39.9 0.0 collective-permute-start.3
  39.9 0.0 collective-permute-done.4.refs_2_
  39.9 3.2 %collective-permute-start.5 = (bf16[2,264,256]{2,1,0:T(8,128)(2,1)S(1)}, bf16[2,264,256]{2,1,0:T(8,128)(2,1)}, u32[]{:S(2)}, u32[]{:S(2)}) collective-permute-start(bf16[2,264,256]{2,1,0:T(8,128)(2,1)S(1)} %collective-permute-done.4.refs_2_), channel_id=1, source_target_pairs={{0,224},{32,0},{64,32},{96,64},{128,96},{160,128},{192,160},{224,1... | collective-permute-start | bytes 811016 | tf_op jit(solution)/shard_map/ppermute | solution.py:479
  43.2 0.0 all-to-all-done.1.refs_0_
  43.2 9.5 %shard_map.145 = (f32[8,256,512]{2,1,0:T(8,128)S(1)}, f32[8,256,256]{2,1,0:T(8,128)S(1)}) custom-call(s32[4]{0:T(128)S(1)} %pad_add_fusion.info, bf16[8,264,256]{2,1,0:T(8,128)(2,1)S(1)} %all-to-all-done.1.refs_0_, bf16[2,264,256]{2,1,0:T(8,128)(2,1)S(1)} %copy-done.6, bf16[2,264,256]{2,1,0:T(8,128)(2,1)} %collective-permute-done.refs_2_, ...), custom_call_target="tpu_custom_call" | custom-call | flops 4831838208 | bytes 6000000 | tf_op jit(solution)/shard_map/pallas_call | solution.py:216
  52.7 0.0 collective-permute-done.3.refs_1_
  52.7 0.0 collective-permute-done.5.refs_2_
  52.7 0.0 collective-permute-done.6.refs_1_
  52.7 1.6 collective-permute-start.9
  54.3 0.0 collective-permute-start.7
  54.3 7.0 %shard_map.146 = (f32[8,256,512]{2,1,0:T(8,128)S(1)}, f32[8,256,256]{2,1,0:T(8,128)S(1)}) custom-call(s32[4]{0:T(128)S(1)} %pad_add_fusion.info, bf16[8,264,256]{2,1,0:T(8,128)(2,1)S(1)} %all-to-all-done.1.refs_0_, bf16[2,264,256]{2,1,0:T(8,128)(2,1)S(1)} %collective-permute-done.2.refs_1_, ...), custom_call_target="tpu_custom_call", output_to_operand_aliasing={{0}: (4, {}), {1}: (5, {})} | custom-call | flops 3221225472 | bytes 6000000 | tf_op jit(solution)/shard_map/pallas_call | solution.py:216
  61.3 0.0 collective-permute-done.8.refs_3_
  61.3 0.8 collective-permute-done.7.refs_3_
  62.1 10.2 %shard_map.147 = bf16[32,72,256]{2,1,0:T(8,128)(2,1)S(1)} custom-call(s32[4]{0:T(128)S(1)} %pad_add_fusion.info, bf16[8,264,256]{2,1,0:T(8,128)(2,1)S(1)} %all-to-all-done.1.refs_0_, bf16[2,264,256]{2,1,0:T(8,128)(2,1)} %collective-permute-done.3.refs_1_, bf16[2,264,256]{2,1,0:T(8,128)(2,1)} %collective-permute-done.5.refs_2_, ...), custom_call_target="tpu_custom_call" | custom-call | flops 4831838208 | bytes 6000000 | tf_op jit(solution)/shard_map/pallas_call | solution.py:216
  72.4 0.0 copy-start.5
  72.4 1.0 copy-done.5
  73.4 3.9 %collective-permute-done.9.refs_5_ = bf16[256,2048]{1,0:T(8,128)(2,1)} collective-permute-done((bf16[256,2048]{1,0:T(8,128)(2,1)}, bf16[256,2048]{1,0:T(8,128)(2,1)}, u32[]{:S(2)}, u32[]{:S(2)}) %collective-permute-start.9) | collective-permute-done | bytes 1048608 | tf_op jit(solution)/shard_map/ppermute | solution.py:488
  77.3 5.8 %all-to-all-start.2 = ((bf16[32,72,256]{2,1,0:T(8,128)(2,1)}), bf16[32,72,256]{2,1,0:T(8,128)(2,1)S(1)}, u32[]{:S(2)}, u32[]{:S(2)}) async-start(bf16[32,72,256]{2,1,0:T(8,128)(2,1)} %copy-done.5), calls=%async_computation.2 | async-start | bytes 2359296 | tf_op jit(solution)/shard_map/all_to_all | solution.py:495
  83.1 0.2 collective-permute-start.10
  83.3 0.4 collective-permute-start.11
  83.7 0.1 collective-permute-start.12
  83.8 3.7 %collective-permute-done.11.refs_4_ = bf16[256,2048]{1,0:T(8,128)(2,1)S(1)} collective-permute-done((bf16[256,2048]{1,0:T(8,128)(2,1)}, bf16[256,2048]{1,0:T(8,128)(2,1)S(1)}, u32[]{:S(2)}, u32[]{:S(2)}) %collective-permute-start.11) | collective-permute-done | bytes 1048608 | tf_op jit(solution)/shard_map/ppermute | solution.py:473
  87.6 1.0 copy-done.9
  88.6 0.0 collective-permute-done.10.refs_2_
  88.6 1.0 copy-done.7
  89.5 0.0 collective-permute-done.12.refs_6_
  89.5 1.0 copy-done.11
  90.5 10.2 %all-to-all-done.2.part_ref = bf16[32,72,256]{2,1,0:T(8,128)(2,1)S(1)} async-done(((bf16[32,72,256]{2,1,0:T(8,128)(2,1)}), bf16[32,72,256]{2,1,0:T(8,128)(2,1)S(1)}, u32[]{:S(2)}, u32[]{:S(2)}) %all-to-all-start.2) | async-done | bytes 1179680 | tf_op jit(solution)/shard_map/all_to_all | solution.py:495
  100.7 0.0 copy-start.1
  100.8 1.6 copy-done.1
  102.3 1.2 copy-done.8
  103.6 1.2 copy-done.10
  104.8 1.2 copy-done.12
  106.0 5.0 %post.1 = (bf16[64,2048]{1,0:T(8,128)(2,1)S(1)}, bf16[64,2048]{1,0:T(8,128)(2,1)S(1)}, bf16[64,8,2048]{2,1,0:T(8,128)(2,1)S(1)}) custom-call(s32[4]{0:T(128)S(1)} %pad_add_fusion.info, bf16[32,72,256]{2,1,0:T(8,128)(2,1)S(1)} %all-to-all-done.2.part_ref, bf16[512,2048]{1,0:T(8,128)(2,1)S(1)} %copy-done.1, bf16[256,2048]{1,0:T(8,128)(2,1)} %collective-permute-done.6.refs_1_, ...), custom_call_target="tpu_custom_call" | custom-call | tf_op jit(solution)/shard_map/post/pallas_call | solution.py:316
  111.0 0.0 copy-start.2
  111.0 0.0 copy-start.3
  111.1 59.3 %all_to_all.26.x_ref = bf16[64,8,2048]{2,1,0:T(8,128)(2,1)S(1)} all-to-all(bf16[64,8,2048]{2,1,0:T(8,128)(2,1)S(1)} %get-tuple-element.36), channel_id=1, replica_groups=mesh['z'=8,'y'=4,'c'=2,'tp'=4] {'z','y','c'}, dimensions={0} | all-to-all | bytes 4194304 | tf_op jit(solution)/shard_map/all_to_all | solution.py:508
  170.3 0.0 copy-done.3
  170.3 5.2 %expert.1 = bf16[64,8,2048]{2,1,0:T(8,128)(2,1)} custom-call(bf16[64,8,2048]{2,1,0:T(8,128)(2,1)S(1)} %all_to_all.26.x_ref, bf16[1,2048,384]{2,1,0:T(8,128)(2,1)S(1)} %copy-done.2, bf16[1,2048,384]{2,1,0:T(8,128)(2,1)S(1)} %copy-done.3, bf16[1,384,2048]{2,1,0:T(8,128)(2,1)S(1)} %copy-done.4), custom_call_target="tpu_custom_call" | custom-call | tf_op jit(solution)/shard_map/expert/pallas_call | solution.py:351
  175.6 5.8 %all-to-all-start.4 = ((bf16[64,8,2048]{2,1,0:T(8,128)(2,1)}), bf16[64,8,2048]{2,1,0:T(8,128)(2,1)}, u32[]{:S(2)}, u32[]{:S(2)}) async-start(bf16[64,8,2048]{2,1,0:T(8,128)(2,1)} %expert.1), calls=%async_computation.4 | async-start | bytes 4194304 | tf_op jit(solution)/shard_map/all_to_all | solution.py:515
  181.3 0.7 copy.18.ids_ref
  182.0 0.7 copy.19.route_ref
  182.8 1.8 fusion.5
  184.5 0.0 copy-done
  184.5 3.0 %convert_add_fusion.base_ref = f32[64,2048]{1,0:T(8,128)} fusion(bf16[64,2048]{1,0:T(8,128)(2,1)S(1)} %get-tuple-element.37, bf16[384,2048]{1,0:T(8,128)(2,1)S(1)} %copy-done, f32[64,384]{1,0:T(8,128)S(1)} %fusion.5, bf16[64,2048]{1,0:T(8,128)(2,1)S(1)} %get-tuple-element.38, bf16[2048,384]{1,0:T(8,128)(2,1)} %param.28), kind=kOutput, calls=%fused_computation | convolution fusion | flops 201736192 | bytes 4292608 | tf_op jit(solution)/shard_map/dot_general | solution.py:513
  187.6 44.9 %all-to-all-done.4.res_ref = bf16[64,8,2048]{2,1,0:T(8,128)(2,1)} async-done(((bf16[64,8,2048]{2,1,0:T(8,128)(2,1)}), bf16[64,8,2048]{2,1,0:T(8,128)(2,1)}, u32[]{:S(2)}, u32[]{:S(2)}) %all-to-all-start.4) | async-done | bytes 2097184 | tf_op jit(solution)/shard_map/all_to_all | solution.py:515
  232.5 4.4 %finish.1 = bf16[64,2048]{1,0:T(8,128)(2,1)} custom-call(bf16[64,8,2048]{2,1,0:T(8,128)(2,1)} %all-to-all-done.4.res_ref, f32[64,2048]{1,0:T(8,128)} %convert_add_fusion.base_ref, s32[64,4]{1,0:T(8,128)} %copy.18.ids_ref, f32[64,4]{1,0:T(8,128)} %copy.19.route_ref), custom_call_target="tpu_custom_call" | custom-call | tf_op jit(solution)/shard_map/finish/pallas_call | solution.py:414
  (18 shorter events, 0.0 us)
Async XLA Ops:
  0.0 184.5 %copy-start = (bf16[384,2048]{1,0:T(8,128)(2,1)S(1)}, bf16[384,2048]{1,0:T(8,128)(2,1)}, u32[]{:S(2)}) copy-start(bf16[384,2048]{1,0:T(8,128)(2,1)} %param.29) | copy-start | bytes 4718596
  9.7 33.5 %all-to-all-start.1 = ((bf16[8,264,256]{2,1,0:T(8,128)(2,1)}), bf16[8,264,256]{2,1,0:T(8,128)(2,1)S(1)}, u32[]{:S(2)}, u32[]{:S(2)}) async-start(bf16[8,264,256]{2,1,0:T(8,128)(2,1)} %pack_queries.1), calls=%async_computation.1 | async-start | bytes 2162688 | tf_op jit(solution)/shard_map/all_to_all | solution.py:463
  15.3 3.1 %copy-start.6 = (bf16[2,264,256]{2,1,0:T(8,128)(2,1)S(1)}, bf16[2,264,256]{2,1,0:T(8,128)(2,1)}, u32[]{:S(2)}) copy-start(bf16[2,264,256]{2,1,0:T(8,128)(2,1)} %all_to_all.25._.refs_1_) | copy-start | bytes 811012
  17.6 35.0 %collective-permute-start.6 = (bf16[256,2048]{1,0:T(8,128)(2,1)}, bf16[256,2048]{1,0:T(8,128)(2,1)}, u32[]{:S(2)}, u32[]{:S(2)}) collective-permute-start(bf16[256,2048]{1,0:T(8,128)(2,1)} %constant_dynamic-slice_fusion), channel_id=1, source_target_pairs={{0,1},{1,2},{2,3},{3,0},{4,5},{5,6},{6,7},{7,4},{8,9},{9,10},{10,1... | collective-permute-start | bytes 3145736 | tf_op jit(solution)/shard_map/ppermute | solution.py:469
  18.4 12.4 %collective-permute-start = (bf16[2,264,256]{2,1,0:T(8,128)(2,1)S(1)}, bf16[2,264,256]{2,1,0:T(8,128)(2,1)}, u32[]{:S(2)}, u32[]{:S(2)}) collective-permute-start(bf16[2,264,256]{2,1,0:T(8,128)(2,1)S(1)} %copy-done.6), channel_id=1, source_target_pairs={{0,32},{32,64},{64,96},{96,128},{128,160},{160,192},{192,224},{224... | collective-permute-start | bytes 811016 | tf_op jit(solution)/shard_map/ppermute | solution.py:476
  20.3 10.5 %collective-permute-start.1 = (bf16[2,264,256]{2,1,0:T(8,128)(2,1)S(1)}, bf16[2,264,256]{2,1,0:T(8,128)(2,1)}, u32[]{:S(2)}, u32[]{:S(2)}) collective-permute-start(bf16[2,264,256]{2,1,0:T(8,128)(2,1)S(1)} %copy-done.6), channel_id=1, source_target_pairs={{0,224},{32,0},{64,32},{96,64},{128,96},{160,128},{192,160},{224,1... | collective-permute-start | bytes 811016 | tf_op jit(solution)/shard_map/ppermute | solution.py:479
  30.9 9.1 %collective-permute-start.2 = (bf16[2,264,256]{2,1,0:T(8,128)(2,1)}, bf16[2,264,256]{2,1,0:T(8,128)(2,1)S(1)}, u32[]{:S(2)}, u32[]{:S(2)}) collective-permute-start(bf16[2,264,256]{2,1,0:T(8,128)(2,1)} %collective-permute-done.refs_2_), channel_id=1, source_target_pairs={{0,32},{32,64},{64,96},{96,128},{128,160},{160,192},{192,224},{224... | collective-permute-start | bytes 811016 | tf_op jit(solution)/shard_map/ppermute | solution.py:476
  30.9 9.1 %collective-permute-start.4 = (bf16[2,264,256]{2,1,0:T(8,128)(2,1)}, bf16[2,264,256]{2,1,0:T(8,128)(2,1)S(1)}, u32[]{:S(2)}, u32[]{:S(2)}) collective-permute-start(bf16[2,264,256]{2,1,0:T(8,128)(2,1)} %collective-permute-done.1.refs_3_), channel_id=1, source_target_pairs={{0,224},{32,0},{64,32},{96,64},{128,96},{160,128},{192,160},{224,1... | collective-permute-start | bytes 811016 | tf_op jit(solution)/shard_map/ppermute | solution.py:479
  34.1 27.2 %collective-permute-start.8 = (bf16[256,2048]{1,0:T(8,128)(2,1)}, bf16[256,2048]{1,0:T(8,128)(2,1)}, u32[]{:S(2)}, u32[]{:S(2)}) collective-permute-start(bf16[256,2048]{1,0:T(8,128)(2,1)} %constant_dynamic-slice_fusion), channel_id=1, source_target_pairs={{0,3},{1,0},{2,1},{3,2},{4,7},{5,4},{6,5},{7,6},{8,11},{9,8},{10,9... | collective-permute-start | bytes 3145736 | tf_op jit(solution)/shard_map/ppermute | solution.py:470
  39.9 12.7 %collective-permute-start.3 = (bf16[2,264,256]{2,1,0:T(8,128)(2,1)S(1)}, bf16[2,264,256]{2,1,0:T(8,128)(2,1)}, u32[]{:S(2)}, u32[]{:S(2)}) collective-permute-start(bf16[2,264,256]{2,1,0:T(8,128)(2,1)S(1)} %collective-permute-done.2.refs_1_), channel_id=1, source_target_pairs={{0,32},{32,64},{64,96},{96,128},{128,160},{160,192},{192,224},{224... | collective-permute-start | bytes 811016 | tf_op jit(solution)/shard_map/ppermute | solution.py:476
  39.9 12.7 %collective-permute-start.5 = (bf16[2,264,256]{2,1,0:T(8,128)(2,1)S(1)}, bf16[2,264,256]{2,1,0:T(8,128)(2,1)}, u32[]{:S(2)}, u32[]{:S(2)}) collective-permute-start(bf16[2,264,256]{2,1,0:T(8,128)(2,1)S(1)} %collective-permute-done.4.refs_2_), channel_id=1, source_target_pairs={{0,224},{32,0},{64,32},{96,64},{128,96},{160,128},{192,160},{224,1... | collective-permute-start | bytes 811016 | tf_op jit(solution)/shard_map/ppermute | solution.py:479
  52.7 24.6 %collective-permute-start.9 = (bf16[256,2048]{1,0:T(8,128)(2,1)}, bf16[256,2048]{1,0:T(8,128)(2,1)}, u32[]{:S(2)}, u32[]{:S(2)}) collective-permute-start(bf16[256,2048]{1,0:T(8,128)(2,1)} %collective-permute-done.6.refs_1_), channel_id=1, source_target_pairs={{0,1},{1,2},{2,3},{3,0},{4,5},{5,6},{6,7},{7,4},{8,9},{9,10},{10,1... | collective-permute-start | bytes 3145736 | tf_op jit(solution)/shard_map/ppermute | solution.py:488
  54.3 7.9 %collective-permute-start.7 = (bf16[2,264,256]{2,1,0:T(8,128)(2,1)}, bf16[2,264,256]{2,1,0:T(8,128)(2,1)S(1)}, u32[]{:S(2)}, u32[]{:S(2)}) collective-permute-start(bf16[2,264,256]{2,1,0:T(8,128)(2,1)} %collective-permute-done.3.refs_1_), channel_id=1, source_target_pairs={{0,32},{32,64},{64,96},{96,128},{128,160},{160,192},{192,224},{224... | collective-permute-start | bytes 811016 | tf_op jit(solution)/shard_map/ppermute | solution.py:476
  72.4 1.1 copy-start.5
  73.4 27.3 %copy-start.13 = (bf16[64,2048]{1,0:T(8,128)(2,1)S(1)}, bf16[64,2048]{1,0:T(8,128)(2,1)}, u32[]{:S(2)}) copy-start(bf16[64,2048]{1,0:T(8,128)(2,1)} %refs_7_.1) | copy-start | bytes 786436
  73.4 27.3 %copy-start.14 = (f32[2048]{0:T(1024)S(1)}, f32[2048]{0:T(1024)}, u32[]{:S(2)}) copy-start(f32[2048]{0:T(1024)} %param.21) | copy-start | bytes 24580
  73.4 27.3 %copy-start.15 = (s32[64,4]{0,1:T(4,128)S(1)}, s32[64,4]{0,1:T(4,128)}, u32[]{:S(2)}) copy-start(s32[64,4]{0,1:T(4,128)} %param.22) | copy-start | bytes 3076
  77.3 23.4 %all-to-all-start.2 = ((bf16[32,72,256]{2,1,0:T(8,128)(2,1)}), bf16[32,72,256]{2,1,0:T(8,128)(2,1)S(1)}, u32[]{:S(2)}, u32[]{:S(2)}) async-start(bf16[32,72,256]{2,1,0:T(8,128)(2,1)} %copy-done.5), calls=%async_computation.2 | async-start | bytes 2359296 | tf_op jit(solution)/shard_map/all_to_all | solution.py:495
  83.1 5.4 %collective-permute-start.10 = (bf16[256,2048]{1,0:T(8,128)(2,1)}, bf16[256,2048]{1,0:T(8,128)(2,1)S(1)}, u32[]{:S(2)}, u32[]{:S(2)}) collective-permute-start(bf16[256,2048]{1,0:T(8,128)(2,1)} %collective-permute-done.6.refs_1_), channel_id=1, source_target_pairs={{0,4},{4,0},{1,5},{5,1},{2,6},{6,2},{3,7},{7,3},{8,12},{12,8},{9,1... | collective-permute-start | bytes 3145736 | tf_op jit(solution)/shard_map/ppermute | solution.py:473
  83.3 4.3 %collective-permute-start.11 = (bf16[256,2048]{1,0:T(8,128)(2,1)}, bf16[256,2048]{1,0:T(8,128)(2,1)S(1)}, u32[]{:S(2)}, u32[]{:S(2)}) collective-permute-start(bf16[256,2048]{1,0:T(8,128)(2,1)} %collective-permute-done.8.refs_3_), channel_id=1, source_target_pairs={{0,4},{4,0},{1,5},{5,1},{2,6},{6,2},{3,7},{7,3},{8,12},{12,8},{9,1... | collective-permute-start | bytes 3145736 | tf_op jit(solution)/shard_map/ppermute | solution.py:473
  83.7 5.8 %collective-permute-start.12 = (bf16[256,2048]{1,0:T(8,128)(2,1)}, bf16[256,2048]{1,0:T(8,128)(2,1)S(1)}, u32[]{:S(2)}, u32[]{:S(2)}) collective-permute-start(bf16[256,2048]{1,0:T(8,128)(2,1)} %collective-permute-done.9.refs_5_), channel_id=1, source_target_pairs={{0,4},{4,0},{1,5},{5,1},{2,6},{6,2},{3,7},{7,3},{8,12},{12,8},{9,1... | collective-permute-start | bytes 3145736 | tf_op jit(solution)/shard_map/ppermute | solution.py:473
  87.6 1.0 copy-start.9
  88.6 1.0 copy-start.7
  89.5 1.0 copy-start.11
  100.7 1.6 copy-start.1
  102.3 1.2 copy-start.8
  103.6 1.2 copy-start.10
  104.8 1.2 copy-start.12
  106.0 64.3 %copy-start.4 = (bf16[1,384,2048]{2,1,0:T(8,128)(2,1)S(1)}, bf16[1,384,2048]{2,1,0:T(8,128)(2,1)}, u32[]{:S(2)}) copy-start(bf16[1,384,2048]{2,1,0:T(8,128)(2,1)} %down_ref.1) | copy-start | bytes 4718596
  111.0 59.3 %copy-start.2 = (bf16[1,2048,384]{2,1,0:T(8,128)(2,1)S(1)}, bf16[1,2048,384]{2,1,0:T(8,128)(2,1)}, u32[]{:S(2)}) copy-start(bf16[1,2048,384]{2,1,0:T(8,128)(2,1)} %gate_ref.1) | copy-start | bytes 4718596
  111.0 59.3 %copy-start.3 = (bf16[1,2048,384]{2,1,0:T(8,128)(2,1)S(1)}, bf16[1,2048,384]{2,1,0:T(8,128)(2,1)}, u32[]{:S(2)}) copy-start(bf16[1,2048,384]{2,1,0:T(8,128)(2,1)} %up_ref.1) | copy-start | bytes 4718596
  175.6 6.5 %copy-start.16 = (f32[64,4]{0,1:T(4,128)S(1)}, f32[64,4]{0,1:T(4,128)}, u32[]{:S(2)}) copy-start(f32[64,4]{0,1:T(4,128)} %param.23) | copy-start | bytes 3076
  175.6 56.9 %all-to-all-start.4 = ((bf16[64,8,2048]{2,1,0:T(8,128)(2,1)}), bf16[64,8,2048]{2,1,0:T(8,128)(2,1)}, u32[]{:S(2)}, u32[]{:S(2)}) async-start(bf16[64,8,2048]{2,1,0:T(8,128)(2,1)} %expert.1), calls=%async_computation.4 | async-start | bytes 4194304 | tf_op jit(solution)/shard_map/all_to_all | solution.py:515

commit v4 on v3

--- a/solution.py
+++ b/solution.py
@@ -228,13 +228,12 @@
     )(info, *operands)
 
 
-def post_kernel(info, part_ref, *refs, turns, count):
-    w_refs = refs[:count]
-    res_ref, gain_ref, ids_ref, stream_out, normed_out, send_out, att, weight, sems = refs[count:]
+def post_kernel(info, part_ref, *refs, tps):
+    w_refs = refs[:tps]
+    res_ref, gain_ref, ids_ref, stream_out, normed_out, send_out, att, weight, sems = refs[tps:]
     sources = part_ref.shape[0]
     own_rows = res_ref.shape[0]
     width = part_ref.shape[2]
-    tps = len(turns)
     groups = 2 * tps
     ys = sources // groups
     copies = []
@@ -248,11 +247,11 @@
     pick = lax.broadcasted_iota(jnp.int32, (own_rows, width), 1) == (
         info[2] * own_rows + lax.broadcasted_iota(jnp.int32, (own_rows, width), 0)
     )
-    for s, turn in enumerate(turns):
-        tp = (info[2] + turn) % tps
-        for k in range(2):
-            core = k if turn == 0 else info[3] ^ k
-            col = (2 * s + k) * width
+    near = 2 * info[3] - 1
+    for s, turn in enumerate((0, near, -near, 2)):
+        tp = (info[2] + turn + tps) % tps
+        for core in range(2):
+            col = (2 * s + core) * width
             index = core * tps + tp
             tails = [part_ref[y * groups + index, own_rows:, :].astype(F32) for y in range(ys)]
             for j in range(2):
@@ -310,11 +309,11 @@
         send_out[:, :, cols] = sent.reshape(experts, cap, 2 * block)
 
 
-def post(info, parts, weights, turns, residual, gain, ids_t, experts, cap):
+def post(info, parts, weights, residual, gain, ids_t, experts, cap):
     rows, width = residual.shape
     vmem = pl.BlockSpec(memory_space=pltpu.VMEM)
     return pl.pallas_call(
-        functools.partial(post_kernel, turns=turns, count=len(weights)),
+        functools.partial(post_kernel, tps=len(weights)),
         in_specs=[pl.BlockSpec(memory_space=pltpu.SMEM), vmem]
         + [pl.BlockSpec(memory_space=pltpu.HBM)] * len(weights)
         + [vmem] * 3,
@@ -329,7 +328,7 @@
             jax.ShapeDtypeStruct((rows, width), BF),
             jax.ShapeDtypeStruct((experts, cap, width), BF),
         ],
-        compiler_params=pltpu.CompilerParams(vmem_limit_bytes=40 * 1024 * 1024),
+        compiler_params=pltpu.CompilerParams(vmem_limit_bytes=56 * 1024 * 1024),
         name="post",
     )(info, parts, *weights, residual, gain, ids_t)
 
@@ -366,66 +365,72 @@
     )(arrived, gate, up, down)
 
 
-def finish_kernel(res_ref, base_ref, ids_ref, route_ref, out_ref, mix):
+def mix_kernel(ids_ref, route_ref, mix, *, cap):
+    rows = ids_ref.shape[0]
+    slots = mix.shape[1]
+    experts = slots // cap
+    route = route_ref[...]
+    gates = route / jnp.sum(route, axis=1, keepdims=True) * ROUTED_SCALE
+    expert = lax.broadcasted_iota(jnp.int32, (rows, experts), 1)
+    named = jnp.zeros((rows, experts), F32)
+    gate = jnp.zeros((rows, experts), F32)
+    for k in range(TOPK):
+        here = ids_ref[:, k : k + 1] == expert
+        named = jnp.where(here, 1.0, named)
+        gate = jnp.where(here, gates[:, k : k + 1], gate)
+    earlier = (
+        lax.broadcasted_iota(jnp.int32, (rows, rows), 1)
+        < lax.broadcasted_iota(jnp.int32, (rows, rows), 0)
+    ).astype(BF)
+    rank = jnp.dot(earlier, named.astype(BF), preferred_element_type=F32)
+    rank = jnp.where(named > 0.5, rank, 128.0)
+    high = gate.astype(BF)
+    low = (gate - high.astype(F32)).astype(BF)
+    slot = lax.broadcasted_iota(jnp.int32, (experts, slots), 1)
+    first = lax.broadcasted_iota(jnp.int32, (experts, slots), 0) * cap
+    spread = ((slot >= first) & (slot < first + cap)).astype(BF)
+    stacked = jnp.concatenate([rank.astype(BF), high, low], axis=0)
+    wide = jnp.dot(stacked, spread, preferred_element_type=F32)
+    place = (lax.broadcasted_iota(jnp.int32, (rows, slots), 1) % cap).astype(F32)
+    chosen = wide[:rows] == place
+    mix[:rows] = jnp.where(chosen, wide[rows : 2 * rows], 0.0).astype(BF)
+    mix[rows:] = jnp.where(chosen, wide[2 * rows :], 0.0).astype(BF)
+
+
+def mixing(ids, route, experts, cap):
+    return pl.pallas_call(
+        functools.partial(mix_kernel, cap=cap),
+        out_shape=jax.ShapeDtypeStruct((2 * ids.shape[0], experts * cap), BF),
+        name="mixing",
+    )(ids, route)
+
+
+def finish_kernel(res_ref, base_ref, mix_ref, out_ref):
     rows = base_ref.shape[0]
     experts, cap, block = res_ref.shape
-    slots = experts * cap
-
-    @pl.when(pl.program_id(0) == 0)
-    def _():
-        route = route_ref[...]
-        gates = route / jnp.sum(route, axis=1, keepdims=True) * ROUTED_SCALE
-        expert = lax.broadcasted_iota(jnp.int32, (rows, experts), 1)
-        named = jnp.zeros((rows, experts), F32)
-        gate = jnp.zeros((rows, experts), F32)
-        for k in range(TOPK):
-            here = ids_ref[:, k : k + 1] == expert
-            named = jnp.where(here, 1.0, named)
-            gate = jnp.where(here, gates[:, k : k + 1], gate)
-        earlier = (
-            lax.broadcasted_iota(jnp.int32, (rows, rows), 1)
-            < lax.broadcasted_iota(jnp.int32, (rows, rows), 0)
-        ).astype(BF)
-        rank = jnp.dot(earlier, named.astype(BF), preferred_element_type=F32)
-        rank = jnp.where(named > 0.5, rank, 128.0)
-        high = gate.astype(BF)
-        low = (gate - high.astype(F32)).astype(BF)
-        slot = lax.broadcasted_iota(jnp.int32, (experts, slots), 1)
-        first = lax.broadcasted_iota(jnp.int32, (experts, slots), 0) * cap
-        spread = ((slot >= first) & (slot < first + cap)).astype(BF)
-        stacked = jnp.concatenate([rank.astype(BF), high, low], axis=0)
-        wide = jnp.dot(stacked, spread, preferred_element_type=F32)
-        place = (lax.broadcasted_iota(jnp.int32, (rows, slots), 1) % cap).astype(F32)
-        chosen = wide[:rows] == place
-        mix[:rows] = jnp.where(chosen, wide[rows : 2 * rows], 0.0).astype(BF)
-        mix[rows:] = jnp.where(chosen, wide[2 * rows :], 0.0).astype(BF)
-
-    results = res_ref[...].reshape(slots, block)
-    routed = jnp.dot(mix[...], results, preferred_element_type=F32)
+    results = res_ref[...].reshape(experts * cap, block)
+    routed = jnp.dot(mix_ref[...], results, preferred_element_type=F32)
     out_ref[...] = (base_ref[...] + routed[:rows] + routed[rows:]).astype(BF)
 
 
-def finish(results, base, ids, route):
+def finish(results, base, mix):
     experts, cap, width = results.shape
     rows = base.shape[0]
     block = 512
     tiled = pl.BlockSpec((rows, block), lambda g: (0, g))
-    fixed = pl.BlockSpec(ids.shape, lambda g: (0, 0))
     return pl.pallas_call(
         finish_kernel,
         grid=(width // block,),
         in_specs=[
             pl.BlockSpec((experts, cap, block), lambda g: (0, 0, g)),
             tiled,
-            fixed,
-            fixed,
+            pl.BlockSpec(mix.shape, lambda g: (0, 0)),
         ],
         out_specs=tiled,
-        scratch_shapes=[pltpu.VMEM((2 * rows, experts * cap), BF)],
         out_shape=jax.ShapeDtypeStruct(base.shape, BF),
         compiler_params=pltpu.CompilerParams(dimension_semantics=("arbitrary",)),
         name="finish",
-    )(results, base, ids, route)
+    )(results, base, mix)
 
 
 def local(
@@ -462,15 +467,9 @@
     q_send = pack_queries(queries, f_t, own, y_count)
     q_all = lax.all_to_all(q_send, ("y", "c"), split_axis=0, concat_axis=0)
     core = lax.axis_index("c")
-    half_rows = out_weight.shape[0] // 2
-    mine = lax.dynamic_slice_in_dim(out_weight, core * half_rows, half_rows, 0)
-    next_tp = [(i, (i + 1) % tps) for i in range(tps)]
-    last_tp = [(i, (i - 1) % tps) for i in range(tps)]
-    w_up = lax.ppermute(mine, "tp", next_tp)
-    w_down = lax.ppermute(mine, "tp", last_tp)
-
-    def swap(x):
-        return lax.ppermute(x, "c", [(0, 1), (1, 0)])
+    turn = [(i, (i + 1) % tps) for i in range(tps)]
+    turn += [(tps + i, tps + (i - 1) % tps) for i in range(tps)]
+    w_near = lax.ppermute(out_weight, ("c", "tp"), turn)
 
     def up(block):
         return lax.ppermute(block, "z", up_ring)
@@ -483,22 +482,18 @@
     up2, down2 = up(up1), down(down1)
     up3, down3 = up(up2), down(down2)
     state = attend(info, q_all, [own, up1, down1], (0, 1, -1), z_count, None, False)
-    state, up3, down3, w_up = lax.optimization_barrier((state, up3, down3, w_up))
+    state, up3, down3, _ = lax.optimization_barrier((state, up3, down3, w_near))
     up4 = up(up3)
-    w_far = lax.ppermute(w_up, "tp", next_tp)
+    w_far = lax.ppermute(w_near, ("c", "tp"), turn)
     state = attend(info, q_all, [up2, down2], (2, -2), z_count, state, False)
-    state, w_down = lax.optimization_barrier((state, w_down))
-    w_up2, w_down2 = swap(w_up), swap(w_down)
+    w_other = lax.ppermute(w_near, "c", [(0, 1), (1, 0)])
     sent = attend(info, q_all, [up3, down3, up4], (3, -3, 4), z_count, state, True)
-    sent, w_far = lax.optimization_barrier((sent, w_far))
-    w_far2 = swap(w_far)
     parts = lax.all_to_all(sent, ("y", "c", "tp"), split_axis=0, concat_axis=0)
-    weights = [out_weight, w_up, w_up2, w_down, w_down2, w_far, w_far2]
+    weights = [out_weight, w_near, w_other, w_far]
     stream, normed, outgoing = post(
         info,
         parts,
         weights,
-        (0, tps - 1, 1, 2),
         residual,
         norm_gain[None, :],
         expert_ids.T,
@@ -515,7 +510,8 @@
     returned = lax.all_to_all(
         processed, ("z", "y", "c"), split_axis=0, concat_axis=0
     )
-    return finish(returned, base, expert_ids, route_weights)
+    mix = mixing(expert_ids, route_weights, experts, cap)
+    return finish(returned, base, mix)
 
 
 def solution(mesh):

time: 238 us -> 232 us (0.975)
  blocking collectives: 65.1 us -> 89.5 us
  waiting for transfers between devices: 74.2 us -> 59 us
  local copies, waits for them, and re-layouts: 13.1 us -> 1.47 us
  starting transfers between devices: 34.3 us -> 26 us
  Pallas kernels: 45.2 us -> 50.5 us
    all_to_all x0 -> x1, blocking collectives: none -> 23.8 us  [local(): parts = lax.all_to_all(sent, ('y', 'c', 'tp'), split_axis=0, concat_axis=0)]
    all_to_all x1 -> x0, waiting for transfers between devices: 10.2 us -> none  [local(): parts = lax.all_to_all(sent, ('y', 'c', 'tp'), split_axis=0, concat_axis=0)]
    unnamed x36 -> x22, local copies, waits for them, and re-layouts: 10.7 us -> 1.47 us
    ppermute x6 -> x3, waiting for transfers between devices: 7.62 us -> 0.01 us  [the longest x1 0.01 us: local(): w_near = lax.ppermute(out_weight, ('c', 'tp'), turn)]
    pallas_call x1 -> x2, Pallas kernels: 5 us -> 11.1 us  [the longest x1 9.22 us: post(): pl.pallas_call(functools.partial(post_kernel, tps=len(weights)), in_specs...]
    all_to_all x1 -> x0, starting transfers between devices: 5.82 us -> none  [local(): parts = lax.all_to_all(sent, ('y', 'c', 'tp'), split_axis=0, concat_axis=0)]
    ppermute x4, waiting for transfers between devices: 11.4 us -> 15.5 us  [up(): return lax.ppermute(block, 'z', up_ring)]
    ppermute x6 -> x3, starting transfers between devices: 4.81 us -> 2.66 us  [the longest x1 1.49 us: local(): w_near = lax.ppermute(out_weight, ('c', 'tp'), turn)]
  transfers between devices with their start and end apart: 16 -> 12, of which waited for: 7 -> 4; matrix products, arithmetic and copies ran while one was open for 4% -> 3% of each run, Pallas kernels for 11% -> 14%
where the time goes in v4:
time: 232 us; the launch traced here: 231 us
  blocking collectives  89.5 us (39%)
  waiting for transfers between devices  59 us (25%)
  Pallas kernels  50.5 us (22%)
  starting transfers between devices  26 us (11%)
  matrix products  4.33 us (2%)
    all_to_all x1, blocking collectives, local(): lax.all_to_all(outgoing, ('z', 'y', 'c'), split_axis=0, concat_axis=0)  59.5 us
    all_to_all x1, waiting for transfers between devices, local(): lax.all_to_all(processed, ('z', 'y', 'c'), split_axis=0, concat_axis=0)  43.5 us
    pallas_call x3, Pallas kernels, attend(): pl.pallas_call(functools.partial(attend_kernel, steps=steps, z_count=z_co...  26.3 us
    all_to_all x1, blocking collectives, local(): parts = lax.all_to_all(sent, ('y', 'c', 'tp'), split_axis=0, concat_axis=0)  23.8 us
    ppermute x4, waiting for transfers between devices, up(): return lax.ppermute(block, 'z', up_ring)  15.5 us
    ppermute x3, starting transfers between devices, down(): return lax.ppermute(block, 'z', down_ring)  10.5 us
    pallas_call x1, Pallas kernels, post(): pl.pallas_call(functools.partial(post_kernel, tps=len(weights)), in_specs...  9.22 us
    all_to_all x1, blocking collectives, local(): own = lax.all_to_all(kv_send, 'c', split_axis=0, concat_axis=0)  6.11 us
  transfers between devices with their start and end apart: 12, of which 4 were waited for; matrix products, arithmetic and copies ran while one was open for 3% of the time, Pallas kernels for 14%

profile of v4, /device:TPU:8, one launch (start us, length us, event | category | flops | bytes accessed | tf_op | source)
XLA Modules:
  0.0 231.0 jit_solution(18331011534594867423)
XLA Ops:
  0.0 0.0 copy-start
  0.0 1.5 collective-permute-start.6
  1.5 1.8 pack_keys.1
  3.3 6.1 %all_to_all.25._.refs_1_ = bf16[2,264,256]{2,1,0:T(8,128)(2,1)} all-to-all(bf16[2,264,256]{2,1,0:T(8,128)(2,1)} %pack_keys.1), channel_id=1, replica_groups=mesh['z'=8,'y'=4,'c'=2,'tp'=4] {'c'}, dimensions={0} | all-to-all | bytes 540672 | tf_op jit(solution)/shard_map/all_to_all | solution.py:464
  9.4 0.0 copy-start.4
  9.4 2.0 pack_queries.1
  11.4 4.9 %all-to-all-start.1 = ((bf16[8,264,256]{2,1,0:T(8,128)(2,1)}), bf16[8,264,256]{2,1,0:T(8,128)(2,1)S(1)}, u32[]{:S(2)}, u32[]{:S(2)}) async-start(bf16[8,264,256]{2,1,0:T(8,128)(2,1)} %pack_queries.1), calls=%async_computation.1 | async-start | bytes 2162688 | tf_op jit(solution)/shard_map/all_to_all | solution.py:468
  16.3 0.0 copy-done.4
  16.3 1.9 collective-permute-start
  18.3 4.0 %collective-permute-start.1 = (bf16[2,264,256]{2,1,0:T(8,128)(2,1)S(1)}, bf16[2,264,256]{2,1,0:T(8,128)(2,1)}, u32[]{:S(2)}, u32[]{:S(2)}) collective-permute-start(bf16[2,264,256]{2,1,0:T(8,128)(2,1)S(1)} %copy-done.4), channel_id=1, source_target_pairs={{0,224},{32,0},{64,32},{96,64},{128,96},{160,128},{192,160},{224,1... | collective-permute-start | bytes 811016 | tf_op jit(solution)/shard_map/ppermute | solution.py:478
  22.3 6.7 %collective-permute-done.refs_2_ = bf16[2,264,256]{2,1,0:T(8,128)(2,1)S(1)} collective-permute-done((bf16[2,264,256]{2,1,0:T(8,128)(2,1)S(1)}, bf16[2,264,256]{2,1,0:T(8,128)(2,1)S(1)}, u32[]{:S(2)}, u32[]{:S(2)}) %collective-permute-start) | collective-permute-done | bytes 270368 | tf_op jit(solution)/shard_map/ppermute | solution.py:475
  29.0 0.0 collective-permute-start.2
  29.0 0.0 collective-permute-done.1.refs_3_
  29.0 3.2 %collective-permute-start.4 = (bf16[2,264,256]{2,1,0:T(8,128)(2,1)}, bf16[2,264,256]{2,1,0:T(8,128)(2,1)}, u32[]{:S(2)}, u32[]{:S(2)}) collective-permute-start(bf16[2,264,256]{2,1,0:T(8,128)(2,1)} %collective-permute-done.1.refs_3_), channel_id=1, source_target_pairs={{0,224},{32,0},{64,32},{96,64},{128,96},{160,128},{192,160},{224,1... | collective-permute-start | bytes 811016 | tf_op jit(solution)/shard_map/ppermute | solution.py:478
  32.2 0.1 pad_add_fusion.info
  32.3 0.0 copy-start.5
  32.3 5.8 %collective-permute-done.2.refs_1_ = bf16[2,264,256]{2,1,0:T(8,128)(2,1)S(1)} collective-permute-done((bf16[2,264,256]{2,1,0:T(8,128)(2,1)S(1)}, bf16[2,264,256]{2,1,0:T(8,128)(2,1)S(1)}, u32[]{:S(2)}, u32[]{:S(2)}) %collective-permute-start.2) | collective-permute-done | bytes 270368 | tf_op jit(solution)/shard_map/ppermute | solution.py:475
  38.1 0.0 collective-permute-start.3
  38.1 0.0 collective-permute-done.4.refs_2_
  38.1 3.3 %collective-permute-start.5 = (bf16[2,264,256]{2,1,0:T(8,128)(2,1)}, bf16[2,264,256]{2,1,0:T(8,128)(2,1)}, u32[]{:S(2)}, u32[]{:S(2)}) collective-permute-start(bf16[2,264,256]{2,1,0:T(8,128)(2,1)} %collective-permute-done.4.refs_2_), channel_id=1, source_target_pairs={{0,224},{32,0},{64,32},{96,64},{128,96},{160,128},{192,160},{224,1... | collective-permute-start | bytes 811016 | tf_op jit(solution)/shard_map/ppermute | solution.py:478
  41.4 0.0 collective-permute-done.6.refs_1_
  41.4 0.0 collective-permute-start.8
  41.4 1.2 collective-permute-start.9
  42.5 0.0 all-to-all-done.1.refs_0_
  42.5 9.1 %shard_map.145 = (f32[8,256,512]{2,1,0:T(8,128)S(1)}, f32[8,256,256]{2,1,0:T(8,128)S(1)}) custom-call(s32[4]{0:T(128)S(1)} %pad_add_fusion.info, bf16[8,264,256]{2,1,0:T(8,128)(2,1)S(1)} %all-to-all-done.1.refs_0_, bf16[2,264,256]{2,1,0:T(8,128)(2,1)S(1)} %copy-done.4, bf16[2,264,256]{2,1,0:T(8,128)(2,1)S(1)} %collective-permute-done.refs_2_, ...), custom_call_target="tpu_custom_call" | custom-call | flops 4831838208 | bytes 6000000 | tf_op jit(solution)/shard_map/pallas_call | solution.py:216
  51.6 0.0 collective-permute-done.3.refs_1_
  51.6 0.0 collective-permute-done.5.refs_2_
  51.6 0.3 collective-permute-start.7
  51.9 7.2 %shard_map.146 = (f32[8,256,512]{2,1,0:T(8,128)S(1)}, f32[8,256,256]{2,1,0:T(8,128)S(1)}) custom-call(s32[4]{0:T(128)S(1)} %pad_add_fusion.info, bf16[8,264,256]{2,1,0:T(8,128)(2,1)S(1)} %all-to-all-done.1.refs_0_, bf16[2,264,256]{2,1,0:T(8,128)(2,1)S(1)} %collective-permute-done.2.refs_1_, ...), custom_call_target="tpu_custom_call", output_to_operand_aliasing={{0}: (4, {}), {1}: (5, {})} | custom-call | flops 3221225472 | bytes 6000000 | tf_op jit(solution)/shard_map/pallas_call | solution.py:216
  59.2 3.0 %collective-permute-done.7.refs_3_ = bf16[2,264,256]{2,1,0:T(8,128)(2,1)S(1)} collective-permute-done((bf16[2,264,256]{2,1,0:T(8,128)(2,1)}, bf16[2,264,256]{2,1,0:T(8,128)(2,1)S(1)}, u32[]{:S(2)}, u32[]{:S(2)}) %collective-permute-start.7) | collective-permute-done | bytes 270368 | tf_op jit(solution)/shard_map/ppermute | solution.py:475
  62.2 0.0 copy-done.5
  62.2 9.9 %shard_map.147 = bf16[32,72,256]{2,1,0:T(8,128)(2,1)S(1)} custom-call(s32[4]{0:T(128)S(1)} %pad_add_fusion.info, bf16[8,264,256]{2,1,0:T(8,128)(2,1)S(1)} %all-to-all-done.1.refs_0_, bf16[2,264,256]{2,1,0:T(8,128)(2,1)} %collective-permute-done.3.refs_1_, bf16[2,264,256]{2,1,0:T(8,128)(2,1)} %collective-permute-done.5.refs_2_, ...), custom_call_target="tpu_custom_call" | custom-call | flops 4831838208 | bytes 6000000 | tf_op jit(solution)/shard_map/pallas_call | solution.py:216
  72.1 23.8 %all_to_all.26.part_ref = bf16[32,72,256]{2,1,0:T(8,128)(2,1)} all-to-all(bf16[32,72,256]{2,1,0:T(8,128)(2,1)S(1)} %shard_map.147), channel_id=1, replica_groups=mesh['z'=8,'y'=4,'c'=2,'tp'=4] {'y','c','tp'}, dimensions={0} | all-to-all | bytes 2359296 | tf_op jit(solution)/shard_map/all_to_all | solution.py:491
  96.0 0.0 collective-permute-done.8.refs_2_
  96.0 0.0 collective-permute-done.9.refs_3_
  96.0 0.0 copy-start.3
  96.0 9.2 %post.1 = (bf16[64,2048]{1,0:T(8,128)(2,1)}, bf16[64,2048]{1,0:T(8,128)(2,1)}, bf16[64,8,2048]{2,1,0:T(8,128)(2,1)}) custom-call(s32[4]{0:T(128)} %copy-done.5, bf16[32,72,256]{2,1,0:T(8,128)(2,1)} %all_to_all.26.part_ref, bf16[512,2048]{1,0:T(8,128)(2,1)} %refs_0_.1, bf16[512,2048]{1,0:T(8,128)(2,1)} %collective-permute-done.6.refs_1_, ...), custom_call_target="tpu_custom_call" | custom-call | tf_op jit(solution)/shard_map/post/pallas_call | solution.py:315
  105.2 0.0 copy-start.1
  105.2 0.0 copy-start.2
  105.2 59.5 %all_to_all.27.x_ref = bf16[64,8,2048]{2,1,0:T(8,128)(2,1)S(1)} all-to-all(bf16[64,8,2048]{2,1,0:T(8,128)(2,1)} %get-tuple-element.24), channel_id=1, replica_groups=mesh['z'=8,'y'=4,'c'=2,'tp'=4] {'z','y','c'}, dimensions={0} | all-to-all | bytes 4194304 | tf_op jit(solution)/shard_map/all_to_all | solution.py:503
  164.8 0.0 copy-done.3
  164.8 0.0 copy-done.1
  164.8 0.0 copy-done.2
  164.8 5.2 %expert.1 = bf16[64,8,2048]{2,1,0:T(8,128)(2,1)} custom-call(bf16[64,8,2048]{2,1,0:T(8,128)(2,1)S(1)} %all_to_all.27.x_ref, bf16[1,2048,384]{2,1,0:T(8,128)(2,1)S(1)} %copy-done.1, bf16[1,2048,384]{2,1,0:T(8,128)(2,1)S(1)} %copy-done.2, bf16[1,384,2048]{2,1,0:T(8,128)(2,1)S(1)} %copy-done.3), custom_call_target="tpu_custom_call" | custom-call | tf_op jit(solution)/shard_map/expert/pallas_call | solution.py:350
  170.0 0.0 copy-start.8
  170.0 0.0 copy-start.9
  170.0 0.0 copy-start.7
  170.0 5.8 %all-to-all-start.4 = ((bf16[64,8,2048]{2,1,0:T(8,128)(2,1)}), bf16[64,8,2048]{2,1,0:T(8,128)(2,1)}, u32[]{:S(2)}, u32[]{:S(2)}) async-start(bf16[64,8,2048]{2,1,0:T(8,128)(2,1)} %expert.1), calls=%async_computation.4 | async-start | bytes 4194304 | tf_op jit(solution)/shard_map/all_to_all | solution.py:510
  175.7 0.0 copy-done.8
  175.8 0.0 copy-start.6
  175.8 0.7 copy.18.ids_ref
  176.5 0.0 copy-done.9
  176.5 0.7 copy.19.route_ref
  177.2 1.9 mixing.1.mix_ref
  179.1 0.0 copy-done.7
  179.1 1.8 fusion.5
  180.8 0.0 copy-done
  180.8 0.0 copy-done.6
  180.8 2.6 %convert_add_fusion.base_ref = f32[64,2048]{1,0:T(8,128)} fusion(bf16[64,2048]{1,0:T(8,128)(2,1)} %get-tuple-element.25, bf16[384,2048]{1,0:T(8,128)(2,1)S(1)} %copy-done, f32[64,384]{1,0:T(8,128)S(1)} %fusion.5, bf16[64,2048]{1,0:T(8,128)(2,1)S(1)} %copy-done.7, bf16[2048,384]{1,0:T(8,128)(2,1)S(1)} %copy-done.6), kind=kOutput, calls=%fused_computation | convolution fusion | flops 201736192 | bytes 4292608 | tf_op jit(solution)/shard_map/dot_general | solution.py:508
  183.4 43.5 %all-to-all-done.4.res_ref = bf16[64,8,2048]{2,1,0:T(8,128)(2,1)} async-done(((bf16[64,8,2048]{2,1,0:T(8,128)(2,1)}), bf16[64,8,2048]{2,1,0:T(8,128)(2,1)}, u32[]{:S(2)}, u32[]{:S(2)}) %all-to-all-start.4) | async-done | bytes 2097184 | tf_op jit(solution)/shard_map/all_to_all | solution.py:510
  226.9 4.1 %finish.1 = bf16[64,2048]{1,0:T(8,128)(2,1)} custom-call(bf16[64,8,2048]{2,1,0:T(8,128)(2,1)} %all-to-all-done.4.res_ref, f32[64,2048]{1,0:T(8,128)} %convert_add_fusion.base_ref, bf16[128,512]{1,0:T(8,128)(2,1)} %mixing.1.mix_ref), custom_call_target="tpu_custom_call" | custom-call | tf_op jit(solution)/shard_map/finish/pallas_call | solution.py:421
Async XLA Ops:
  0.0 180.8 %copy-start = (bf16[384,2048]{1,0:T(8,128)(2,1)S(1)}, bf16[384,2048]{1,0:T(8,128)(2,1)}, u32[]{:S(2)}) copy-start(bf16[384,2048]{1,0:T(8,128)(2,1)} %param.29) | copy-start | bytes 4718596
  0.0 41.4 %collective-permute-start.6 = (bf16[512,2048]{1,0:T(8,128)(2,1)}, bf16[512,2048]{1,0:T(8,128)(2,1)}, u32[]{:S(2)}, u32[]{:S(2)}) collective-permute-start(bf16[512,2048]{1,0:T(8,128)(2,1)} %refs_0_.1), channel_id=1, source_target_pairs={{0,1},{1,2},{2,3},{3,0},{4,7},{5,4},{6,5},{7,6},{8,9},{9,10},{10,1... | collective-permute-start | bytes 6291464 | tf_op jit(solution)/shard_map/ppermute | solution.py:472
  9.4 7.0 %copy-start.4 = (bf16[2,264,256]{2,1,0:T(8,128)(2,1)S(1)}, bf16[2,264,256]{2,1,0:T(8,128)(2,1)}, u32[]{:S(2)}) copy-start(bf16[2,264,256]{2,1,0:T(8,128)(2,1)} %all_to_all.25._.refs_1_) | copy-start | bytes 811012
  11.4 31.1 %all-to-all-start.1 = ((bf16[8,264,256]{2,1,0:T(8,128)(2,1)}), bf16[8,264,256]{2,1,0:T(8,128)(2,1)S(1)}, u32[]{:S(2)}, u32[]{:S(2)}) async-start(bf16[8,264,256]{2,1,0:T(8,128)(2,1)} %pack_queries.1), calls=%async_computation.1 | async-start | bytes 2162688 | tf_op jit(solution)/shard_map/all_to_all | solution.py:468
  16.3 12.6 %collective-permute-start = (bf16[2,264,256]{2,1,0:T(8,128)(2,1)S(1)}, bf16[2,264,256]{2,1,0:T(8,128)(2,1)S(1)}, u32[]{:S(2)}, u32[]{:S(2)}) collective-permute-start(bf16[2,264,256]{2,1,0:T(8,128)(2,1)S(1)} %copy-done.4), channel_id=1, source_target_pairs={{0,32},{32,64},{64,96},{96,128},{128,160},{160,192},{192,224},{224... | collective-permute-start | bytes 811016 | tf_op jit(solution)/shard_map/ppermute | solution.py:475
  18.3 10.7 %collective-permute-start.1 = (bf16[2,264,256]{2,1,0:T(8,128)(2,1)S(1)}, bf16[2,264,256]{2,1,0:T(8,128)(2,1)}, u32[]{:S(2)}, u32[]{:S(2)}) collective-permute-start(bf16[2,264,256]{2,1,0:T(8,128)(2,1)S(1)} %copy-done.4), channel_id=1, source_target_pairs={{0,224},{32,0},{64,32},{96,64},{128,96},{160,128},{192,160},{224,1... | collective-permute-start | bytes 811016 | tf_op jit(solution)/shard_map/ppermute | solution.py:478
  29.0 9.1 %collective-permute-start.2 = (bf16[2,264,256]{2,1,0:T(8,128)(2,1)S(1)}, bf16[2,264,256]{2,1,0:T(8,128)(2,1)S(1)}, u32[]{:S(2)}, u32[]{:S(2)}) collective-permute-start(bf16[2,264,256]{2,1,0:T(8,128)(2,1)S(1)} %collective-permute-done.refs_2_), channel_id=1, source_target_pairs={{0,32},{32,64},{64,96},{96,128},{128,160},{160,192},{192,224},{224... | collective-permute-start | bytes 811016 | tf_op jit(solution)/shard_map/ppermute | solution.py:475
  29.0 9.1 %collective-permute-start.4 = (bf16[2,264,256]{2,1,0:T(8,128)(2,1)}, bf16[2,264,256]{2,1,0:T(8,128)(2,1)}, u32[]{:S(2)}, u32[]{:S(2)}) collective-permute-start(bf16[2,264,256]{2,1,0:T(8,128)(2,1)} %collective-permute-done.1.refs_3_), channel_id=1, source_target_pairs={{0,224},{32,0},{64,32},{96,64},{128,96},{160,128},{192,160},{224,1... | collective-permute-start | bytes 811016 | tf_op jit(solution)/shard_map/ppermute | solution.py:478
  32.3 29.9 %copy-start.5 = (s32[4]{0:T(128)}, s32[4]{0:T(128)S(1)}, u32[]{:S(2)}) copy-start(s32[4]{0:T(128)S(1)} %pad_add_fusion.info) | copy-start | bytes 52
  38.1 13.5 %collective-permute-start.3 = (bf16[2,264,256]{2,1,0:T(8,128)(2,1)S(1)}, bf16[2,264,256]{2,1,0:T(8,128)(2,1)}, u32[]{:S(2)}, u32[]{:S(2)}) collective-permute-start(bf16[2,264,256]{2,1,0:T(8,128)(2,1)S(1)} %collective-permute-done.2.refs_1_), channel_id=1, source_target_pairs={{0,32},{32,64},{64,96},{96,128},{128,160},{160,192},{192,224},{224... | collective-permute-start | bytes 811016 | tf_op jit(solution)/shard_map/ppermute | solution.py:475
  38.1 13.5 %collective-permute-start.5 = (bf16[2,264,256]{2,1,0:T(8,128)(2,1)}, bf16[2,264,256]{2,1,0:T(8,128)(2,1)}, u32[]{:S(2)}, u32[]{:S(2)}) collective-permute-start(bf16[2,264,256]{2,1,0:T(8,128)(2,1)} %collective-permute-done.4.refs_2_), channel_id=1, source_target_pairs={{0,224},{32,0},{64,32},{96,64},{128,96},{160,128},{192,160},{224,1... | collective-permute-start | bytes 811016 | tf_op jit(solution)/shard_map/ppermute | solution.py:478
  41.4 54.6 %collective-permute-start.8 = (bf16[512,2048]{1,0:T(8,128)(2,1)}, bf16[512,2048]{1,0:T(8,128)(2,1)}, u32[]{:S(2)}, u32[]{:S(2)}) collective-permute-start(bf16[512,2048]{1,0:T(8,128)(2,1)} %collective-permute-done.6.refs_1_), channel_id=1, source_target_pairs={{0,4},{4,0},{1,5},{5,1},{2,6},{6,2},{3,7},{7,3},{8,12},{12,8},{9,1... | collective-permute-start | bytes 6291464 | tf_op jit(solution)/shard_map/ppermute | solution.py:489
  41.4 54.6 %collective-permute-start.9 = (bf16[512,2048]{1,0:T(8,128)(2,1)}, bf16[512,2048]{1,0:T(8,128)(2,1)}, u32[]{:S(2)}, u32[]{:S(2)}) collective-permute-start(bf16[512,2048]{1,0:T(8,128)(2,1)} %collective-permute-done.6.refs_1_), channel_id=1, source_target_pairs={{0,1},{1,2},{2,3},{3,0},{4,7},{5,4},{6,5},{7,6},{8,9},{9,10},{10,1... | collective-permute-start | bytes 6291464 | tf_op jit(solution)/shard_map/ppermute | solution.py:487
  51.6 10.5 %collective-permute-start.7 = (bf16[2,264,256]{2,1,0:T(8,128)(2,1)}, bf16[2,264,256]{2,1,0:T(8,128)(2,1)S(1)}, u32[]{:S(2)}, u32[]{:S(2)}) collective-permute-start(bf16[2,264,256]{2,1,0:T(8,128)(2,1)} %collective-permute-done.3.refs_1_), channel_id=1, source_target_pairs={{0,32},{32,64},{64,96},{96,128},{128,160},{160,192},{192,224},{224... | collective-permute-start | bytes 811016 | tf_op jit(solution)/shard_map/ppermute | solution.py:475
  96.0 68.8 %copy-start.3 = (bf16[1,384,2048]{2,1,0:T(8,128)(2,1)S(1)}, bf16[1,384,2048]{2,1,0:T(8,128)(2,1)}, u32[]{:S(2)}) copy-start(bf16[1,384,2048]{2,1,0:T(8,128)(2,1)} %down_ref.1) | copy-start | bytes 4718596
  105.2 59.5 %copy-start.1 = (bf16[1,2048,384]{2,1,0:T(8,128)(2,1)S(1)}, bf16[1,2048,384]{2,1,0:T(8,128)(2,1)}, u32[]{:S(2)}) copy-start(bf16[1,2048,384]{2,1,0:T(8,128)(2,1)} %gate_ref.1) | copy-start | bytes 4718596
  105.2 59.5 %copy-start.2 = (bf16[1,2048,384]{2,1,0:T(8,128)(2,1)S(1)}, bf16[1,2048,384]{2,1,0:T(8,128)(2,1)}, u32[]{:S(2)}) copy-start(bf16[1,2048,384]{2,1,0:T(8,128)(2,1)} %up_ref.1) | copy-start | bytes 4718596
  170.0 5.8 %copy-start.8 = (s32[64,4]{0,1:T(4,128)S(1)}, s32[64,4]{0,1:T(4,128)}, u32[]{:S(2)}) copy-start(s32[64,4]{0,1:T(4,128)} %param.22) | copy-start | bytes 3076
  170.0 6.5 %copy-start.9 = (f32[64,4]{0,1:T(4,128)S(1)}, f32[64,4]{0,1:T(4,128)}, u32[]{:S(2)}) copy-start(f32[64,4]{0,1:T(4,128)} %param.23) | copy-start | bytes 3076
  170.0 9.1 %copy-start.7 = (bf16[64,2048]{1,0:T(8,128)(2,1)S(1)}, bf16[64,2048]{1,0:T(8,128)(2,1)}, u32[]{:S(2)}) copy-start(bf16[64,2048]{1,0:T(8,128)(2,1)} %get-tuple-element.26) | copy-start | bytes 786436
  170.0 56.9 %all-to-all-start.4 = ((bf16[64,8,2048]{2,1,0:T(8,128)(2,1)}), bf16[64,8,2048]{2,1,0:T(8,128)(2,1)}, u32[]{:S(2)}, u32[]{:S(2)}) async-start(bf16[64,8,2048]{2,1,0:T(8,128)(2,1)} %expert.1), calls=%async_computation.4 | async-start | bytes 4194304 | tf_op jit(solution)/shard_map/all_to_all | solution.py:510
  175.8 5.1 %copy-start.6 = (bf16[2048,384]{1,0:T(8,128)(2,1)S(1)}, bf16[2048,384]{1,0:T(8,128)(2,1)}, u32[]{:S(2)}) copy-start(bf16[2048,384]{1,0:T(8,128)(2,1)} %param.28) | copy-start | bytes 4718596

commit v5 on v4

--- a/solution.py
+++ b/solution.py
@@ -39,12 +39,13 @@
     return tail[3 * j : 3 * j + 1] + tail[3 * j + 1 : 3 * j + 2] + tail[3 * j + 2 : 3 * j + 3]
 
 
-def pack_keys_kernel(k_ref, v_ref, f_ref, out):
+def pack_keys_kernel(info, k_ref, v_ref, f_ref, mine, other):
     rows = k_ref.shape[0]
-    for c in range(2):
-        out[c, :rows, :HEAD_DIM] = k_ref[:, c * HEAD_DIM : (c + 1) * HEAD_DIM]
-        out[c, :rows, HEAD_DIM:] = v_ref[:, c * HEAD_DIM : (c + 1) * HEAD_DIM]
-        out[c, rows:, :] = tail_block([f_ref[2 * c : 2 * c + 1, :], f_ref[2 * c + 1 : 2 * c + 2, :]], rows)
+    for out, c in ((mine, info[3]), (other, 1 - info[3])):
+        cols = pl.ds(pl.multiple_of(c * HEAD_DIM, HEAD_DIM), HEAD_DIM)
+        out[:rows, :HEAD_DIM] = k_ref[:, cols]
+        out[:rows, HEAD_DIM:] = v_ref[:, cols]
+        out[rows:, :] = tail_block([f_ref[pl.ds(2 * c + j, 1), :] for j in range(2)], rows)
 
 
 def pack_queries_kernel(q_ref, f_ref, _, out):
@@ -57,12 +58,15 @@
             out[2 * y + c, rows:, :] = tail
 
 
-def pack_keys(k, v, f_t):
+def pack_keys(info, k, v, f_t):
+    shape = (k.shape[0] + TAIL, 2 * HEAD_DIM)
+    vmem = pl.BlockSpec(memory_space=pltpu.VMEM)
     return pl.pallas_call(
         pack_keys_kernel,
-        out_shape=pltpu.HBM((2, k.shape[0] + TAIL, 2 * HEAD_DIM), BF),
+        in_specs=[pl.BlockSpec(memory_space=pltpu.SMEM)] + [vmem] * 3,
+        out_shape=(pltpu.HBM(shape, BF), pltpu.HBM(shape, BF)),
         name="pack_keys",
-    )(k, v, f_t)
+    )(info, k, v, f_t)
 
 
 def pack_queries(q, f_t, after, ys):
@@ -116,7 +120,7 @@
                     q_pos = i * rows + lax.broadcasted_iota(
                         jnp.int32, (rows, rows), 0
                     )
-                    k_pos = info[0] + u * rows + lax.broadcasted_iota(jnp.int32, (rows, rows), 1)
+                    k_pos = info[0] + (u ^ info[3]) * rows + lax.broadcasted_iota(jnp.int32, (rows, rows), 1)
                     score = jnp.where(q_pos >= k_pos, score, -jnp.inf)
                 found[j].append(score)
         return found
@@ -230,7 +234,7 @@
 
 def post_kernel(info, part_ref, *refs, tps):
     w_refs = refs[:tps]
-    res_ref, gain_ref, ids_ref, stream_out, normed_out, send_out, att, weight, sems = refs[tps:]
+    res_ref, gain_ref, ids_ref, stream_out, normed_out, send_out, total_ref, weight, share, sems = refs[tps:]
     sources = part_ref.shape[0]
     own_rows = res_ref.shape[0]
     width = part_ref.shape[2]
@@ -247,33 +251,56 @@
     pick = lax.broadcasted_iota(jnp.int32, (own_rows, width), 1) == (
         info[2] * own_rows + lax.broadcasted_iota(jnp.int32, (own_rows, width), 0)
     )
+    tails = part_ref[:, own_rows:, :].reshape(sources * TAIL, width)
+    pieces_t = lax.dot_general(
+        pick.astype(F32).astype(BF), tails, (((1,), (1,)), ((), ())), preferred_element_type=F32
+    )
+    last = pieces_t.shape[1]
+    lses = pieces_t + pltpu.roll(pieces_t, last - 1, 1) + pltpu.roll(pieces_t, last - 2, 1)
+    span = last // ys
+    lses = [lses[:, y * span : (y + 1) * span] for y in range(ys)]
+    top = lses[0]
+    for one in lses[1:]:
+        top = jnp.maximum(top, one)
+    shares = [jnp.exp2(one - top) for one in lses]
+    total = shares[0]
+    for one in shares[1:]:
+        total = total + one
+    inverse = 1.0 / total
+    shares = [one * inverse for one in shares]
+    spare = jnp.zeros((own_rows, HEAD_DIM - 2 * ys), F32)
+    for index in range(groups):
+        columns = [
+            shares[y][:, TAIL * index + 3 * j : TAIL * index + 3 * j + 1]
+            for y in range(ys)
+            for j in range(2)
+        ]
+        share[index] = jnp.concatenate([*columns, spare], axis=1)
     near = 2 * info[3] - 1
-    for s, turn in enumerate((0, near, -near, 2)):
-        tp = (info[2] + turn + tps) % tps
+    turns = [(info[2] + turn + tps) % tps for turn in (0, near, -near, 2)]
+    block = 2 * width
+    quarter = weight.shape[0] // tps
+    for s, tp in enumerate(turns):
+        merged = []
         for core in range(2):
-            col = (2 * s + core) * width
             index = core * tps + tp
-            tails = [part_ref[y * groups + index, own_rows:, :].astype(F32) for y in range(ys)]
             for j in range(2):
-                sums = []
-                for y in range(ys):
-                    row = row_of(tails[y], j)
-                    sums.append(jnp.sum(jnp.where(pick, row, 0.0), axis=1, keepdims=True))
-                top = sums[0]
-                for one in sums[1:]:
-                    top = jnp.maximum(top, one)
-                weights = [jnp.exp2(one - top) for one in sums]
-                total = weights[0]
-                for w in weights[1:]:
-                    total = total + w
-                inverse = 1.0 / total
                 mixed = None
                 for y in range(ys):
                     part = part_ref[
                         y * groups + index, pl.ds(0, own_rows), pl.ds(j * HEAD_DIM, HEAD_DIM)
-                    ].astype(F32) * (weights[y] * inverse)
+                    ].astype(F32) * share[index, :, y * 2 + j : y * 2 + j + 1]
                     mixed = part if mixed is None else mixed + part
-                att[:, pl.ds(col + j * HEAD_DIM, HEAD_DIM)] = mixed.astype(BF)
+                merged.append(mixed.astype(BF))
+        attended = jnp.concatenate(merged, axis=1)
+        copies[s].wait()
+        for n in range(0, weight.shape[1], block):
+            product = jnp.dot(
+                attended,
+                weight[s * quarter : (s + 1) * quarter, n : n + block],
+                preferred_element_type=F32,
+            )
+            total_ref[:, n : n + block] = product if s == 0 else total_ref[:, n : n + block] + product
 
     experts = send_out.shape[0]
     cap = send_out.shape[1]
@@ -290,23 +317,19 @@
     slot = lax.broadcasted_iota(jnp.int32, (experts, cap, own_rows), 1).astype(F32)
     chosen = (rank[:, None, :] == slot).astype(F32).reshape(experts * cap, own_rows).astype(BF)
 
-    for copy in copies:
-        copy.wait()
-    block = 256
     squares = jnp.zeros((own_rows, 1), F32)
     for n in range(0, weight.shape[1], block):
-        branch = jnp.dot(att[...], weight[:, n : n + block], preferred_element_type=F32)
-        stream = (res_ref[:, n : n + block].astype(F32) + branch).astype(BF)
+        stream = (res_ref[:, n : n + block].astype(F32) + total_ref[:, n : n + block]).astype(BF)
         stream_out[:, n : n + block] = stream
         wide = stream.astype(F32)
         squares = squares + jnp.sum(wide * wide, axis=1, keepdims=True)
     scale = lax.rsqrt(squares / weight.shape[1] + NORM_EPS)
-    for n in range(0, weight.shape[1], 2 * block):
-        cols = slice(n, n + 2 * block)
+    for n in range(0, weight.shape[1], block):
+        cols = slice(n, n + block)
         normed = (stream_out[:, cols].astype(F32) * scale * gain_ref[:, cols]).astype(BF)
         normed_out[:, cols] = normed
         sent = jnp.dot(chosen, normed, preferred_element_type=F32).astype(BF)
-        send_out[:, :, cols] = sent.reshape(experts, cap, 2 * block)
+        send_out[:, :, cols] = sent.reshape(experts, cap, block)
 
 
 def post(info, parts, weights, residual, gain, ids_t, experts, cap):
@@ -319,8 +342,9 @@
         + [vmem] * 3,
         out_specs=[vmem] * 3,
         scratch_shapes=[
-            pltpu.VMEM((rows, width), BF),
+            pltpu.VMEM((rows, width), F32),
             pltpu.VMEM((width, width), BF),
+            pltpu.VMEM((2 * len(weights), rows, HEAD_DIM), F32),
             pltpu.SemaphoreType.DMA((len(weights),)),
         ],
         out_shape=[
@@ -328,7 +352,7 @@
             jax.ShapeDtypeStruct((rows, width), BF),
             jax.ShapeDtypeStruct((experts, cap, width), BF),
         ],
-        compiler_params=pltpu.CompilerParams(vmem_limit_bytes=56 * 1024 * 1024),
+        compiler_params=pltpu.CompilerParams(vmem_limit_bytes=40 * 1024 * 1024),
         name="post",
     )(info, parts, *weights, residual, gain, ids_t)
 
@@ -343,7 +367,7 @@
     out_ref[...] = out.reshape(peers, cap, width)
 
 
-def expert(arrived, gate, up, down, steps=4):
+def expert(arrived, gate, up, down, steps=2):
     peers, cap, width = arrived.shape
     rows = pl.BlockSpec((peers // steps, cap, width), lambda g: (g, 0, 0))
     whole = lambda g: (0, 0, 0)
@@ -413,10 +437,9 @@
     out_ref[...] = (base_ref[...] + routed[:rows] + routed[rows:]).astype(BF)
 
 
-def finish(results, base, mix):
+def finish(results, base, mix, block=1024):
     experts, cap, width = results.shape
     rows = base.shape[0]
-    block = 512
     tiled = pl.BlockSpec((rows, block), lambda g: (0, g))
     return pl.pallas_call(
         finish_kernel,
@@ -459,14 +482,16 @@
     cap = 2 * residual.shape[0] * TOPK // experts
 
     tps = lax.axis_size("tp")
+    core = lax.axis_index("c")
+    info = jnp.stack([2 * y * rows, z, lax.axis_index("tp"), core]).astype(jnp.int32)
     f_t = forget_sums.T
-    kv_send = pack_keys(key_rows, value_rows, f_t)
-    own = lax.all_to_all(kv_send, "c", split_axis=0, concat_axis=0)
+    mine, other = pack_keys(info, key_rows, value_rows, f_t)
+    theirs = lax.ppermute(other, "c", [(0, 1), (1, 0)])
+    own = jnp.stack([mine, theirs])
     up_ring = [(i, (i + 1) % z_count) for i in range(z_count)]
     down_ring = [(i, (i - 1) % z_count) for i in range(z_count)]
-    q_send = pack_queries(queries, f_t, own, y_count)
+    q_send = pack_queries(queries, f_t, other, y_count)
     q_all = lax.all_to_all(q_send, ("y", "c"), split_axis=0, concat_axis=0)
-    core = lax.axis_index("c")
     turn = [(i, (i + 1) % tps) for i in range(tps)]
     turn += [(tps + i, tps + (i - 1) % tps) for i in range(tps)]
     w_near = lax.ppermute(out_weight, ("c", "tp"), turn)
@@ -477,17 +502,18 @@
     def down(block):
         return lax.ppermute(block, "z", down_ring)
 
-    info = jnp.stack([2 * y * rows, z, lax.axis_index("tp"), core]).astype(jnp.int32)
     up1, down1 = up(own), down(own)
     up2, down2 = up(up1), down(down1)
+    state = attend(info, q_all, [own, up1, down1], (0, 1, -1), z_count, None, False)
+    state, up2, down2, w_near = lax.optimization_barrier((state, up2, down2, w_near))
     up3, down3 = up(up2), down(down2)
-    state = attend(info, q_all, [own, up1, down1], (0, 1, -1), z_count, None, False)
-    state, up3, down3, _ = lax.optimization_barrier((state, up3, down3, w_near))
-    up4 = up(up3)
     w_far = lax.ppermute(w_near, ("c", "tp"), turn)
     state = attend(info, q_all, [up2, down2], (2, -2), z_count, state, False)
+    state, up3, down3 = lax.optimization_barrier((state, up3, down3))
+    up4 = up(up3)
     w_other = lax.ppermute(w_near, "c", [(0, 1), (1, 0)])
-    sent = attend(info, q_all, [up3, down3, up4], (3, -3, 4), z_count, state, True)
+    state = attend(info, q_all, [up3, down3], (3, -3), z_count, state, False)
+    sent = attend(info, q_all, [up4], (4,), z_count, state, True)
     parts = lax.all_to_all(sent, ("y", "c", "tp"), split_axis=0, concat_axis=0)
     weights = [out_weight, w_near, w_other, w_far]
     stream, normed, outgoing = post(

time: 232 us -> 217 us (0.935)
  blocking collectives: 89.5 us -> 83.8 us
  Pallas kernels: 50.5 us -> 45.5 us
  waiting for transfers between devices: 59 us -> 54 us
    all_to_all x1 -> x0, blocking collectives: 6.11 us -> none  [local(): own = lax.all_to_all(kv_send, 'c', split_axis=0, concat_axis=0)]
    ppermute x4, waiting for transfers between devices: 15.5 us -> 9.66 us  [up(): return lax.ppermute(block, 'z', up_ring)]
    pallas_call x1, Pallas kernels: 9.22 us -> 4.79 us  [post(): pl.pallas_call(functools.partial(post_kernel, tps=len(weights)), in_specs...]
    pallas_call x3 -> x4, Pallas kernels: 26.3 us -> 27.6 us  [attend(): pl.pallas_call(functools.partial(attend_kernel, steps=steps, z_count=z_co...]
  transfers between devices with their start and end apart: 12 -> 13, of which waited for: 4 -> 4; matrix products, arithmetic and copies ran while one was open for 3% -> 3% of each run, Pallas kernels for 14% -> 15%
where the time goes in v5:
time: 217 us
  blocking collectives  83.8 us (39%)
  waiting for transfers between devices  54 us (25%)
  Pallas kernels  45.5 us (21%)
  starting transfers between devices  26.6 us (12%)
  matrix products  4.81 us (2%)
    all_to_all x1, blocking collectives, local(): lax.all_to_all(outgoing, ('z', 'y', 'c'), split_axis=0, concat_axis=0)  59.6 us
    all_to_all x1, waiting for transfers between devices, local(): lax.all_to_all(processed, ('z', 'y', 'c'), split_axis=0, concat_axis=0)  43.1 us
    pallas_call x4, Pallas kernels, attend(): pl.pallas_call(functools.partial(attend_kernel, steps=steps, z_count=z_co...  27.6 us
    all_to_all x1, blocking collectives, local(): parts = lax.all_to_all(sent, ('y', 'c', 'tp'), split_axis=0, concat_axis=0)  24.2 us
    ppermute x3, starting transfers between devices, down(): return lax.ppermute(block, 'z', down_ring)  10.5 us
    ppermute x4, waiting for transfers between devices, up(): return lax.ppermute(block, 'z', up_ring)  9.66 us
    all_to_all x1, starting transfers between devices, local(): lax.all_to_all(processed, ('z', 'y', 'c'), split_axis=0, concat_axis=0)  5.75 us
    all_to_all x1, starting transfers between devices, local(): q_all = lax.all_to_all(q_send, ('y', 'c'), split_axis=0, concat_axis=0)  5.47 us
  transfers between devices with their start and end apart: 13, of which 4 were waited for; matrix products, arithmetic and copies ran while one was open for 3% of the time, Pallas kernels for 15%

profile of v5, /device:TPU:8, one launch (start us, length us, event | category | flops | bytes accessed | tf_op | source)
XLA Modules:
  0.0 216.9 jit_solution(1438247001010133408)
XLA Ops:
  0.0 0.0 copy-start
  0.0 1.5 collective-permute-start.5
  1.5 0.6 pad_add_fusion.info
  2.1 1.7 pack_keys.1
  3.8 0.0 copy-start.9
  3.8 0.0 copy-start.10
  3.8 2.1 pack_queries.1
  5.9 5.5 %all-to-all-start = ((bf16[8,264,256]{2,1,0:T(8,128)(2,1)}), bf16[8,264,256]{2,1,0:T(8,128)(2,1)S(1)}, u32[]{:S(2)}, u32[]{:S(2)}) async-start(bf16[8,264,256]{2,1,0:T(8,128)(2,1)} %pack_queries.1), calls=%async_computation | async-start | bytes 2162688 | tf_op jit(solution)/shard_map/all_to_all | solution.py:494
  11.4 0.0 copy-done.9
  11.4 0.1 collective-permute-start
  11.5 1.3 collective-permute-done
  12.8 0.0 copy-done.10
  12.8 2.0 collective-permute-start.1
  14.8 4.0 %collective-permute-start.2 = (bf16[2,264,256]{2,1,0:T(8,128)(2,1)S(1)}, bf16[2,264,256]{2,1,0:T(8,128)(2,1)}, u32[]{:S(2)}, u32[]{:S(2)}) collective-permute-start(bf16[2,264,256]{2,1,0:T(8,128)(2,1)S(1)} %pad_maximum_fusion.refs_1_), channel_id=1, source_target_pairs={{0,224},{32,0},{64,32},{96,64},{128,96},{160,128},{192,160},{224,1... | collective-permute-start | bytes 811016 | tf_op jit(solution)/shard_map/ppermute | solution.py:503
  18.8 7.0 %collective-permute-done.1.refs_2_ = bf16[2,264,256]{2,1,0:T(8,128)(2,1)} collective-permute-done((bf16[2,264,256]{2,1,0:T(8,128)(2,1)S(1)}, bf16[2,264,256]{2,1,0:T(8,128)(2,1)}, u32[]{:S(2)}, u32[]{:S(2)}) %collective-permute-start.1) | collective-permute-done | bytes 270368 | tf_op jit(solution)/shard_map/ppermute | solution.py:500
  25.8 0.0 collective-permute-start.3
  25.8 0.0 collective-permute-done.2.refs_3_
  25.9 3.2 %collective-permute-start.4 = (bf16[2,264,256]{2,1,0:T(8,128)(2,1)}, bf16[2,264,256]{2,1,0:T(8,128)(2,1)S(1)}, u32[]{:S(2)}, u32[]{:S(2)}) collective-permute-start(bf16[2,264,256]{2,1,0:T(8,128)(2,1)} %collective-permute-done.2.refs_3_), channel_id=1, source_target_pairs={{0,224},{32,0},{64,32},{96,64},{128,96},{160,128},{192,160},{224,1... | collective-permute-start | bytes 811016 | tf_op jit(solution)/shard_map/ppermute | solution.py:503
  29.1 0.0 all-to-all-done.refs_0_
  29.1 0.0 copy-done.8
  29.1 9.4 %shard_map.145 = (f32[8,256,512]{2,1,0:T(8,128)S(1)}, f32[8,256,256]{2,1,0:T(8,128)S(1)}) custom-call(s32[4]{0:T(128)S(1)} %copy-done.8, bf16[8,264,256]{2,1,0:T(8,128)(2,1)S(1)} %all-to-all-done.refs_0_, bf16[2,264,256]{2,1,0:T(8,128)(2,1)S(1)} %pad_maximum_fusion.refs_1_, bf16[2,264,256]{2,1,0:T(8,128)(2,1)} %collective-permute-done.1.refs_2_, ...), custom_call_target="tpu_custom_call" | custom-call | flops 4831838208 | bytes 6000000 | tf_op jit(solution)/shard_map/pallas_call | solution.py:220
  38.5 0.0 collective-permute-done.3.refs_1_
  38.5 0.0 collective-permute-done.4.refs_2_
  38.5 0.0 collective-permute-done.5.refs_1_
  38.5 1.1 collective-permute-start.10
  39.7 0.0 collective-permute-start.9
  39.7 0.0 collective-permute-start.6
  39.7 3.2 %collective-permute-start.7 = (bf16[2,264,256]{2,1,0:T(8,128)(2,1)S(1)}, bf16[2,264,256]{2,1,0:T(8,128)(2,1)S(1)}, u32[]{:S(2)}, u32[]{:S(2)}) collective-permute-start(bf16[2,264,256]{2,1,0:T(8,128)(2,1)S(1)} %collective-permute-done.4.refs_2_), channel_id=1, source_target_pairs={{0,224},{32,0},{64,32},{96,64},{128,96},{160,128},{192,160},{224,1... | collective-permute-start | bytes 811016 | tf_op jit(solution)/shard_map/ppermute | solution.py:503
  42.9 6.9 %shard_map.146 = (f32[8,256,512]{2,1,0:T(8,128)S(1)}, f32[8,256,256]{2,1,0:T(8,128)S(1)}) custom-call(s32[4]{0:T(128)S(1)} %copy-done.8, bf16[8,264,256]{2,1,0:T(8,128)(2,1)S(1)} %all-to-all-done.refs_0_, bf16[2,264,256]{2,1,0:T(8,128)(2,1)S(1)} %collective-permute-done.3.refs_1_, ...), custom_call_target="tpu_custom_call", output_to_operand_aliasing={{0}: (4, {}), {1}: (5, {})} | custom-call | flops 3221225472 | bytes 6000000 | tf_op jit(solution)/shard_map/pallas_call | solution.py:220
  49.9 0.0 collective-permute-done.6.refs_1_
  49.9 0.0 collective-permute-done.7.refs_2_
  49.9 0.1 collective-permute-start.8
  50.0 6.9 %shard_map.147 = (f32[8,256,512]{2,1,0:T(8,128)S(1)}, f32[8,256,256]{2,1,0:T(8,128)S(1)}) custom-call(s32[4]{0:T(128)S(1)} %copy-done.8, bf16[8,264,256]{2,1,0:T(8,128)(2,1)S(1)} %all-to-all-done.refs_0_, bf16[2,264,256]{2,1,0:T(8,128)(2,1)S(1)} %collective-permute-done.6.refs_1_, ...), custom_call_target="tpu_custom_call", output_to_operand_aliasing={{0}: (4, {}), {1}: (5, {})} | custom-call | flops 3221225472 | bytes 6000000 | tf_op jit(solution)/shard_map/pallas_call | solution.py:220
  56.9 2.6 %collective-permute-done.8.refs_1_ = bf16[2,264,256]{2,1,0:T(8,128)(2,1)S(1)} collective-permute-done((bf16[2,264,256]{2,1,0:T(8,128)(2,1)S(1)}, bf16[2,264,256]{2,1,0:T(8,128)(2,1)S(1)}, u32[]{:S(2)}, u32[]{:S(2)}) %collective-permute-start.8) | collective-permute-done | bytes 270368 | tf_op jit(solution)/shard_map/ppermute | solution.py:500
  59.5 4.3 %shard_map.148 = bf16[32,72,256]{2,1,0:T(8,128)(2,1)S(1)} custom-call(s32[4]{0:T(128)S(1)} %copy-done.8, bf16[8,264,256]{2,1,0:T(8,128)(2,1)S(1)} %all-to-all-done.refs_0_, bf16[2,264,256]{2,1,0:T(8,128)(2,1)S(1)} %collective-permute-done.8.refs_1_, f32[8,256,512]{2,1,0:T(8,128)S(1)} %get-tuple-element.39.refs_2_, f32[8,256,256]{2,1,0:T(8,128)S(1)} %get-tuple-element.40.refs_3_), custom_call_target="tpu_custom_call" | custom-call | flops 1610612736 | bytes 6000000 | tf_op jit(solution)/shard_map/pallas_call | solution.py:220
  63.9 0.0 copy-start.1
  63.9 0.0 copy-start.5
  63.9 0.0 copy-start.7
  63.9 24.2 %all_to_all.20.part_ref = bf16[32,72,256]{2,1,0:T(8,128)(2,1)S(1)} all-to-all(bf16[32,72,256]{2,1,0:T(8,128)(2,1)S(1)} %shard_map.148), channel_id=1, replica_groups=mesh['z'=8,'y'=4,'c'=2,'tp'=4] {'y','c','tp'}, dimensions={0} | all-to-all | bytes 2359296 | tf_op jit(solution)/shard_map/all_to_all | solution.py:517
  88.1 0.0 collective-permute-done.10.refs_3_
  88.1 0.0 collective-permute-done.9.refs_2_
  88.1 0.0 copy-done.6
  88.1 0.0 copy-done.1
  88.1 0.0 copy-done.5
  88.2 0.0 copy-done.7
  88.2 0.0 copy-start.4
  88.2 4.8 %post.1 = (bf16[64,2048]{1,0:T(8,128)(2,1)S(1)}, bf16[64,2048]{1,0:T(8,128)(2,1)S(1)}, bf16[64,8,2048]{2,1,0:T(8,128)(2,1)S(1)}) custom-call(s32[4]{0:T(128)S(1)} %copy-done.8, bf16[32,72,256]{2,1,0:T(8,128)(2,1)S(1)} %all_to_all.20.part_ref, bf16[512,2048]{1,0:T(8,128)(2,1)S(1)} %copy-done.1, bf16[512,2048]{1,0:T(8,128)(2,1)} %collective-permute-done.5.refs_1_, ...), custom_call_target="tpu_custom_call" | custom-call | tf_op jit(solution)/shard_map/post/pallas_call | solution.py:338
  93.0 0.0 copy-start.2
  93.0 0.0 copy-start.3
  93.0 59.6 %all_to_all.21.x_ref = bf16[64,8,2048]{2,1,0:T(8,128)(2,1)S(1)} all-to-all(bf16[64,8,2048]{2,1,0:T(8,128)(2,1)S(1)} %get-tuple-element.42), channel_id=1, replica_groups=mesh['z'=8,'y'=4,'c'=2,'tp'=4] {'z','y','c'}, dimensions={0} | all-to-all | bytes 4194304 | tf_op jit(solution)/shard_map/all_to_all | solution.py:529
  152.6 0.0 copy-done.4
  152.6 0.0 copy-done.2
  152.6 0.0 copy-done.3
  152.6 4.8 %expert.1 = bf16[64,8,2048]{2,1,0:T(8,128)(2,1)} custom-call(bf16[64,8,2048]{2,1,0:T(8,128)(2,1)S(1)} %all_to_all.21.x_ref, bf16[1,2048,384]{2,1,0:T(8,128)(2,1)S(1)} %copy-done.2, bf16[1,2048,384]{2,1,0:T(8,128)(2,1)S(1)} %copy-done.3, bf16[1,384,2048]{2,1,0:T(8,128)(2,1)S(1)} %copy-done.4), custom_call_target="tpu_custom_call" | custom-call | tf_op jit(solution)/shard_map/expert/pallas_call | solution.py:374
  157.3 5.8 %all-to-all-start.3 = ((bf16[64,8,2048]{2,1,0:T(8,128)(2,1)}), bf16[64,8,2048]{2,1,0:T(8,128)(2,1)}, u32[]{:S(2)}, u32[]{:S(2)}) async-start(bf16[64,8,2048]{2,1,0:T(8,128)(2,1)} %expert.1), calls=%async_computation.3 | async-start | bytes 4194304 | tf_op jit(solution)/shard_map/all_to_all | solution.py:536
  163.1 0.7 copy.20.ids_ref
  163.8 0.0 copy-done.11
  163.8 0.7 copy.21.route_ref
  164.5 1.9 mixing.1.mix_ref
  166.4 1.8 fusion.5
  168.1 0.0 copy-done
  168.1 3.1 %convert_add_fusion.base_ref = f32[64,2048]{1,0:T(8,128)} fusion(bf16[64,2048]{1,0:T(8,128)(2,1)S(1)} %get-tuple-element.43, bf16[384,2048]{1,0:T(8,128)(2,1)S(1)} %copy-done, f32[64,384]{1,0:T(8,128)S(1)} %fusion.5, bf16[64,2048]{1,0:T(8,128)(2,1)S(1)} %get-tuple-element.44, bf16[2048,384]{1,0:T(8,128)(2,1)} %param.28), kind=kOutput, calls=%fused_computation | convolution fusion | flops 201736192 | bytes 4292608 | tf_op jit(solution)/shard_map/dot_general | solution.py:534
  171.2 43.1 %all-to-all-done.3.res_ref = bf16[64,8,2048]{2,1,0:T(8,128)(2,1)} async-done(((bf16[64,8,2048]{2,1,0:T(8,128)(2,1)}), bf16[64,8,2048]{2,1,0:T(8,128)(2,1)}, u32[]{:S(2)}, u32[]{:S(2)}) %all-to-all-start.3) | async-done | bytes 2097184 | tf_op jit(solution)/shard_map/all_to_all | solution.py:536
  214.2 2.7 %finish.1 = bf16[64,2048]{1,0:T(8,128)(2,1)} custom-call(bf16[64,8,2048]{2,1,0:T(8,128)(2,1)} %all-to-all-done.3.res_ref, f32[64,2048]{1,0:T(8,128)} %convert_add_fusion.base_ref, bf16[128,512]{1,0:T(8,128)(2,1)} %mixing.1.mix_ref), custom_call_target="tpu_custom_call" | custom-call | tf_op jit(solution)/shard_map/finish/pallas_call | solution.py:444
  (4 shorter events, 0.0 us)
Async XLA Ops:
  0.0 168.1 %copy-start = (bf16[384,2048]{1,0:T(8,128)(2,1)S(1)}, bf16[384,2048]{1,0:T(8,128)(2,1)}, u32[]{:S(2)}) copy-start(bf16[384,2048]{1,0:T(8,128)(2,1)} %param.29) | copy-start | bytes 4718596
  0.0 38.5 %collective-permute-start.5 = (bf16[512,2048]{1,0:T(8,128)(2,1)}, bf16[512,2048]{1,0:T(8,128)(2,1)}, u32[]{:S(2)}, u32[]{:S(2)}) collective-permute-start(bf16[512,2048]{1,0:T(8,128)(2,1)} %refs_0_.1), channel_id=1, source_target_pairs={{0,1},{1,2},{2,3},{3,0},{4,7},{5,4},{6,5},{7,6},{8,9},{9,10},{10,1... | collective-permute-start | bytes 6291464 | tf_op jit(solution)/shard_map/ppermute | solution.py:497
  3.8 7.6 %copy-start.9 = (bf16[264,256]{1,0:T(8,128)(2,1)S(1)}, bf16[264,256]{1,0:T(8,128)(2,1)}, u32[]{:S(2)}) copy-start(bf16[264,256]{1,0:T(8,128)(2,1)} %get-tuple-element.25._) | copy-start | bytes 405508
  3.8 8.9 %copy-start.10 = (bf16[264,256]{1,0:T(8,128)(2,1)S(1)}, bf16[264,256]{1,0:T(8,128)(2,1)}, u32[]{:S(2)}) copy-start(bf16[264,256]{1,0:T(8,128)(2,1)} %get-tuple-element.26) | copy-start | bytes 405508
  5.9 23.2 %copy-start.8 = (s32[4]{0:T(128)S(1)}, s32[4]{0:T(128)}, u32[]{:S(2)}) copy-start(s32[4]{0:T(128)} %pad_add_fusion.info) | copy-start | bytes 52
  5.9 23.2 %all-to-all-start = ((bf16[8,264,256]{2,1,0:T(8,128)(2,1)}), bf16[8,264,256]{2,1,0:T(8,128)(2,1)S(1)}, u32[]{:S(2)}, u32[]{:S(2)}) async-start(bf16[8,264,256]{2,1,0:T(8,128)(2,1)} %pack_queries.1), calls=%async_computation | async-start | bytes 2162688 | tf_op jit(solution)/shard_map/all_to_all | solution.py:494
  11.4 1.4 collective-permute-start
  12.8 13.1 %collective-permute-start.1 = (bf16[2,264,256]{2,1,0:T(8,128)(2,1)S(1)}, bf16[2,264,256]{2,1,0:T(8,128)(2,1)}, u32[]{:S(2)}, u32[]{:S(2)}) collective-permute-start(bf16[2,264,256]{2,1,0:T(8,128)(2,1)S(1)} %pad_maximum_fusion.refs_1_), channel_id=1, source_target_pairs={{0,32},{32,64},{64,96},{96,128},{128,160},{160,192},{192,224},{224... | collective-permute-start | bytes 811016 | tf_op jit(solution)/shard_map/ppermute | solution.py:500
  14.8 11.1 %collective-permute-start.2 = (bf16[2,264,256]{2,1,0:T(8,128)(2,1)S(1)}, bf16[2,264,256]{2,1,0:T(8,128)(2,1)}, u32[]{:S(2)}, u32[]{:S(2)}) collective-permute-start(bf16[2,264,256]{2,1,0:T(8,128)(2,1)S(1)} %pad_maximum_fusion.refs_1_), channel_id=1, source_target_pairs={{0,224},{32,0},{64,32},{96,64},{128,96},{160,128},{192,160},{224,1... | collective-permute-start | bytes 811016 | tf_op jit(solution)/shard_map/ppermute | solution.py:503
  25.8 12.7 %collective-permute-start.3 = (bf16[2,264,256]{2,1,0:T(8,128)(2,1)}, bf16[2,264,256]{2,1,0:T(8,128)(2,1)S(1)}, u32[]{:S(2)}, u32[]{:S(2)}) collective-permute-start(bf16[2,264,256]{2,1,0:T(8,128)(2,1)} %collective-permute-done.1.refs_2_), channel_id=1, source_target_pairs={{0,32},{32,64},{64,96},{96,128},{128,160},{160,192},{192,224},{224... | collective-permute-start | bytes 811016 | tf_op jit(solution)/shard_map/ppermute | solution.py:500
  25.9 12.7 %collective-permute-start.4 = (bf16[2,264,256]{2,1,0:T(8,128)(2,1)}, bf16[2,264,256]{2,1,0:T(8,128)(2,1)S(1)}, u32[]{:S(2)}, u32[]{:S(2)}) collective-permute-start(bf16[2,264,256]{2,1,0:T(8,128)(2,1)} %collective-permute-done.2.refs_3_), channel_id=1, source_target_pairs={{0,224},{32,0},{64,32},{96,64},{128,96},{160,128},{192,160},{224,1... | collective-permute-start | bytes 811016 | tf_op jit(solution)/shard_map/ppermute | solution.py:503
  38.5 49.6 %collective-permute-start.10 = (bf16[512,2048]{1,0:T(8,128)(2,1)}, bf16[512,2048]{1,0:T(8,128)(2,1)S(1)}, u32[]{:S(2)}, u32[]{:S(2)}) collective-permute-start(bf16[512,2048]{1,0:T(8,128)(2,1)} %collective-permute-done.5.refs_1_), channel_id=1, source_target_pairs={{0,1},{1,2},{2,3},{3,0},{4,7},{5,4},{6,5},{7,6},{8,9},{9,10},{10,1... | collective-permute-start | bytes 6291464 | tf_op jit(solution)/shard_map/ppermute | solution.py:510
  39.7 48.4 %collective-permute-start.9 = (bf16[512,2048]{1,0:T(8,128)(2,1)}, bf16[512,2048]{1,0:T(8,128)(2,1)S(1)}, u32[]{:S(2)}, u32[]{:S(2)}) collective-permute-start(bf16[512,2048]{1,0:T(8,128)(2,1)} %collective-permute-done.5.refs_1_), channel_id=1, source_target_pairs={{0,4},{4,0},{1,5},{5,1},{2,6},{6,2},{3,7},{7,3},{8,12},{12,8},{9,1... | collective-permute-start | bytes 6291464 | tf_op jit(solution)/shard_map/ppermute | solution.py:514
  39.7 10.2 %collective-permute-start.6 = (bf16[2,264,256]{2,1,0:T(8,128)(2,1)S(1)}, bf16[2,264,256]{2,1,0:T(8,128)(2,1)S(1)}, u32[]{:S(2)}, u32[]{:S(2)}) collective-permute-start(bf16[2,264,256]{2,1,0:T(8,128)(2,1)S(1)} %collective-permute-done.3.refs_1_), channel_id=1, source_target_pairs={{0,32},{32,64},{64,96},{96,128},{128,160},{160,192},{192,224},{224... | collective-permute-start | bytes 811016 | tf_op jit(solution)/shard_map/ppermute | solution.py:500
  39.7 10.2 %collective-permute-start.7 = (bf16[2,264,256]{2,1,0:T(8,128)(2,1)S(1)}, bf16[2,264,256]{2,1,0:T(8,128)(2,1)S(1)}, u32[]{:S(2)}, u32[]{:S(2)}) collective-permute-start(bf16[2,264,256]{2,1,0:T(8,128)(2,1)S(1)} %collective-permute-done.4.refs_2_), channel_id=1, source_target_pairs={{0,224},{32,0},{64,32},{96,64},{128,96},{160,128},{192,160},{224,1... | collective-permute-start | bytes 811016 | tf_op jit(solution)/shard_map/ppermute | solution.py:503
  49.9 9.6 %collective-permute-start.8 = (bf16[2,264,256]{2,1,0:T(8,128)(2,1)S(1)}, bf16[2,264,256]{2,1,0:T(8,128)(2,1)S(1)}, u32[]{:S(2)}, u32[]{:S(2)}) collective-permute-start(bf16[2,264,256]{2,1,0:T(8,128)(2,1)S(1)} %collective-permute-done.6.refs_1_), channel_id=1, source_target_pairs={{0,32},{32,64},{64,96},{96,128},{128,160},{160,192},{192,224},{224... | collective-permute-start | bytes 811016 | tf_op jit(solution)/shard_map/ppermute | solution.py:500
  59.5 28.6 %copy-start.6 = (f32[2048]{0:T(1024)S(1)}, f32[2048]{0:T(1024)}, u32[]{:S(2)}) copy-start(f32[2048]{0:T(1024)} %param.21) | copy-start | bytes 24580
  63.9 24.3 %copy-start.1 = (bf16[512,2048]{1,0:T(8,128)(2,1)S(1)}, bf16[512,2048]{1,0:T(8,128)(2,1)}, u32[]{:S(2)}) copy-start(bf16[512,2048]{1,0:T(8,128)(2,1)} %refs_0_.1) | copy-start | bytes 6291460
  63.9 24.3 %copy-start.5 = (bf16[64,2048]{1,0:T(8,128)(2,1)S(1)}, bf16[64,2048]{1,0:T(8,128)(2,1)}, u32[]{:S(2)}) copy-start(bf16[64,2048]{1,0:T(8,128)(2,1)} %refs_4_.1) | copy-start | bytes 786436
  63.9 24.3 %copy-start.7 = (s32[64,4]{0,1:T(4,128)S(1)}, s32[64,4]{0,1:T(4,128)}, u32[]{:S(2)}) copy-start(s32[64,4]{0,1:T(4,128)} %param.22) | copy-start | bytes 3076
  88.2 64.4 %copy-start.4 = (bf16[1,384,2048]{2,1,0:T(8,128)(2,1)S(1)}, bf16[1,384,2048]{2,1,0:T(8,128)(2,1)}, u32[]{:S(2)}) copy-start(bf16[1,384,2048]{2,1,0:T(8,128)(2,1)} %down_ref.1) | copy-start | bytes 4718596
  93.0 59.6 %copy-start.2 = (bf16[1,2048,384]{2,1,0:T(8,128)(2,1)S(1)}, bf16[1,2048,384]{2,1,0:T(8,128)(2,1)}, u32[]{:S(2)}) copy-start(bf16[1,2048,384]{2,1,0:T(8,128)(2,1)} %gate_ref.1) | copy-start | bytes 4718596
  93.0 59.6 %copy-start.3 = (bf16[1,2048,384]{2,1,0:T(8,128)(2,1)S(1)}, bf16[1,2048,384]{2,1,0:T(8,128)(2,1)}, u32[]{:S(2)}) copy-start(bf16[1,2048,384]{2,1,0:T(8,128)(2,1)} %up_ref.1) | copy-start | bytes 4718596
  157.3 6.5 %copy-start.11 = (f32[64,4]{0,1:T(4,128)S(1)}, f32[64,4]{0,1:T(4,128)}, u32[]{:S(2)}) copy-start(f32[64,4]{0,1:T(4,128)} %param.23) | copy-start | bytes 3076
  157.3 56.9 %all-to-all-start.3 = ((bf16[64,8,2048]{2,1,0:T(8,128)(2,1)}), bf16[64,8,2048]{2,1,0:T(8,128)(2,1)}, u32[]{:S(2)}, u32[]{:S(2)}) async-start(bf16[64,8,2048]{2,1,0:T(8,128)(2,1)} %expert.1), calls=%async_computation.3 | async-start | bytes 4194304 | tf_op jit(solution)/shard_map/all_to_all | solution.py:536

commit v6 on v5

--- a/solution.py
+++ b/solution.py
@@ -357,34 +357,33 @@
     )(info, parts, *weights, residual, gain, ids_t)
 
 
-def expert_kernel(x_ref, gate_ref, up_ref, down_ref, out_ref):
+def expert_kernel(x_ref, gate_ref, up_ref, down_ref, out_ref, staged, sems, *, steps):
     peers, cap, width = x_ref.shape
-    x = x_ref[...].reshape(peers * cap, width)
-    gate = jnp.dot(x, gate_ref[0], preferred_element_type=F32)
-    up = jnp.dot(x, up_ref[0], preferred_element_type=F32)
-    hidden = (gate / (1.0 + jnp.exp(-gate)) * up).astype(BF)
-    out = jnp.dot(hidden, down_ref[0], preferred_element_type=F32).astype(BF)
-    out_ref[...] = out.reshape(peers, cap, width)
+    part = peers // steps
+    copies = []
+    for n in range(steps):
+        rows = pl.ds(n * part, part)
+        x = x_ref[rows].reshape(part * cap, width)
+        gate = jnp.dot(x, gate_ref[0], preferred_element_type=F32)
+        up = jnp.dot(x, up_ref[0], preferred_element_type=F32)
+        hidden = (gate / (1.0 + jnp.exp(-gate)) * up).astype(BF)
+        out = jnp.dot(hidden, down_ref[0], preferred_element_type=F32).astype(BF)
+        staged[rows] = out.reshape(part, cap, width)
+        copies.append(pltpu.make_async_copy(staged.at[rows], out_ref.at[rows], sems.at[n]))
+        copies[-1].start()
+    for copy in copies:
+        copy.wait()
 
 
 def expert(arrived, gate, up, down, steps=2):
-    peers, cap, width = arrived.shape
-    rows = pl.BlockSpec((peers // steps, cap, width), lambda g: (g, 0, 0))
-    whole = lambda g: (0, 0, 0)
-    return pl.pallas_call(
-        expert_kernel,
-        grid=(steps,),
-        in_specs=[
-            rows,
-            pl.BlockSpec(gate.shape, whole),
-            pl.BlockSpec(up.shape, whole),
-            pl.BlockSpec(down.shape, whole),
-        ],
-        out_specs=rows,
+    vmem = pl.BlockSpec(memory_space=pltpu.VMEM)
+    return pl.pallas_call(
+        functools.partial(expert_kernel, steps=steps),
+        in_specs=[vmem] * 4,
+        out_specs=pl.BlockSpec(memory_space=pltpu.HBM),
         out_shape=pltpu.HBM(arrived.shape, BF),
-        compiler_params=pltpu.CompilerParams(
-            dimension_semantics=("arbitrary",), vmem_limit_bytes=40 * 1024 * 1024
-        ),
+        scratch_shapes=[pltpu.VMEM(arrived.shape, BF), pltpu.SemaphoreType.DMA((steps,))],
+        compiler_params=pltpu.CompilerParams(vmem_limit_bytes=32 * 1024 * 1024),
         name="expert",
     )(arrived, gate, up, down)
 
@@ -513,7 +512,7 @@
     up4 = up(up3)
     w_other = lax.ppermute(w_near, "c", [(0, 1), (1, 0)])
     state = attend(info, q_all, [up3, down3], (3, -3), z_count, state, False)
-    sent = attend(info, q_all, [up4], (4,), z_count, state, True)
+    sent = attend(info, q_all, [up4], (4,), z_count, state, True, tiles=8)
     parts = lax.all_to_all(sent, ("y", "c", "tp"), split_axis=0, concat_axis=0)
     weights = [out_weight, w_near, w_other, w_far]
     stream, normed, outgoing = post(

time: 217 us -> 217 us (level)
  no operation moved by 1% of the time
where the time goes in v6:
time: 217 us; the launch traced here: 216 us
  blocking collectives  83.8 us (39%)
  waiting for transfers between devices  54 us (25%)
  Pallas kernels  45 us (21%)
  starting transfers between devices  26.4 us (12%)
  matrix products  4.82 us (2%)
    all_to_all x1, blocking collectives, local(): lax.all_to_all(outgoing, ('z', 'y', 'c'), split_axis=0, concat_axis=0)  59.6 us
    all_to_all x1, waiting for transfers between devices, local(): lax.all_to_all(processed, ('z', 'y', 'c'), split_axis=0, concat_axis=0)  43.1 us
    pallas_call x4, Pallas kernels, attend(): pl.pallas_call(functools.partial(attend_kernel, steps=steps, z_count=z_co...  27.3 us
    all_to_all x1, blocking collectives, local(): parts = lax.all_to_all(sent, ('y', 'c', 'tp'), split_axis=0, concat_axis=0)  24.2 us
    ppermute x3, starting transfers between devices, down(): return lax.ppermute(block, 'z', down_ring)  10.5 us
    ppermute x4, waiting for transfers between devices, up(): return lax.ppermute(block, 'z', up_ring)  9.66 us
    all_to_all x1, starting transfers between devices, local(): lax.all_to_all(processed, ('z', 'y', 'c'), split_axis=0, concat_axis=0)  5.64 us
    all_to_all x1, starting transfers between devices, local(): q_all = lax.all_to_all(q_send, ('y', 'c'), split_axis=0, concat_axis=0)  5.47 us
  transfers between devices with their start and end apart: 13, of which 4 were waited for; matrix products, arithmetic and copies ran while one was open for 3% of the time, Pallas kernels for 15%

profile of v6, /device:TPU:8, one launch (start us, length us, event | category | flops | bytes accessed | tf_op | source)
XLA Modules:
  0.0 216.4 jit_solution(13195545474994240177)
XLA Ops:
  0.0 0.0 copy-start
  0.0 1.5 collective-permute-start.5
  1.5 0.6 pad_add_fusion.info
  2.1 1.7 pack_keys.1
  3.8 0.0 copy-start.9
  3.8 2.1 pack_queries.1
  5.9 5.5 %all-to-all-start = ((bf16[8,264,256]{2,1,0:T(8,128)(2,1)}), bf16[8,264,256]{2,1,0:T(8,128)(2,1)S(1)}, u32[]{:S(2)}, u32[]{:S(2)}) async-start(bf16[8,264,256]{2,1,0:T(8,128)(2,1)} %pack_queries.1), calls=%async_computation | async-start | bytes 2162688 | tf_op jit(solution)/shard_map/all_to_all | solution.py:493
  11.4 0.0 copy-done.9
  11.4 0.1 collective-permute-start
  11.5 1.3 collective-permute-done
  12.8 0.0 copy-done.10
  12.8 2.0 collective-permute-start.1
  14.8 4.0 %collective-permute-start.2 = (bf16[2,264,256]{2,1,0:T(8,128)(2,1)S(1)}, bf16[2,264,256]{2,1,0:T(8,128)(2,1)}, u32[]{:S(2)}, u32[]{:S(2)}) collective-permute-start(bf16[2,264,256]{2,1,0:T(8,128)(2,1)S(1)} %pad_maximum_fusion.refs_1_), channel_id=1, source_target_pairs={{0,224},{32,0},{64,32},{96,64},{128,96},{160,128},{192,160},{224,1... | collective-permute-start | bytes 811016 | tf_op jit(solution)/shard_map/ppermute | solution.py:502
  18.8 7.0 %collective-permute-done.1.refs_2_ = bf16[2,264,256]{2,1,0:T(8,128)(2,1)} collective-permute-done((bf16[2,264,256]{2,1,0:T(8,128)(2,1)S(1)}, bf16[2,264,256]{2,1,0:T(8,128)(2,1)}, u32[]{:S(2)}, u32[]{:S(2)}) %collective-permute-start.1) | collective-permute-done | bytes 270368 | tf_op jit(solution)/shard_map/ppermute | solution.py:499
  25.8 0.0 collective-permute-start.3
  25.8 0.0 collective-permute-done.2.refs_3_
  25.9 3.2 %collective-permute-start.4 = (bf16[2,264,256]{2,1,0:T(8,128)(2,1)}, bf16[2,264,256]{2,1,0:T(8,128)(2,1)S(1)}, u32[]{:S(2)}, u32[]{:S(2)}) collective-permute-start(bf16[2,264,256]{2,1,0:T(8,128)(2,1)} %collective-permute-done.2.refs_3_), channel_id=1, source_target_pairs={{0,224},{32,0},{64,32},{96,64},{128,96},{160,128},{192,160},{224,1... | collective-permute-start | bytes 811016 | tf_op jit(solution)/shard_map/ppermute | solution.py:502
  29.1 0.0 all-to-all-done.refs_0_
  29.1 0.0 copy-done.8
  29.1 9.4 %shard_map.145 = (f32[8,256,512]{2,1,0:T(8,128)S(1)}, f32[8,256,256]{2,1,0:T(8,128)S(1)}) custom-call(s32[4]{0:T(128)S(1)} %copy-done.8, bf16[8,264,256]{2,1,0:T(8,128)(2,1)S(1)} %all-to-all-done.refs_0_, bf16[2,264,256]{2,1,0:T(8,128)(2,1)S(1)} %pad_maximum_fusion.refs_1_, bf16[2,264,256]{2,1,0:T(8,128)(2,1)} %collective-permute-done.1.refs_2_, ...), custom_call_target="tpu_custom_call" | custom-call | flops 4831838208 | bytes 6000000 | tf_op jit(solution)/shard_map/pallas_call | solution.py:220
  38.5 0.0 collective-permute-done.3.refs_1_
  38.5 0.0 collective-permute-done.4.refs_2_
  38.5 0.0 collective-permute-done.5.refs_1_
  38.5 1.1 collective-permute-start.10
  39.7 0.0 collective-permute-start.9
  39.7 0.0 collective-permute-start.6
  39.7 3.2 %collective-permute-start.7 = (bf16[2,264,256]{2,1,0:T(8,128)(2,1)S(1)}, bf16[2,264,256]{2,1,0:T(8,128)(2,1)S(1)}, u32[]{:S(2)}, u32[]{:S(2)}) collective-permute-start(bf16[2,264,256]{2,1,0:T(8,128)(2,1)S(1)} %collective-permute-done.4.refs_2_), channel_id=1, source_target_pairs={{0,224},{32,0},{64,32},{96,64},{128,96},{160,128},{192,160},{224,1... | collective-permute-start | bytes 811016 | tf_op jit(solution)/shard_map/ppermute | solution.py:502
  42.9 6.9 %shard_map.146 = (f32[8,256,512]{2,1,0:T(8,128)S(1)}, f32[8,256,256]{2,1,0:T(8,128)S(1)}) custom-call(s32[4]{0:T(128)S(1)} %copy-done.8, bf16[8,264,256]{2,1,0:T(8,128)(2,1)S(1)} %all-to-all-done.refs_0_, bf16[2,264,256]{2,1,0:T(8,128)(2,1)S(1)} %collective-permute-done.3.refs_1_, ...), custom_call_target="tpu_custom_call", output_to_operand_aliasing={{0}: (4, {}), {1}: (5, {})} | custom-call | flops 3221225472 | bytes 6000000 | tf_op jit(solution)/shard_map/pallas_call | solution.py:220
  49.9 0.0 collective-permute-done.6.refs_1_
  49.9 0.0 collective-permute-done.7.refs_2_
  49.9 0.1 collective-permute-start.8
  50.0 6.9 %shard_map.147 = (f32[8,256,512]{2,1,0:T(8,128)S(1)}, f32[8,256,256]{2,1,0:T(8,128)S(1)}) custom-call(s32[4]{0:T(128)S(1)} %copy-done.8, bf16[8,264,256]{2,1,0:T(8,128)(2,1)S(1)} %all-to-all-done.refs_0_, bf16[2,264,256]{2,1,0:T(8,128)(2,1)S(1)} %collective-permute-done.6.refs_1_, ...), custom_call_target="tpu_custom_call", output_to_operand_aliasing={{0}: (4, {}), {1}: (5, {})} | custom-call | flops 3221225472 | bytes 6000000 | tf_op jit(solution)/shard_map/pallas_call | solution.py:220
  56.9 2.6 %collective-permute-done.8.refs_1_ = bf16[2,264,256]{2,1,0:T(8,128)(2,1)S(1)} collective-permute-done((bf16[2,264,256]{2,1,0:T(8,128)(2,1)S(1)}, bf16[2,264,256]{2,1,0:T(8,128)(2,1)S(1)}, u32[]{:S(2)}, u32[]{:S(2)}) %collective-permute-start.8) | collective-permute-done | bytes 270368 | tf_op jit(solution)/shard_map/ppermute | solution.py:499
  59.5 4.0 %shard_map.148 = bf16[32,72,256]{2,1,0:T(8,128)(2,1)S(1)} custom-call(s32[4]{0:T(128)S(1)} %copy-done.8, bf16[8,264,256]{2,1,0:T(8,128)(2,1)S(1)} %all-to-all-done.refs_0_, bf16[2,264,256]{2,1,0:T(8,128)(2,1)S(1)} %collective-permute-done.8.refs_1_, f32[8,256,512]{2,1,0:T(8,128)S(1)} %get-tuple-element.39.refs_2_, f32[8,256,256]{2,1,0:T(8,128)S(1)} %get-tuple-element.40.refs_3_), custom_call_target="tpu_custom_call" | custom-call | flops 1610612736 | bytes 6000000 | tf_op jit(solution)/shard_map/pallas_call | solution.py:220
  63.5 0.0 copy-start.1
  63.6 0.0 copy-start.5
  63.6 0.0 copy-start.7
  63.6 24.2 %all_to_all.20.part_ref = bf16[32,72,256]{2,1,0:T(8,128)(2,1)S(1)} all-to-all(bf16[32,72,256]{2,1,0:T(8,128)(2,1)S(1)} %shard_map.148), channel_id=1, replica_groups=mesh['z'=8,'y'=4,'c'=2,'tp'=4] {'y','c','tp'}, dimensions={0} | all-to-all | bytes 2359296 | tf_op jit(solution)/shard_map/all_to_all | solution.py:516
  87.8 0.0 collective-permute-done.10.refs_3_
  87.8 0.0 collective-permute-done.9.refs_2_
  87.8 0.0 copy-done.6
  87.8 0.0 copy-done.1
  87.8 0.0 copy-done.5
  87.8 0.0 copy-done.7
  87.8 0.0 copy-start.4
  87.9 4.8 %post.1 = (bf16[64,2048]{1,0:T(8,128)(2,1)S(1)}, bf16[64,2048]{1,0:T(8,128)(2,1)S(1)}, bf16[64,8,2048]{2,1,0:T(8,128)(2,1)S(1)}) custom-call(s32[4]{0:T(128)S(1)} %copy-done.8, bf16[32,72,256]{2,1,0:T(8,128)(2,1)S(1)} %all_to_all.20.part_ref, bf16[512,2048]{1,0:T(8,128)(2,1)S(1)} %copy-done.1, bf16[512,2048]{1,0:T(8,128)(2,1)} %collective-permute-done.5.refs_1_, ...), custom_call_target="tpu_custom_call" | custom-call | tf_op jit(solution)/shard_map/post/pallas_call | solution.py:338
  92.7 0.0 copy-start.2
  92.7 0.0 copy-start.3
  92.7 59.6 %all_to_all.21.x_ref = bf16[64,8,2048]{2,1,0:T(8,128)(2,1)S(1)} all-to-all(bf16[64,8,2048]{2,1,0:T(8,128)(2,1)S(1)} %get-tuple-element.42), channel_id=1, replica_groups=mesh['z'=8,'y'=4,'c'=2,'tp'=4] {'z','y','c'}, dimensions={0} | all-to-all | bytes 4194304 | tf_op jit(solution)/shard_map/all_to_all | solution.py:528
  152.3 0.0 copy-done.4
  152.3 0.0 copy-done.2
  152.3 0.0 copy-done.3
  152.3 4.6 %expert.1 = bf16[64,8,2048]{2,1,0:T(8,128)(2,1)} custom-call(bf16[64,8,2048]{2,1,0:T(8,128)(2,1)S(1)} %all_to_all.21.x_ref, bf16[1,2048,384]{2,1,0:T(8,128)(2,1)S(1)} %copy-done.2, bf16[1,2048,384]{2,1,0:T(8,128)(2,1)S(1)} %copy-done.3, bf16[1,384,2048]{2,1,0:T(8,128)(2,1)S(1)} %copy-done.4), custom_call_target="tpu_custom_call" | custom-call | tf_op jit(solution)/shard_map/expert/pallas_call | solution.py:380
  156.9 0.0 copy-start.11
  156.9 5.6 %all-to-all-start.3 = ((bf16[64,8,2048]{2,1,0:T(8,128)(2,1)}), bf16[64,8,2048]{2,1,0:T(8,128)(2,1)}, u32[]{:S(2)}, u32[]{:S(2)}) async-start(bf16[64,8,2048]{2,1,0:T(8,128)(2,1)} %expert.1), calls=%async_computation.3 | async-start | bytes 4194304 | tf_op jit(solution)/shard_map/all_to_all | solution.py:535
  162.5 0.7 copy.20.ids_ref
  163.2 0.0 copy-done.11
  163.2 0.7 copy.21.route_ref
  163.9 1.9 mixing.1.mix_ref
  165.8 1.8 fusion.5
  167.6 0.0 copy-done
  167.6 3.1 %convert_add_fusion.base_ref = f32[64,2048]{1,0:T(8,128)} fusion(bf16[64,2048]{1,0:T(8,128)(2,1)S(1)} %get-tuple-element.43, bf16[384,2048]{1,0:T(8,128)(2,1)S(1)} %copy-done, f32[64,384]{1,0:T(8,128)S(1)} %fusion.5, bf16[64,2048]{1,0:T(8,128)(2,1)S(1)} %get-tuple-element.44, bf16[2048,384]{1,0:T(8,128)(2,1)} %param.28), kind=kOutput, calls=%fused_computation | convolution fusion | flops 201736192 | bytes 4292608 | tf_op jit(solution)/shard_map/dot_general | solution.py:533
  170.6 43.1 %all-to-all-done.3.res_ref = bf16[64,8,2048]{2,1,0:T(8,128)(2,1)} async-done(((bf16[64,8,2048]{2,1,0:T(8,128)(2,1)}), bf16[64,8,2048]{2,1,0:T(8,128)(2,1)}, u32[]{:S(2)}, u32[]{:S(2)}) %all-to-all-start.3) | async-done | bytes 2097184 | tf_op jit(solution)/shard_map/all_to_all | solution.py:535
  213.7 2.7 %finish.1 = bf16[64,2048]{1,0:T(8,128)(2,1)} custom-call(bf16[64,8,2048]{2,1,0:T(8,128)(2,1)} %all-to-all-done.3.res_ref, f32[64,2048]{1,0:T(8,128)} %convert_add_fusion.base_ref, bf16[128,512]{1,0:T(8,128)(2,1)} %mixing.1.mix_ref), custom_call_target="tpu_custom_call" | custom-call | tf_op jit(solution)/shard_map/finish/pallas_call | solution.py:443
  (4 shorter events, 0.0 us)
Async XLA Ops:
  0.0 167.6 %copy-start = (bf16[384,2048]{1,0:T(8,128)(2,1)S(1)}, bf16[384,2048]{1,0:T(8,128)(2,1)}, u32[]{:S(2)}) copy-start(bf16[384,2048]{1,0:T(8,128)(2,1)} %param.29) | copy-start | bytes 4718596
  0.0 38.5 %collective-permute-start.5 = (bf16[512,2048]{1,0:T(8,128)(2,1)}, bf16[512,2048]{1,0:T(8,128)(2,1)}, u32[]{:S(2)}, u32[]{:S(2)}) collective-permute-start(bf16[512,2048]{1,0:T(8,128)(2,1)} %refs_0_.1), channel_id=1, source_target_pairs={{0,1},{1,2},{2,3},{3,0},{4,7},{5,4},{6,5},{7,6},{8,9},{9,10},{10,1... | collective-permute-start | bytes 6291464 | tf_op jit(solution)/shard_map/ppermute | solution.py:496
  3.8 7.6 %copy-start.9 = (bf16[264,256]{1,0:T(8,128)(2,1)S(1)}, bf16[264,256]{1,0:T(8,128)(2,1)}, u32[]{:S(2)}) copy-start(bf16[264,256]{1,0:T(8,128)(2,1)} %get-tuple-element.25._) | copy-start | bytes 405508
  3.8 8.9 %copy-start.10 = (bf16[264,256]{1,0:T(8,128)(2,1)S(1)}, bf16[264,256]{1,0:T(8,128)(2,1)}, u32[]{:S(2)}) copy-start(bf16[264,256]{1,0:T(8,128)(2,1)} %get-tuple-element.26) | copy-start | bytes 405508
  5.9 23.2 %copy-start.8 = (s32[4]{0:T(128)S(1)}, s32[4]{0:T(128)}, u32[]{:S(2)}) copy-start(s32[4]{0:T(128)} %pad_add_fusion.info) | copy-start | bytes 52
  5.9 23.2 %all-to-all-start = ((bf16[8,264,256]{2,1,0:T(8,128)(2,1)}), bf16[8,264,256]{2,1,0:T(8,128)(2,1)S(1)}, u32[]{:S(2)}, u32[]{:S(2)}) async-start(bf16[8,264,256]{2,1,0:T(8,128)(2,1)} %pack_queries.1), calls=%async_computation | async-start | bytes 2162688 | tf_op jit(solution)/shard_map/all_to_all | solution.py:493
  11.4 1.4 collective-permute-start
  12.8 13.1 %collective-permute-start.1 = (bf16[2,264,256]{2,1,0:T(8,128)(2,1)S(1)}, bf16[2,264,256]{2,1,0:T(8,128)(2,1)}, u32[]{:S(2)}, u32[]{:S(2)}) collective-permute-start(bf16[2,264,256]{2,1,0:T(8,128)(2,1)S(1)} %pad_maximum_fusion.refs_1_), channel_id=1, source_target_pairs={{0,32},{32,64},{64,96},{96,128},{128,160},{160,192},{192,224},{224... | collective-permute-start | bytes 811016 | tf_op jit(solution)/shard_map/ppermute | solution.py:499
  14.8 11.1 %collective-permute-start.2 = (bf16[2,264,256]{2,1,0:T(8,128)(2,1)S(1)}, bf16[2,264,256]{2,1,0:T(8,128)(2,1)}, u32[]{:S(2)}, u32[]{:S(2)}) collective-permute-start(bf16[2,264,256]{2,1,0:T(8,128)(2,1)S(1)} %pad_maximum_fusion.refs_1_), channel_id=1, source_target_pairs={{0,224},{32,0},{64,32},{96,64},{128,96},{160,128},{192,160},{224,1... | collective-permute-start | bytes 811016 | tf_op jit(solution)/shard_map/ppermute | solution.py:502
  25.8 12.7 %collective-permute-start.3 = (bf16[2,264,256]{2,1,0:T(8,128)(2,1)}, bf16[2,264,256]{2,1,0:T(8,128)(2,1)S(1)}, u32[]{:S(2)}, u32[]{:S(2)}) collective-permute-start(bf16[2,264,256]{2,1,0:T(8,128)(2,1)} %collective-permute-done.1.refs_2_), channel_id=1, source_target_pairs={{0,32},{32,64},{64,96},{96,128},{128,160},{160,192},{192,224},{224... | collective-permute-start | bytes 811016 | tf_op jit(solution)/shard_map/ppermute | solution.py:499
  25.9 12.7 %collective-permute-start.4 = (bf16[2,264,256]{2,1,0:T(8,128)(2,1)}, bf16[2,264,256]{2,1,0:T(8,128)(2,1)S(1)}, u32[]{:S(2)}, u32[]{:S(2)}) collective-permute-start(bf16[2,264,256]{2,1,0:T(8,128)(2,1)} %collective-permute-done.2.refs_3_), channel_id=1, source_target_pairs={{0,224},{32,0},{64,32},{96,64},{128,96},{160,128},{192,160},{224,1... | collective-permute-start | bytes 811016 | tf_op jit(solution)/shard_map/ppermute | solution.py:502
  38.5 49.3 %collective-permute-start.10 = (bf16[512,2048]{1,0:T(8,128)(2,1)}, bf16[512,2048]{1,0:T(8,128)(2,1)S(1)}, u32[]{:S(2)}, u32[]{:S(2)}) collective-permute-start(bf16[512,2048]{1,0:T(8,128)(2,1)} %collective-permute-done.5.refs_1_), channel_id=1, source_target_pairs={{0,1},{1,2},{2,3},{3,0},{4,7},{5,4},{6,5},{7,6},{8,9},{9,10},{10,1... | collective-permute-start | bytes 6291464 | tf_op jit(solution)/shard_map/ppermute | solution.py:509
  39.7 48.1 %collective-permute-start.9 = (bf16[512,2048]{1,0:T(8,128)(2,1)}, bf16[512,2048]{1,0:T(8,128)(2,1)S(1)}, u32[]{:S(2)}, u32[]{:S(2)}) collective-permute-start(bf16[512,2048]{1,0:T(8,128)(2,1)} %collective-permute-done.5.refs_1_), channel_id=1, source_target_pairs={{0,4},{4,0},{1,5},{5,1},{2,6},{6,2},{3,7},{7,3},{8,12},{12,8},{9,1... | collective-permute-start | bytes 6291464 | tf_op jit(solution)/shard_map/ppermute | solution.py:513
  39.7 10.2 %collective-permute-start.6 = (bf16[2,264,256]{2,1,0:T(8,128)(2,1)S(1)}, bf16[2,264,256]{2,1,0:T(8,128)(2,1)S(1)}, u32[]{:S(2)}, u32[]{:S(2)}) collective-permute-start(bf16[2,264,256]{2,1,0:T(8,128)(2,1)S(1)} %collective-permute-done.3.refs_1_), channel_id=1, source_target_pairs={{0,32},{32,64},{64,96},{96,128},{128,160},{160,192},{192,224},{224... | collective-permute-start | bytes 811016 | tf_op jit(solution)/shard_map/ppermute | solution.py:499
  39.7 10.2 %collective-permute-start.7 = (bf16[2,264,256]{2,1,0:T(8,128)(2,1)S(1)}, bf16[2,264,256]{2,1,0:T(8,128)(2,1)S(1)}, u32[]{:S(2)}, u32[]{:S(2)}) collective-permute-start(bf16[2,264,256]{2,1,0:T(8,128)(2,1)S(1)} %collective-permute-done.4.refs_2_), channel_id=1, source_target_pairs={{0,224},{32,0},{64,32},{96,64},{128,96},{160,128},{192,160},{224,1... | collective-permute-start | bytes 811016 | tf_op jit(solution)/shard_map/ppermute | solution.py:502
  49.9 9.6 %collective-permute-start.8 = (bf16[2,264,256]{2,1,0:T(8,128)(2,1)S(1)}, bf16[2,264,256]{2,1,0:T(8,128)(2,1)S(1)}, u32[]{:S(2)}, u32[]{:S(2)}) collective-permute-start(bf16[2,264,256]{2,1,0:T(8,128)(2,1)S(1)} %collective-permute-done.6.refs_1_), channel_id=1, source_target_pairs={{0,32},{32,64},{64,96},{96,128},{128,160},{160,192},{192,224},{224... | collective-permute-start | bytes 811016 | tf_op jit(solution)/shard_map/ppermute | solution.py:499
  59.5 28.3 %copy-start.6 = (f32[2048]{0:T(1024)S(1)}, f32[2048]{0:T(1024)}, u32[]{:S(2)}) copy-start(f32[2048]{0:T(1024)} %param.21) | copy-start | bytes 24580
  63.5 24.3 %copy-start.1 = (bf16[512,2048]{1,0:T(8,128)(2,1)S(1)}, bf16[512,2048]{1,0:T(8,128)(2,1)}, u32[]{:S(2)}) copy-start(bf16[512,2048]{1,0:T(8,128)(2,1)} %refs_0_.1) | copy-start | bytes 6291460
  63.6 24.3 %copy-start.5 = (bf16[64,2048]{1,0:T(8,128)(2,1)S(1)}, bf16[64,2048]{1,0:T(8,128)(2,1)}, u32[]{:S(2)}) copy-start(bf16[64,2048]{1,0:T(8,128)(2,1)} %refs_4_.1) | copy-start | bytes 786436
  63.6 24.3 %copy-start.7 = (s32[64,4]{0,1:T(4,128)S(1)}, s32[64,4]{0,1:T(4,128)}, u32[]{:S(2)}) copy-start(s32[64,4]{0,1:T(4,128)} %param.22) | copy-start | bytes 3076
  87.8 64.4 %copy-start.4 = (bf16[1,384,2048]{2,1,0:T(8,128)(2,1)S(1)}, bf16[1,384,2048]{2,1,0:T(8,128)(2,1)}, u32[]{:S(2)}) copy-start(bf16[1,384,2048]{2,1,0:T(8,128)(2,1)} %down_ref.1) | copy-start | bytes 4718596
  92.7 59.6 %copy-start.2 = (bf16[1,2048,384]{2,1,0:T(8,128)(2,1)S(1)}, bf16[1,2048,384]{2,1,0:T(8,128)(2,1)}, u32[]{:S(2)}) copy-start(bf16[1,2048,384]{2,1,0:T(8,128)(2,1)} %gate_ref.1) | copy-start | bytes 4718596
  92.7 59.6 %copy-start.3 = (bf16[1,2048,384]{2,1,0:T(8,128)(2,1)S(1)}, bf16[1,2048,384]{2,1,0:T(8,128)(2,1)}, u32[]{:S(2)}) copy-start(bf16[1,2048,384]{2,1,0:T(8,128)(2,1)} %up_ref.1) | copy-start | bytes 4718596
  156.9 6.4 %copy-start.11 = (f32[64,4]{0,1:T(4,128)S(1)}, f32[64,4]{0,1:T(4,128)}, u32[]{:S(2)}) copy-start(f32[64,4]{0,1:T(4,128)} %param.23) | copy-start | bytes 3076
  156.9 56.8 %all-to-all-start.3 = ((bf16[64,8,2048]{2,1,0:T(8,128)(2,1)}), bf16[64,8,2048]{2,1,0:T(8,128)(2,1)}, u32[]{:S(2)}, u32[]{:S(2)}) async-start(bf16[64,8,2048]{2,1,0:T(8,128)(2,1)} %expert.1), calls=%async_computation.3 | async-start | bytes 4194304 | tf_op jit(solution)/shard_map/all_to_all | solution.py:535
